TPU v7x, 512 devices: a whole 4x8x8 slice. The times are simulated.
512 devices in a mesh: sp: 32 (over z, x), tp: 16 (over y, core).
Axes of the slice: x: 4, y: 8, z: 8, core: 2. Of those that a mesh axis runs over, the one named last changes fastest.
Arguments:
- outer_gate: bfloat16 [512, 12288], P('tp', 'sp'), may hold values from -6 to 6
- inner_gate: bfloat16 [512, 12288], P('tp', 'sp'), may hold values from -6 to 6
- conv_input: bfloat16 [512, 12288], P('tp', 'sp'), may hold values from -6 to 6
- conv_taps: bfloat16 [3, 512], P(None, 'tp'), may hold values from -3.5 to 3.5
- mix_weight: bfloat16 [512, 2048], P(None, 'tp'), may hold values from -0.25 to 0.25
- residual: bfloat16 [12288, 2048], P('sp', 'tp'), may hold values from -24 to 24
- norm_gain: bfloat16 [2048], P('tp'), may hold values from 0.099609375 to 1.8984375
- routes: int32 [12288, 2], P('sp'), may hold values from 0 to 63, all different within a row; in each aligned block of 384 rows (0 to 383, 384 to 767, ...) at most 24 rows name the same one
- route_scores: float32 [12288, 2], P('sp'), may hold values from 0.05 to 1
- expert_gate: bfloat16 [64, 2048, 2048], P('sp', None, 'tp'), may hold values from -0.125 to 0.125
- expert_up: bfloat16 [64, 2048, 2048], P('sp', None, 'tp'), may hold values from -0.125 to 0.125
- expert_down: bfloat16 [64, 2048, 2048], P('sp', None, 'tp'), may hold values from -0.125 to 0.125
- shared_gate: bfloat16 [2048, 512], P(None, 'tp'), may hold values from -0.125 to 0.125
- shared_up: bfloat16 [2048, 512], P(None, 'tp'), may hold values from -0.125 to 0.125
- shared_down: bfloat16 [512, 2048], P(None, 'tp'), may hold values from -0.25 to 0.25
Outputs:
- layer_out: bfloat16 [12288, 2048], P('sp', 'tp')
Inputs may be any that keep to these rules, and one draw needn't show every extreme that they name: `routes`: within the rows of one index of sp (384 tokens), no expert is named by more than 24 of the token and choice pairs, a bound that some block reaches; the experts of one token differ.
All inputs are finite; a program needn't handle non-finite values.
Results may differ from a plain program's by a relative error of at most 0.014.
Values may be sent and summed in bfloat16 or wider, within the bound.
No kernel may reach another device: no remote copies, remote signals or barrier semaphores. Data moves between devices by JAX's collectives and lax.ppermute only.
A program may use at most 64 MiB of HBM per device.

v0:
```python
import jax
import jax.numpy as jnp
from jax import lax
from jax.sharding import PartitionSpec as P

D = 2048


epsilon = 1e-06
routed_scale = 2.5


def extended(array, sides, width):
    for axis, dim in sides:
        peers, length = (lax.axis_size(axis), array.shape[dim])
        up = [(i, (i + 1) % peers) for i in range(peers - 1)]
        down = [(j, i) for i, j in up]
        last = lax.slice_in_dim(array, length - width, length, axis=dim)
        first = lax.slice_in_dim(array, 0, width, axis=dim)
        before = lax.ppermute(last, axis, up)
        after = lax.ppermute(first, axis, down)
        array = jnp.concatenate([before, array, after], axis=dim)
    return array


def copy_for_each(array, axis):
    peers = lax.axis_size(axis)
    return lax.all_to_all(
        jnp.broadcast_to(array[None], (peers, *array.shape)), axis, 0, 0, tiled=True
    )


def taken_together(array, axis):
    return copy_for_each(array, axis).sum(axis=0)


def slot_tables(routes_block, expert_count, capacity):
    count_rows, top_count = routes_block.shape
    flat_route = routes_block.reshape(-1)
    onehot = (flat_route[:, None] == jnp.arange(expert_count, dtype=jnp.int32)[None, :]).astype(
        jnp.int32
    )
    before = jnp.cumsum(onehot, axis=0) - onehot
    position = jnp.sum(before * onehot, axis=1)
    slot_index = flat_route * capacity + position
    token_ids = jnp.arange(count_rows * top_count, dtype=jnp.int32) // top_count
    owners = jnp.full((expert_count * capacity,), -1, jnp.int32).at[slot_index].set(token_ids)
    return (slot_index.reshape(count_rows, top_count), owners)


def local(
    outer_gate,
    inner_gate,
    conv_input,
    conv_taps,
    mix_weight,
    residual,
    norm_gain,
    routes,
    route_scores,
    expert_gate,
    expert_up,
    expert_down,
    shared_gate,
    shared_up,
    shared_down,
):
    product = (inner_gate.astype(jnp.float32) * conv_input.astype(jnp.float32)).astype(jnp.bfloat16)
    padded = extended(product, (("sp", 1),), 1).astype(jnp.float32)
    kernel = conv_taps.astype(jnp.float32)
    filtered = (
        kernel[0][:, None] * padded[:, :-2]
        + kernel[1][:, None] * padded[:, 1:-1]
        + kernel[2][:, None] * padded[:, 2:]
    )
    mixed = (outer_gate.astype(jnp.float32) * filtered).astype(jnp.bfloat16)
    token_count = mixed.shape[1]
    rows_w = mix_weight
    projected = lax.dot_general(
        lax.all_gather(mixed, "tp", axis=0, tiled=True),
        rows_w,
        (((0,), (0,)), ((), ())),
        preferred_element_type=jnp.float32,
    )
    stream = (residual.astype(jnp.float32) + projected).astype(jnp.bfloat16)
    levels = stream.astype(jnp.float32)
    squares = taken_together(jnp.sum(levels * levels, axis=1), "tp")
    inverse_rms = lax.rsqrt(squares / D + epsilon)
    normed = (levels * inverse_rms[:, None] * norm_gain.astype(jnp.float32)).astype(jnp.bfloat16)
    whole_rows = lax.all_gather(normed, "tp", axis=1, tiled=True)
    shared_act = (
        jax.nn.silu(jnp.dot(whole_rows, shared_gate, preferred_element_type=jnp.float32))
        * jnp.dot(whole_rows, shared_up, preferred_element_type=jnp.float32)
    ).astype(jnp.bfloat16)
    rows_w = shared_down
    shared_out = jnp.dot(
        lax.all_gather(shared_act, "tp", axis=1, tiled=True),
        rows_w,
        preferred_element_type=jnp.float32,
    )
    group_count = lax.axis_size("sp")
    local_experts = expert_gate.shape[0]
    expert_count = local_experts * group_count
    capacity = 2 * token_count * routes.shape[1] // expert_count
    slot_index, owners = slot_tables(routes, expert_count, capacity)
    filled = owners >= 0
    source_ids = jnp.maximum(owners, 0)
    outgoing = jnp.where(filled[:, None], normed[source_ids], jnp.zeros((), jnp.bfloat16)).reshape(
        group_count, local_experts * capacity, -1
    )
    sliced = lax.all_to_all(outgoing, "sp", split_axis=0, concat_axis=1, tiled=True)
    received = lax.all_gather(sliced, "tp", axis=2, tiled=True)
    arrived = (
        received.reshape(group_count, local_experts, capacity, -1)
        .transpose(1, 0, 2, 3)
        .reshape(local_experts, group_count * capacity, -1)
    )
    gate_act = jnp.einsum("erd,edf->erf", arrived, expert_gate, preferred_element_type=jnp.float32)
    up_act = jnp.einsum("erd,edf->erf", arrived, expert_up, preferred_element_type=jnp.float32)
    hidden = (jax.nn.silu(gate_act) * up_act).astype(jnp.bfloat16)
    rows_w = expert_down
    expert_rows = jnp.einsum(
        "erf,efd->erd",
        lax.all_gather(hidden, "tp", axis=2, tiled=True),
        rows_w,
        preferred_element_type=jnp.float32,
    ).astype(jnp.bfloat16)
    feature_count = expert_rows.shape[2]
    regrouped = (
        expert_rows.reshape(local_experts, group_count, capacity, feature_count)
        .transpose(1, 0, 2, 3)
        .reshape(1, group_count * local_experts * capacity, feature_count)
    )
    returned = lax.all_to_all(regrouped, "sp", split_axis=1, concat_axis=0, tiled=True)
    flat_rows = returned.reshape(expert_count * capacity, feature_count)
    picked = flat_rows[slot_index].astype(jnp.float32)
    weights = route_scores / jnp.sum(route_scores, axis=1, keepdims=True) * routed_scale
    routed = jnp.einsum("tk,tkd->td", weights, picked)
    return (levels + routed + shared_out).astype(jnp.bfloat16)


def solution(mesh):
    in_specs = (
        P("tp", "sp"),
        P("tp", "sp"),
        P("tp", "sp"),
        P(None, "tp"),
        P(None, "tp"),
        P("sp", "tp"),
        P("tp"),
        P("sp", None),
        P("sp", None),
        P("sp", None, "tp"),
        P("sp", None, "tp"),
        P("sp", None, "tp"),
        P(None, "tp"),
        P(None, "tp"),
        P(None, "tp"),
    )
    out_specs = P("sp", "tp")
    return jax.shard_map(local, mesh=mesh, in_specs=in_specs, out_specs=out_specs, check_vma=False)
```

profile of v0, /device:TPU:1, one launch (start us, length us, event | category | flops | bytes accessed | tf_op | source)
XLA Modules:
  0.0 281.1 jit_solution(13468960967642711488)
XLA Ops:
  7.5 3.9 %collective-permute-start = (bf16[32,1]{1,0:T(8,128)(2,1)S(1)}, bf16[32,1]{1,0:T(8,128)(2,1)S(1)}, u32[]{:S(2)}, u32[]{:S(2)}) collective-permute-start(bf16[32,1]{1,0:T(8,128)(2,1)S(1)} %get-tuple-element.7), channel_id=1, source_target_pairs={{0,16},{16,32},{32,48},{48,64},{64,80},{80,96},{96,112},{112,128},... | collective-permute-start | bytes 200 | tf_op jit(solution)/shard_map/ppermute | solution.py:20
  11.4 1.3 collective-permute-start.1
  13.9 1.8 reduce-window.6
  16.5 3.4 %scatter_custom_fusion = s32[1536]{0:T(1024)S(1)} fusion(s32[768]{0:T(1024)S(1)} %fusion.18, s32[768]{0:T(1024)S(1)} %add_select_fusion, s32[]{:T(128)} %constant.23.clone.1), kind=kCustom, calls=%fused_computation.49 | custom fusion | bytes 6148 | tf_op jit(solution)/shard_map/scatter | solution.py:47
  22.6 19.5 %all_gather.15 = bf16[512,384]{1,0:T(8,128)(2,1)S(1)} all-gather(bf16[32,384]{1,0:T(8,128)(2,1)S(1)} %fusion.11), channel_id=1, replica_groups=mesh['sp'=32,'tp'=16] {'tp'}, dimensions={0}, use_global_device_ids=true | all-gather | bytes 417792 | tf_op jit(solution)/shard_map/all_gather | solution.py:80
  42.0 1.2 multiply_reduce_fusion.1
  43.9 4.5 %all-to-all-start = ((f32[16,1,384]{2,1,0:T(1,128)}), f32[16,1,384]{2,1,0:T(1,128)S(1)}, u32[]{:S(2)}, u32[]{:S(2)}) async-start(f32[16,1,384]{2,1,0:T(1,128)} %broadcast_in_dim.38), calls=%async_computation | async-start | bytes 49152 | tf_op jit(solution)/shard_map/all_to_all | solution.py:28
  49.2 6.6 %all-to-all-done = f32[16,1,384]{2,1,0:T(1,128)S(1)} async-done(((f32[16,1,384]{2,1,0:T(1,128)}), f32[16,1,384]{2,1,0:T(1,128)S(1)}, u32[]{:S(2)}, u32[]{:S(2)}) %all-to-all-start) | async-done | bytes 24608 | tf_op jit(solution)/shard_map/all_to_all | solution.py:28
  56.0 3.2 %gather_fusion = bf16[1536,128]{1,0:T(8,128)(2,1)S(1)} fusion(bf16[384,128]{1,0:T(8,128)(2,1)S(1)} %copy.69, s32[2048]{0:T(1024)S(1)} %pad_clamp_fusion), kind=kCustom, calls=%fused_computation | custom fusion | bytes 792576 | tf_op jit(solution)/shard_map/gather | solution.py:108
  59.5 28.7 %all_to_all.27 = bf16[32,48,128]{2,1,0:T(8,128)(2,1)} all-to-all(bf16[32,48,128]{2,1,0:T(8,128)(2,1)S(1)} %broadcast_select_fusion), channel_id=1, replica_groups=mesh['sp'=32,'tp'=16] {'sp'}, dimensions={0} | all-to-all | bytes 786432 | tf_op jit(solution)/shard_map/all_to_all | solution.py:111
  88.2 52.3 %all-gather.4.cloned.1.call-done = bf16[1,1536,2048]{2,1,0:T(8,128)(2,1)} async-done(((bf16[1,1536,128]{2,1,0:T(8,128)(2,1)}), bf16[1,1536,2048]{2,1,0:T(8,128)(2,1)}) %all-gather.4.cloned.1.call-update) | async-done | bytes 6291472 | tf_op jit(solution)/shard_map/all_gather | solution.py:112
  140.5 3.4 %copy.70 = bf16[2,32,24,2048]{3,2,1,0:T(8,128)(2,1)S(1)} copy(bf16[2,32,24,2048]{3,2,0,1:T(8,128)(2,1)} %bitcast.62) | data formatting | bytes 12582912 | tf_op jit(solution)/shard_map/transpose | solution.py:115
  143.9 1.8 fusion.20
  145.7 2.5 fusion
  149.3 58.0 %all-gather.6.cloned.1.call-done = bf16[2,768,2048]{2,1,0:T(8,128)(2,1)} async-done(((bf16[2,768,128]{2,1,0:T(8,128)(2,1)}), bf16[2,768,2048]{2,1,0:T(8,128)(2,1)}) %all-gather.6.cloned.1.call-update) | async-done | bytes 6291472 | tf_op jit(solution)/shard_map/all_gather | solution.py:124
  207.3 4.6 %convolution_convert_fusion = bf16[2,768,128]{2,1,0:T(8,128)(2,1)S(1)} fusion(bf16[2,768,2048]{2,1,0:T(8,128)(2,1)} %all-gather.6.cloned.1.call-done, bf16[2,2048,128]{2,1,0:T(8,128)(2,1)S(1)} %copy-done.7), kind=kOutput, calls=%fused_computation.5 | convolution fusion | flops 805502976 | bytes 7733248 | tf_op jit(solution)/shard_map/erf,efd->erd/dot_general | solution.py:122
  211.9 6.1 %copy.88 = bf16[1,1536,128]{2,0,1:T(2,128)(2,1)S(1)} copy(bf16[1,1536,128]{2,1,0:T(8,128)(2,1)S(1)} %bitcast.67) | data formatting | bytes 786432 | tf_op jit(solution)/shard_map/reshape | solution.py:132
  218.7 8.8 %reduce.7 = bf16[1536,128]{1,0:T(8,128)(2,1)S(1)} reduce(bf16[1536,1,128]{2,1,0:T(2,128)(2,1)S(1)} %bitcast.63, bf16[]{:T(256)} %broadcast.89), dimensions={1}, to_apply=%bitcast.56.reduce_sub_computation | reduce | bytes 786434
  228.3 9.9 %all-to-all-start.2 = ((bf16[32,2,3072]{2,1,0:T(2,128)(2,1)}), bf16[32,2,3072]{2,1,0:T(2,128)(2,1)S(1)}, u32[]{:S(2)}, u32[]{:S(2)}) async-start(bf16[32,2,3072]{2,1,0:T(2,128)(2,1)} %reshape.133), calls=%async_computation.2 | async-start | bytes 786432 | tf_op jit(solution)/shard_map/all_to_all | solution.py:134
  238.4 11.7 %all-gather.8.cloned.1.call-done = bf16[384,2048]{0,1:T(8,128)(2,1)} async-done(((bf16[384,128]{0,1:T(8,128)(2,1)}), bf16[384,2048]{0,1:T(8,128)(2,1)}) %all-gather.8.cloned.1.call-update) | async-done | bytes 1572880 | tf_op jit(solution)/shard_map/all_gather | solution.py:90
  250.1 1.7 fusion.21
  251.9 1.8 fusion.4
  253.7 16.9 %all_gather.19 = bf16[384,512]{0,1:T(8,128)(2,1)S(1)} all-gather(bf16[384,32]{0,1:T(8,128)(2,1)S(1)} %fusion.4), channel_id=1, replica_groups=mesh['sp'=32,'tp'=16] {'tp'}, dimensions={1}, use_global_device_ids=true | all-gather | bytes 417792 | tf_op jit(solution)/shard_map/all_gather | solution.py:97
  270.9 1.9 gather_fusion.1
  (69 shorter events, 12.2 us)
Async XLA Ops:
  6.5 137.4 %copy-start = (bf16[2,2048,128]{2,1,0:T(8,128)(2,1)S(1)}, bf16[2,2048,128]{2,1,0:T(8,128)(2,1)}, u32[]{:S(2)}) copy-start(bf16[2,2048,128]{2,1,0:T(8,128)(2,1)} %param.24) | copy-start | bytes 3145732
  7.5 14.2 %collective-permute-start = (bf16[32,1]{1,0:T(8,128)(2,1)S(1)}, bf16[32,1]{1,0:T(8,128)(2,1)S(1)}, u32[]{:S(2)}, u32[]{:S(2)}) collective-permute-start(bf16[32,1]{1,0:T(8,128)(2,1)S(1)} %get-tuple-element.7), channel_id=1, source_target_pairs={{0,16},{16,32},{32,48},{48,64},{64,80},{80,96},{96,112},{112,128},... | collective-permute-start | bytes 200 | tf_op jit(solution)/shard_map/ppermute | solution.py:20
  11.4 10.2 %collective-permute-start.1 = (bf16[32,1]{1,0:T(8,128)(2,1)S(1)}, bf16[32,1]{1,0:T(8,128)(2,1)S(1)}, u32[]{:S(2)}, u32[]{:S(2)}) collective-permute-start(bf16[32,1]{1,0:T(8,128)(2,1)S(1)} %get-tuple-element.8), channel_id=1, source_target_pairs={{16,0},{32,16},{48,32},{64,48},{80,64},{96,80},{112,96},{128,112},... | collective-permute-start | bytes 200 | tf_op jit(solution)/shard_map/ppermute | solution.py:21
  43.9 11.9 %all-to-all-start = ((f32[16,1,384]{2,1,0:T(1,128)}), f32[16,1,384]{2,1,0:T(1,128)S(1)}, u32[]{:S(2)}, u32[]{:S(2)}) async-start(f32[16,1,384]{2,1,0:T(1,128)} %broadcast_in_dim.38), calls=%async_computation | async-start | bytes 49152 | tf_op jit(solution)/shard_map/all_to_all | solution.py:28
  48.3 92.2 %all-gather.4.cloned.1.call-start = ((), (), s32[]{:S(2)}) async-start(), calls=%async_computation.3 | async-start | bytes 6684672 | tf_op jit(solution)/shard_map/all_gather | solution.py:112
  55.9 88.0 %copy-start.1 = (bf16[384,128]{0,1:T(8,128)(2,1)}, bf16[384,128]{0,1:T(8,128)(2,1)S(1)}, u32[]{:S(2)}) copy-start(bf16[384,128]{0,1:T(8,128)(2,1)S(1)} %multiply_convert_fusion) | copy-start | bytes 294916
  88.2 119.1 %all-gather.6.cloned.1.call-start = ((), (), s32[]{:S(2)}) async-start(), calls=%async_computation.4 | async-start | bytes 6684672 | tf_op jit(solution)/shard_map/all_gather | solution.py:124
  143.9 1.8 copy-start.6
  145.7 3.3 %copy-start.5 = (f32[384,2]{0,1:T(2,128)S(1)}, f32[384,2]{0,1:T(2,128)}, u32[]{:S(2)}) copy-start(f32[384,2]{0,1:T(2,128)} %param.23) | copy-start | bytes 9220
  145.7 61.6 %copy-start.7 = (bf16[2,2048,128]{2,1,0:T(8,128)(2,1)S(1)}, bf16[2,2048,128]{2,1,0:T(8,128)(2,1)}, u32[]{:S(2)}) copy-start(bf16[2,2048,128]{2,1,0:T(8,128)(2,1)} %param.26) | copy-start | bytes 3145732
  148.3 101.8 %all-gather.8.cloned.1.call-start = ((), (), s32[]{:S(2)}) async-start(), calls=%async_computation.5 | async-start | bytes 1671168 | tf_op jit(solution)/shard_map/all_gather | solution.py:90
  149.2 100.9 %copy-start.3 = (bf16[2048,32]{0,1:T(8,128)(2,1)S(1)}, bf16[2048,32]{0,1:T(8,128)(2,1)}, u32[]{:S(2)}) copy-start(bf16[2048,32]{0,1:T(8,128)(2,1)} %param.27) | copy-start | bytes 393220
  149.3 102.6 %copy-start.2 = (bf16[2048,32]{0,1:T(8,128)(2,1)S(1)}, bf16[2048,32]{0,1:T(8,128)(2,1)}, u32[]{:S(2)}) copy-start(bf16[2048,32]{0,1:T(8,128)(2,1)} %param.28) | copy-start | bytes 393220
  218.1 55.5 %copy-start.4 = (bf16[512,128]{1,0:T(8,128)(2,1)S(1)}, bf16[512,128]{1,0:T(8,128)(2,1)}, u32[]{:S(2)}) copy-start(bf16[512,128]{1,0:T(8,128)(2,1)} %param.29) | copy-start | bytes 393220
  228.3 42.2 %all-to-all-start.2 = ((bf16[32,2,3072]{2,1,0:T(2,128)(2,1)}), bf16[32,2,3072]{2,1,0:T(2,128)(2,1)S(1)}, u32[]{:S(2)}, u32[]{:S(2)}) async-start(bf16[32,2,3072]{2,1,0:T(2,128)(2,1)} %reshape.133), calls=%async_computation.2 | async-start | bytes 786432 | tf_op jit(solution)/shard_map/all_to_all | solution.py:134
Sparse Core Ops, SparseCore 0:
  88.3 52.1 all-gather.3
  148.4 58.8 all-gather.5
  209.4 40.6 all-gather.7
where the time goes:
time: 282 us; the launch traced here: 281 us
  waiting for transfers between devices  129 us (46%)
  blocking collectives  65 us (23%)
  local copies, waits for them, and re-layouts  24.6 us (9%)
  starting transfers between devices  19.9 us (7%)
  other arithmetic  15 us (5%)
  matrix products  13.9 us (5%)
  between operations  13.5 us (5%)
    all_gather x1, waiting for transfers between devices, local(): lax.all_gather(hidden, 'tp', axis=2, tiled=True)  58 us
    all_gather x1, waiting for transfers between devices, local(): received = lax.all_gather(sliced, 'tp', axis=2, tiled=True)  52.3 us
    all_to_all x1, blocking collectives, local(): lax.all_to_all(outgoing, 'sp', split_axis=0, concat_axis=1, tiled=True)  28.7 us
    all_gather x1, blocking collectives, local(): lax.all_gather(mixed, 'tp', axis=0, tiled=True)  19.5 us
    all_gather x1, blocking collectives, local(): lax.all_gather(shared_act, 'tp', axis=1, tiled=True)  16.9 us
    all_gather x1, waiting for transfers between devices, local(): whole_rows = lax.all_gather(normed, 'tp', axis=1, tiled=True)  11.7 us
    all_to_all x1, starting transfers between devices, local(): lax.all_to_all(regrouped, 'sp', split_axis=1, concat_axis=0, tiled=True)  9.9 us
    unnamed x2, other arithmetic  9.43 us
  transfers between devices with their start and end apart: 7, of which 4 were waited for; matrix products, arithmetic and copies ran while one was open for 12% of the time, Pallas kernels for 0%

commit v1 on v0

v1 whole, which is shorter than its diff:
```python
import jax
import jax.numpy as jnp
from jax import lax
from jax.experimental import pallas as pl
from jax.experimental.pallas import tpu as pltpu
from jax.sharding import Mesh, PartitionSpec as P


epsilon = 1e-06
routed_scale = 2.5
bf16, f32, i32 = jnp.bfloat16, jnp.float32, jnp.int32

D = 2048
TOK = 384
CAP = 24
SP = 32
EXPERTS = 64
HALF = SP // 2 * CAP
SHARE = TOK // 4
GAIN = 8
USED = HALF + SHARE
BLOCK = USED + GAIN
HROWS = HALF + SHARE // 4

NEAR = [(2 * y, 2 * (y ^ 1)) for y in range(8)] + [
    (2 * y + 1, 2 * ((y + (1 if y % 2 else 7)) % 8) + 1) for y in range(8)
]
DOWN = 2 * D
PACK = 3 * D
SDOWN = PACK + D // 2
WROWS = SDOWN + 512

VM = pl.BlockSpec(memory_space=pltpu.VMEM)
ANY = pl.BlockSpec(memory_space=pl.ANY)
MIB = 1 << 20


def dot(a, b):
    return lax.dot_general(a, b, (((1,), (0,)), ((), ())), preferred_element_type=f32)


def call(body, outs, count, scratch=(), limit=8, space=VM):
    return pl.pallas_call(
        body,
        out_shape=outs,
        in_specs=[space] * count,
        out_specs=jax.tree.map(lambda _: space, outs),
        scratch_shapes=scratch,
        compiler_params=pltpu.CompilerParams(vmem_limit_bytes=limit * MIB),
    )


def index(axis):
    return lax.axis_index(axis)


def pick_body(gate, up, down, sg, su, sd, own, other, pack, sem):
    yl = index("yl")
    copies = [
        (w.at[which], out.at[pl.ds(i * D, D)])
        for out, which in ((other, 1 - yl), (own, yl))
        for i, w in enumerate((gate, up, down))
    ] + [(sd, out.at[pl.ds(SDOWN, 512)]) for out in (other, own)]
    copies = [pltpu.make_async_copy(a, b, sem.at[i]) for i, (a, b) in enumerate(copies)]
    loads = [
        pltpu.make_async_copy(
            w.at[:, pl.ds(128 * b, 128)], pack.at[pl.ds(64 * b + 32 * i, 32)], sem.at[8 + 16 * i + b]
        )
        for i, w in enumerate((sg, su))
        for b in range(16)
    ]
    for copy in loads + copies:
        copy.start()
    for copy in loads:
        copy.wait()
    stores = [
        pltpu.make_async_copy(pack, out.at[pl.ds(PACK, D // 2)], sem.at[40 + i])
        for i, out in enumerate((own, other))
    ]
    for copy in stores:
        copy.start()
    for copy in copies + stores:
        copy.wait()


def mixer_body(outer, inner, conv, taps, before, after, out):
    product = (inner[...].astype(f32) * conv[...].astype(f32)).astype(bf16).astype(f32)
    lane = lax.broadcasted_iota(i32, product.shape, 1)
    left = jnp.where(lane == 0, before[...].astype(f32), pltpu.roll(product, 1, 1))
    right = jnp.where(lane == TOK - 1, after[...].astype(f32), pltpu.roll(product, TOK - 1, 1))
    i = lax.broadcasted_iota(i32, (32, 32), 0)
    j = lax.broadcasted_iota(i32, (32, 32), 1)
    k = taps[...].astype(f32)
    k = [jnp.sum(jnp.where(i == j, k[n : n + 1, :], 0.0), axis=1, keepdims=True) for n in range(3)]
    filtered = k[0] * left + k[1] * product + k[2] * right
    out[...] = (outer[...].astype(f32) * filtered).astype(bf16)


def stream_body(mixed, weight, residual, gain, out):
    projected = lax.dot_general(
        mixed[...], weight[...], (((0,), (0,)), ((), ())), preferred_element_type=f32
    )
    out[0:TOK, :] = (residual[...].astype(f32) + projected).astype(bf16)
    out[TOK : TOK + GAIN, :] = jnp.broadcast_to(gain[...], (GAIN, 128))


def meta_body(routes, scores, rows_out, cols_out):
    yl = index("yl")
    e = lax.broadcasted_iota(i32, (EXPERTS, TOK), 0)
    m0 = e == routes[0:1, :]
    m1 = e == routes[1:2, :]
    member = jnp.where(m0 | m1, 1.0, 0.0).astype(bf16)
    a = lax.broadcasted_iota(i32, (TOK, TOK), 0)
    b = lax.broadcasted_iota(i32, (TOK, TOK), 1)
    earlier = dot(member, jnp.where(a < b, 1.0, 0.0).astype(bf16))
    base = (lax.shift_right_logical(e, 1) * CAP + 1).astype(f32)
    value = jnp.where((e & 1) == yl, base + earlier, 0.0)
    s0 = jnp.sum(jnp.where(m0, value, 0.0), axis=0, keepdims=True) - 1.0
    s1 = jnp.sum(jnp.where(m1, value, 0.0), axis=0, keepdims=True) - 1.0
    row = lax.broadcasted_iota(i32, (8, TOK), 0)
    rows_out[...] = jnp.where(row == 0, s0, s1)
    total = scores[0:1, :] + scores[1:2, :]
    w0 = scores[0:1, :] / total * routed_scale
    w1 = scores[1:2, :] / total * routed_scale
    row = lax.broadcasted_iota(i32, (128, TOK), 0)
    table = jnp.where(row == 0, s0, jnp.where(row == 1, s1, jnp.where(row == 2, w0, w1)))
    cols_out[...] = table.T


def dispatch_body(aug, near, slots, send, shared):
    yl = index("yl")
    tokens = jnp.concatenate([aug[0:TOK, :], near[0:TOK, :]], axis=1)
    row = lax.broadcasted_iota(i32, (SP * CAP, TOK), 0).astype(f32)
    pick = (row == slots[0:1, :]) | (row == slots[1:2, :])
    send[...] = dot(jnp.where(pick, 1.0, 0.0).astype(bf16), tokens).astype(bf16)
    for core in range(2):
        start = pl.multiple_of((yl * 2 + core) * SHARE, SHARE)
        for h, x in enumerate((aug, near)):
            lanes = slice(128 * h, 128 * h + 128)
            shared[core, 0:SHARE, lanes] = x[pl.ds(start, SHARE), :]
            shared[core, SHARE : SHARE + GAIN, lanes] = x[TOK : TOK + GAIN, :]


def silu(v):
    return v * (1.0 / (1.0 + jnp.exp(-v)))


def placed(own, up, down, up2, down2):
    yh, yl = index("yh"), index("yl")
    return (
        (2 * yh + yl, own.at[0], own.at[1]),
        (2 * ((yh + 3) % 4) + yl, up.at[0], up.at[1]),
        (2 * ((yh + 1) % 4) + yl, down.at[0], down.at[1]),
        (2 * ((yh + 2) % 4) + yl, up2.at[0], down2.at[0]),
    )


def slice_of(y, core, near):
    if near:
        yl = index("yl")
        y = (y + 2 * yl + 7) % 8 if core else y + 1 - 2 * yl
    return 2 * y + core


def up_body(*refs):
    ring, (wa, wb, wc, wd), (out, normed, hidden) = refs[0:5], refs[5:9], refs[9:]
    c = index("c")
    blocks = placed(*ring)
    total = jnp.zeros((USED, 128), f32)
    for _, *halves in blocks:
        for x in halves:
            for h in range(2):
                v = x[0:USED, 128 * h : 128 * h + 128].astype(f32)
                total = total + v * v
    inverse = lax.rsqrt(jnp.sum(total, axis=1, keepdims=True) / D + epsilon)
    for y, *halves in blocks:
        for core, x in enumerate(halves):
            for h in range(2):
                lanes = slice(128 * h, 128 * h + 128)
                gain = x[USED:BLOCK, lanes].astype(f32)[0:1, :]
                column = pl.ds(pl.multiple_of(128 * slice_of(y, core, h), 128), 128)
                normed[:, column] = (x[0:USED, lanes].astype(f32) * inverse * gain).astype(bf16)
    x = normed[0:HALF, :]
    for pair, core in (((wa, wb), c), ((wc, wd), 1 - c)):
        g = dot(x, jnp.concatenate([w[0:D, :] for w in pair], axis=1))
        u = dot(x, jnp.concatenate([w[D : 2 * D, :] for w in pair], axis=1))
        out[core, 0:HALF, :] = (silu(g) * u).astype(bf16)
    packed = jnp.concatenate(
        [
            jnp.concatenate([w[PACK + 64 * b : PACK + 64 * b + 64, :] for b in range(16)], axis=1)
            for w in (wa, wc, wb, wd)
        ],
        axis=0,
    )
    s = lax.dot_general(
        normed[HALF:, :], packed, (((1,), (1,)), ((), ())), preferred_element_type=f32
    )
    h = (silu(s) * pltpu.roll(s, 256 - 32, 1)).astype(bf16)
    i = lax.broadcasted_iota(i32, (256, 128), 0)
    j = lax.broadcasted_iota(i32, (256, 128), 1)
    goes = (lax.shift_right_logical(i, 6) * 32 + (i & 31)) ^ (c * 32)
    perm = jnp.where(((i & 32) == 0) & (goes == j), 1.0, 0.0).astype(bf16)
    hidden[...] = dot(h, perm)
    for half in range(2):
        n = 48 * half
        out[half, HALF:HROWS, :] = jnp.concatenate(
            [hidden[n : n + 24, :], hidden[n + 24 : n + 48, :]], axis=1
        ).astype(bf16)


def down_body(*refs):
    ring, (wa, wb, wc, wd), (back, give, skeep, sgive, hidden) = refs[0:5], refs[5:9], refs[9:]
    blocks = placed(*ring)

    def rows_of(pair, first, count):
        n = pl.multiple_of(first, 32)
        return jnp.concatenate([w[pl.ds(n, count), :] for w in pair], axis=1)

    for pair, out, sout in (((wc, wd), give, sgive), ((wa, wb), back.at[index("c")], skeep)):
        total = jnp.zeros((HALF, 256), f32)
        shared = jnp.zeros((SHARE, 256), f32)
        for y, *halves in blocks:
            for core, x in enumerate(halves):
                w = [rows_of(pair, DOWN + 128 * slice_of(y, core, h), 128) for h in range(2)]
                total = total + dot(x[0:HALF, :], jnp.concatenate(w, axis=0))
                tail = x[HALF:HROWS, :].astype(f32)
                hidden[48 * core : 48 * core + 24, :] = tail[:, 0:128]
                hidden[48 * core + 24 : 48 * core + 48, :] = tail[:, 128:256]
            w = [
                rows_of(pair, SDOWN + 32 * slice_of(y, core, h), 32)
                for h in range(2)
                for core in range(2)
            ]
            shared = shared + dot(hidden[...].astype(bf16), jnp.concatenate(w, axis=0))
        out[...] = total.astype(bf16)
        sout[...] = shared


def combine_body(rows, cols, skeep, sother, keep, give, acc):
    yl, c = index("yl"), index("c")
    n = SP * CAP
    slot = lax.broadcasted_iota(i32, (TOK, n), 1).astype(f32)
    meta = cols[...]
    first = dot(jnp.where(slot == meta[:, 0:1], 1.0, 0.0).astype(bf16), rows[...])
    second = dot(jnp.where(slot == meta[:, 1:2], 1.0, 0.0).astype(bf16), rows[...])
    acc[...] = meta[:, 2:3] * first + meta[:, 3:4] * second
    for core, part in ((c, skeep), (1 - c, sother)):
        start = pl.multiple_of((yl * 2 + core) * SHARE, SHARE)
        acc[pl.ds(start, SHARE), :] += part[...]
    keep[...] = acc[:, 0:128]
    give[...] = acc[:, 128:256]


def final_body(aug, keep, other, out):
    out[...] = (aug[0:TOK, :].astype(f32) + keep[...] + other[...]).astype(bf16)


def sds(shape, dtype=bf16):
    return jax.ShapeDtypeStruct(shape, dtype)


def ring(block, after=None):
    up = [(i, (i + 1) % 4) for i in range(4)]
    down = [(j, i) for i, j in up]
    u = lax.ppermute(block, "yh", up)
    d = lax.ppermute(block, "yh", down)
    if after is not None:
        u, d, after = lax.optimization_barrier((u, d, after))
    u2 = lax.ppermute(u[:1], "yh", up)
    d2 = lax.ppermute(d[1:], "yh", down)
    return (block, u, d, u2, d2), after


def layer(
    outer_gate,
    inner_gate,
    conv_input,
    conv_taps,
    mix_weight,
    residual,
    norm_gain,
    routes,
    route_scores,
    expert_gate,
    expert_up,
    expert_down,
    shared_gate,
    shared_up,
    shared_down,
):
    c = index("c")
    swap = [(0, 1), (1, 0)]
    tp = ("yh", "yl", "c")

    def edge(i):
        a = lax.slice_in_dim(inner_gate, i, i + 1, axis=1).astype(f32)
        b = lax.slice_in_dim(conv_input, i, i + 1, axis=1).astype(f32)
        return (a * b).astype(bf16)

    up = [(i, i + 1) for i in range(SP - 1)]
    before = lax.ppermute(edge(TOK - 1), "sp", up)
    after = lax.ppermute(edge(0), "sp", [(j, i) for i, j in up])

    slots, cols = call(meta_body, (sds((8, TOK), f32), sds((TOK, 128), f32)), 2)(
        routes.T, route_scores.T
    )
    w_own, w_other = call(
        pick_body,
        (sds((WROWS, 128)), sds((WROWS, 128))),
        6,
        [pltpu.VMEM((D // 2, 128), bf16), pltpu.SemaphoreType.DMA((42,))],
        space=ANY,
    )(
        *(
            pltpu.with_memory_space_constraint(w, pltpu.HBM)
            for w in (expert_gate, expert_up, expert_down, shared_gate.T, shared_up.T, shared_down)
        )
    )

    mixed = call(mixer_body, sds((32, TOK)), 6)(
        outer_gate, inner_gate, conv_input, conv_taps, before, after
    )
    mixed = lax.all_gather(mixed, ("yh", "yl", "c"), axis=0, tiled=True)
    aug = call(stream_body, sds((TOK + GAIN, 128)), 4)(
        mixed, mix_weight, residual, norm_gain.reshape(1, 128)
    )
    near = lax.ppermute(aug, tp, NEAR)
    near, w_other, w_own = lax.optimization_barrier((near, w_other, w_own))
    w_got = lax.ppermute(w_other, tp, NEAR)
    w_own_c = lax.ppermute(w_own, "c", swap)
    send, shared = call(
        dispatch_body, (sds((SP * CAP, 256)), sds((2, SHARE + GAIN, 256))), 3
    )(aug, near, slots)
    arrived = lax.all_to_all(send.reshape(SP, CAP, 256), "sp", 0, 0, tiled=True)
    block = jnp.concatenate([arrived.reshape(2, HALF, 256), shared], axis=1)
    block = lax.all_to_all(block, "c", 0, 0, tiled=True)
    x_ring, w_got = ring(block, w_got)
    w_got_c = lax.ppermute(w_got, "c", swap)
    weights = (w_own, w_got, w_own_c, w_got_c)

    hidden = call(
        up_body,
        sds((2, HROWS, 256)),
        9,
        [pltpu.VMEM((USED, D), bf16), pltpu.VMEM((SHARE, 128), f32)],
        limit=16,
    )(*x_ring, *weights)
    h_ring, _ = ring(hidden)
    back, give, skeep, sgive = call(
        down_body,
        (sds((2, HALF, 256)), sds((HALF, 256)), sds((SHARE, 256), f32), sds((SHARE, 256), f32)),
        9,
        [pltpu.VMEM((SHARE, 128), f32)],
        limit=12,
    )(*h_ring, *weights)
    got = lax.ppermute(give, "c", swap)
    sgot = lax.ppermute(sgive, "c", swap)
    back = lax.dynamic_update_index_in_dim(back, got, 1 - c, 0)
    back = lax.all_to_all(back.reshape(SP, CAP, 256), "sp", 0, 0, tiled=True)
    mine, other = call(
        combine_body, (sds((TOK, 128), f32), sds((TOK, 128), f32)), 4, [pltpu.VMEM((TOK, 256), f32)]
    )(back.reshape(SP * CAP, 256), cols, skeep, sgot)
    other = lax.ppermute(other, tp, NEAR)
    return call(final_body, sds((TOK, 128)), 3)(aug, mine, other)


def solution(mesh):
    fine = Mesh(mesh.devices.reshape(SP, 4, 2, 2), ("sp", "yh", "yl", "c"))
    tp = ("yh", "yl", "c")
    in_specs = (
        P(tp, "sp"),
        P(tp, "sp"),
        P(tp, "sp"),
        P(None, tp),
        P(None, tp),
        P("sp", tp),
        P(tp),
        P("sp", None),
        P("sp", None),
        P("sp", None, tp),
        P("sp", None, tp),
        P("sp", None, tp),
        P(None, tp),
        P(None, tp),
        P(None, tp),
    )
    return jax.shard_map(
        layer, mesh=fine, in_specs=in_specs, out_specs=P("sp", tp), check_vma=False
    )
```

time: 282 us -> 209 us (0.74)
  waiting for transfers between devices: 129 us -> 59.6 us
  starting transfers between devices: 19.9 us -> 74.8 us
  local copies, waits for them, and re-layouts: 24.6 us -> 6.1 us
  other arithmetic: 15 us -> 0.86 us
  matrix products: 13.9 us -> 0 us
  between operations: 13.5 us -> 0.28 us
  blocking collectives: 65 us -> 54 us
  Pallas kernels: 0 us -> 10.4 us
    all_gather x3 -> x0, waiting for transfers between devices: 122 us -> none  [the longest x1 58 us: local(): lax.all_gather(hidden, 'tp', axis=2, tiled=True)]
    ppermute x2 -> x17, starting transfers between devices: 5.22 us -> 59.5 us  [the longest x2 9.75 us: ring(): d = lax.ppermute(block, 'yh', down)]
    ppermute x2 -> x17, waiting for transfers between devices: 0.01 us -> 49.2 us  [the longest x2 24 us: ring(): u = lax.ppermute(block, 'yh', up)]
    all_gather x2 -> x1, blocking collectives: 36.3 us -> 20.6 us  [layer(): mixed = lax.all_gather(mixed, ('yh', 'yl', 'c'), axis=0, tiled=True)]
    dot_general x7 -> x0, matrix products: 13.9 us -> none  [the longest x1 4.57 us: local(): jnp.einsum('erf,efd->erd', lax.all_gather(hidden, 'tp', axis=2, tiled=Tru...]
    pallas_call x0 -> x9, Pallas kernels: none -> 10.4 us  [the longest x1 3.65 us: layer(): call(up_body, sds((2, HROWS, 256)), 9, [pltpu.VMEM((USED, D), bf16), pltp...]
    unnamed x2 -> x0, other arithmetic: 9.43 us -> none
    reshape x2 -> x0, local copies, waits for them, and re-layouts: 6.16 us -> none  [the longest x1 6.12 us: local(): regrouped = expert_rows.reshape(local_experts, group_count, capacity, fea...]
  transfers between devices with their start and end apart: 7 -> 18, of which waited for: 4 -> 13; matrix products, arithmetic and copies ran while one was open for 12% -> 0% of each run, Pallas kernels for 0% -> 2%
where the time goes in v1:
time: 209 us; the launch traced here: 206 us
  starting transfers between devices  74.8 us (36%)
  waiting for transfers between devices  59.6 us (29%)
  blocking collectives  54 us (26%)
  Pallas kernels  10.4 us (5%)
  local copies, waits for them, and re-layouts  6.1 us (3%)
    all_to_all x1, blocking collectives, layer(): arrived = lax.all_to_all(send.reshape(SP, CAP, 256), 'sp', 0, 0, tiled=True)  28.4 us
    ppermute x2, waiting for transfers between devices, ring(): u = lax.ppermute(block, 'yh', up)  24 us
    all_gather x1, blocking collectives, layer(): mixed = lax.all_gather(mixed, ('yh', 'yl', 'c'), axis=0, tiled=True)  20.6 us
    all_to_all x1, starting transfers between devices, layer(): back = lax.all_to_all(back.reshape(SP, CAP, 256), 'sp', 0, 0, tiled=True)  15.3 us
    all_to_all x1, waiting for transfers between devices, layer(): back = lax.all_to_all(back.reshape(SP, CAP, 256), 'sp', 0, 0, tiled=True)  10.4 us
    ppermute x2, starting transfers between devices, ring(): d = lax.ppermute(block, 'yh', down)  9.75 us
    ppermute x2, starting transfers between devices, ring(): d2 = lax.ppermute(d[1:], 'yh', down)  7.83 us
    ppermute x2, waiting for transfers between devices, ring(): d2 = lax.ppermute(d[1:], 'yh', down)  7.71 us
  transfers between devices with their start and end apart: 18, of which 13 were waited for; matrix products, arithmetic and copies ran while one was open for 0% of the time, Pallas kernels for 2%

profile of v1, /device:TPU:1, one launch (start us, length us, event | category | flops | bytes accessed | tf_op | source)
XLA Modules:
  0.0 206.0 jit_solution(16429188221385183613)
XLA Ops:
  0.8 3.9 %collective-permute-start = (bf16[32,1]{1,0:T(8,128)(2,1)S(1)}, bf16[32,1]{1,0:T(8,128)(2,1)S(1)}, u32[]{:S(2)}, u32[]{:S(2)}) collective-permute-start(bf16[32,1]{1,0:T(8,128)(2,1)S(1)} %get-tuple-element.42), channel_id=1, source_target_pairs={{0,16},{16,32},{32,48},{48,64},{64,80},{80,96},{96,112},{112,128},... | collective-permute-start | bytes 200 | tf_op jit(solution)/shard_map/ppermute | solution.py:301
  6.1 3.1 %collective-permute-done.1.after = bf16[32,1]{1,0:T(8,128)(2,1)S(1)} collective-permute-done((bf16[32,1]{1,0:T(8,128)(2,1)S(1)}, bf16[32,1]{1,0:T(8,128)(2,1)S(1)}, u32[]{:S(2)}, u32[]{:S(2)}) %collective-permute-start.1) | collective-permute-done | bytes 96 | tf_op jit(solution)/shard_map/ppermute | solution.py:302
  12.2 20.6 %all_gather.3.mixed = bf16[512,384]{1,0:T(8,128)(2,1)S(1)} all-gather(bf16[32,384]{1,0:T(8,128)(2,1)S(1)} %shard_map.145), channel_id=1, replica_groups=mesh['sp'=32,'yh'=4,'yl'=2,'c'=2] {'yh','yl','c'}, dimensions={0}, use_global_device_ids=true | all-gather | bytes 417792 | tf_op jit(solution)/shard_map/all_gather | solution.py:323
  35.6 3.4 %collective-permute-start.2 = (bf16[392,128]{1,0:T(8,128)(2,1)S(1)}, bf16[392,128]{1,0:T(8,128)(2,1)S(1)}, u32[]{:S(2)}, u32[]{:S(2)}) collective-permute-start(bf16[392,128]{1,0:T(8,128)(2,1)S(1)} %shard_map.146.aug), channel_id=1, source_target_pairs={{0,2},{2,0},{4,6},{6,4},{8,10},{10,8},{12,14},{14,12},{1,15},{3,5}... | collective-permute-start | bytes 301064 | tf_op jit(solution)/shard_map/ppermute | solution.py:327
  42.2 3.4 %collective-permute-start.5 = (bf16[7680,128]{1,0:T(8,128)(2,1)S(1)}, bf16[7680,128]{1,0:T(8,128)(2,1)S(1)}, u32[]{:S(2)}, u32[]{:S(2)}) collective-permute-start(bf16[7680,128]{1,0:T(8,128)(2,1)S(1)} %get-tuple-element.29), channel_id=1, source_target_pairs={{0,2},{2,0},{4,6},{6,4},{8,10},{10,8},{12,14},{14,12},{1,15},{3,5}... | collective-permute-start | bytes 5898248 | tf_op jit(solution)/shard_map/ppermute | solution.py:329
  46.3 28.4 %all_to_all.15 = bf16[32,24,256]{2,1,0:T(8,128)(2,1)S(1)} all-to-all(bf16[32,24,256]{2,1,0:T(8,128)(2,1)S(1)} %bitcast.12), channel_id=1, replica_groups=mesh['sp'=32,'yh'=4,'yl'=2,'c'=2] {'sp'}, dimensions={0} | all-to-all | bytes 786432 | tf_op jit(solution)/shard_map/all_to_all | solution.py:334
  74.8 5.0 %all_to_all.16.refs_0_ = bf16[2,488,256]{2,1,0:T(8,128)(2,1)S(1)} all-to-all(bf16[2,488,256]{2,1,0:T(8,128)(2,1)S(1)} %pad_maximum_fusion), channel_id=1, replica_groups=mesh['sp'=32,'yh'=4,'yl'=2,'c'=2] {'c'}, dimensions={0} | all-to-all | bytes 999424 | tf_op jit(solution)/shard_map/all_to_all | solution.py:336
  81.7 5.5 %collective-permute-start.4 = (bf16[2,488,256]{2,1,0:T(8,128)(2,1)S(1)}, bf16[2,488,256]{2,1,0:T(8,128)(2,1)S(1)}, u32[]{:S(2)}, u32[]{:S(2)}) collective-permute-start(bf16[2,488,256]{2,1,0:T(8,128)(2,1)S(1)} %all_to_all.16.refs_0_), channel_id=1, source_target_pairs={{4,0},{8,4},{12,8},{0,12},{5,1},{9,5},{13,9},{1,13},{6,2},{10,6},{... | collective-permute-start | bytes 1499144 | tf_op jit(solution)/shard_map/ppermute | solution.py:266
  87.1 2.8 %collective-permute-start.8 = (bf16[7680,128]{1,0:T(8,128)(2,1)S(1)}, bf16[7680,128]{1,0:T(8,128)(2,1)S(1)}, u32[]{:S(2)}, u32[]{:S(2)}) collective-permute-start(bf16[7680,128]{1,0:T(8,128)(2,1)S(1)} %get-tuple-element.32.refs_5_), channel_id=1, source_target_pairs={{0,1},{1,0},{2,3},{3,2},{4,5},{5,4},{6,7},{7,6},{8,9},{9,8},{10,11... | collective-permute-start | bytes 5898248 | tf_op jit(solution)/shard_map/ppermute | solution.py:330
  90.0 17.2 %collective-permute-done.3.refs_1_ = bf16[2,488,256]{2,1,0:T(8,128)(2,1)S(1)} collective-permute-done((bf16[2,488,256]{2,1,0:T(8,128)(2,1)S(1)}, bf16[2,488,256]{2,1,0:T(8,128)(2,1)S(1)}, u32[]{:S(2)}, u32[]{:S(2)}) %collective-permute-start.3) | collective-permute-done | bytes 499744 | tf_op jit(solution)/shard_map/ppermute | solution.py:265
  112.3 4.7 %collective-permute-start.6 = (bf16[1,488,256]{2,1,0:T(8,128)(2,1)S(1)}, bf16[1,488,256]{2,1,0:T(8,128)(2,1)S(1)}, u32[]{:S(2)}, u32[]{:S(2)}) collective-permute-start(bf16[1,488,256]{2,1,0:T(8,128)(2,1)S(1)} %slice.28), channel_id=1, source_target_pairs={{0,4},{4,8},{8,12},{12,0},{1,5},{5,9},{9,13},{13,1},{2,6},{6,10},{... | collective-permute-start | bytes 749576 | tf_op jit(solution)/shard_map/ppermute | solution.py:269
  119.8 4.1 %collective-permute-done.6.refs_3_ = bf16[1,488,256]{2,1,0:T(8,128)(2,1)S(1)} collective-permute-done((bf16[1,488,256]{2,1,0:T(8,128)(2,1)S(1)}, bf16[1,488,256]{2,1,0:T(8,128)(2,1)S(1)}, u32[]{:S(2)}, u32[]{:S(2)}) %collective-permute-start.6) | collective-permute-done | bytes 249888 | tf_op jit(solution)/shard_map/ppermute | solution.py:269
  123.9 3.3 %collective-permute-done.7.refs_4_ = bf16[1,488,256]{2,1,0:T(8,128)(2,1)S(1)} collective-permute-done((bf16[1,488,256]{2,1,0:T(8,128)(2,1)S(1)}, bf16[1,488,256]{2,1,0:T(8,128)(2,1)S(1)}, u32[]{:S(2)}, u32[]{:S(2)}) %collective-permute-start.7) | collective-permute-done | bytes 249888 | tf_op jit(solution)/shard_map/ppermute | solution.py:270
  127.2 3.6 %shard_map.150.refs_0_ = bf16[2,408,256]{2,1,0:T(8,128)(2,1)S(1)} custom-call(bf16[2,488,256]{2,1,0:T(8,128)(2,1)S(1)} %all_to_all.16.refs_0_, bf16[2,488,256]{2,1,0:T(8,128)(2,1)S(1)} %collective-permute-done.3.refs_1_, bf16[2,488,256]{2,1,0:T(8,128)(2,1)S(1)} %collective-permute-done.4.refs_2_, bf16[1,488,256]{2,1,0:T(8,128)(2,1)S(1)} %collective-permute-done.6.refs_3_, ...), custom_call_target="tpu_custom_call" | custom-call | tf_op jit(solution)/shard_map/pallas_call | solution.py:341
  130.8 3.1 %collective-permute-start.10 = (bf16[2,408,256]{2,1,0:T(8,128)(2,1)S(1)}, bf16[2,408,256]{2,1,0:T(8,128)(2,1)S(1)}, u32[]{:S(2)}, u32[]{:S(2)}) collective-permute-start(bf16[2,408,256]{2,1,0:T(8,128)(2,1)S(1)} %shard_map.150.refs_0_), channel_id=1, source_target_pairs={{0,4},{4,8},{8,12},{12,0},{1,5},{5,9},{9,13},{13,1},{2,6},{6,10},{... | collective-permute-start | bytes 1253384 | tf_op jit(solution)/shard_map/ppermute | solution.py:265
  134.0 4.3 %collective-permute-start.11 = (bf16[2,408,256]{2,1,0:T(8,128)(2,1)S(1)}, bf16[2,408,256]{2,1,0:T(8,128)(2,1)S(1)}, u32[]{:S(2)}, u32[]{:S(2)}) collective-permute-start(bf16[2,408,256]{2,1,0:T(8,128)(2,1)S(1)} %shard_map.150.refs_0_), channel_id=1, source_target_pairs={{4,0},{8,4},{12,8},{0,12},{5,1},{9,5},{13,9},{1,13},{6,2},{10,6},{... | collective-permute-start | bytes 1253384 | tf_op jit(solution)/shard_map/ppermute | solution.py:266
  138.3 6.8 %collective-permute-done.10.refs_1_ = bf16[2,408,256]{2,1,0:T(8,128)(2,1)S(1)} collective-permute-done((bf16[2,408,256]{2,1,0:T(8,128)(2,1)S(1)}, bf16[2,408,256]{2,1,0:T(8,128)(2,1)S(1)}, u32[]{:S(2)}, u32[]{:S(2)}) %collective-permute-start.10) | collective-permute-done | bytes 417824 | tf_op jit(solution)/shard_map/ppermute | solution.py:265
  147.3 5.2 %collective-permute-start.13 = (bf16[1,408,256]{2,1,0:T(8,128)(2,1)S(1)}, bf16[1,408,256]{2,1,0:T(8,128)(2,1)S(1)}, u32[]{:S(2)}, u32[]{:S(2)}) collective-permute-start(bf16[1,408,256]{2,1,0:T(8,128)(2,1)S(1)} %slice.33), channel_id=1, source_target_pairs={{4,0},{8,4},{12,8},{0,12},{5,1},{9,5},{13,9},{1,13},{6,2},{10,6},{... | collective-permute-start | bytes 626696 | tf_op jit(solution)/shard_map/ppermute | solution.py:270
  154.4 4.4 %collective-permute-done.13.refs_4_ = bf16[1,408,256]{2,1,0:T(8,128)(2,1)S(1)} collective-permute-done((bf16[1,408,256]{2,1,0:T(8,128)(2,1)S(1)}, bf16[1,408,256]{2,1,0:T(8,128)(2,1)S(1)}, u32[]{:S(2)}, u32[]{:S(2)}) %collective-permute-start.13) | collective-permute-done | bytes 208928 | tf_op jit(solution)/shard_map/ppermute | solution.py:270
  160.7 5.5 %collective-permute-start.14 = (bf16[384,256]{1,0:T(8,128)(2,1)S(1)}, bf16[384,256]{1,0:T(8,128)(2,1)S(1)}, u32[]{:S(2)}, u32[]{:S(2)}) collective-permute-start(bf16[384,256]{1,0:T(8,128)(2,1)S(1)} %get-tuple-element.35), channel_id=1, source_target_pairs={{0,1},{1,0},{2,3},{3,2},{4,5},{5,4},{6,7},{7,6},{8,9},{9,8},{10,11... | collective-permute-start | bytes 589832 | tf_op jit(solution)/shard_map/ppermute | solution.py:356
  167.9 15.3 %all-to-all-start.2 = ((bf16[32,24,256]{2,1,0:T(8,128)(2,1)}), bf16[32,24,256]{2,1,0:T(8,128)(2,1)S(1)}, u32[]{:S(2)}, u32[]{:S(2)}) async-start(bf16[32,24,256]{2,1,0:T(8,128)(2,1)} %bitcast.8), calls=%async_computation.2 | async-start | bytes 786432 | tf_op jit(solution)/shard_map/all_to_all | solution.py:359
  186.7 10.4 %all-to-all-done.2 = bf16[32,24,256]{2,1,0:T(8,128)(2,1)S(1)} async-done(((bf16[32,24,256]{2,1,0:T(8,128)(2,1)}), bf16[32,24,256]{2,1,0:T(8,128)(2,1)S(1)}, u32[]{:S(2)}, u32[]{:S(2)}) %all-to-all-start.2) | async-done | bytes 393248 | tf_op jit(solution)/shard_map/all_to_all | solution.py:359
  197.7 4.6 %collective-permute-start.16 = (f32[384,128]{1,0:T(8,128)S(1)}, f32[384,128]{1,0:T(8,128)S(1)}, u32[]{:S(2)}, u32[]{:S(2)}) collective-permute-start(f32[384,128]{1,0:T(8,128)S(1)} %get-tuple-element.40), channel_id=1, source_target_pairs={{0,2},{2,0},{4,6},{6,4},{8,10},{10,8},{12,14},{14,12},{1,15},{3,5}... | collective-permute-start | bytes 589832 | tf_op jit(solution)/shard_map/ppermute | solution.py:363
  202.3 3.1 %collective-permute-done.16.other = f32[384,128]{1,0:T(8,128)S(1)} collective-permute-done((f32[384,128]{1,0:T(8,128)S(1)}, f32[384,128]{1,0:T(8,128)S(1)}, u32[]{:S(2)}, u32[]{:S(2)}) %collective-permute-start.16) | collective-permute-done | bytes 196640 | tf_op jit(solution)/shard_map/ppermute | solution.py:363
  (49 shorter events, 34.0 us)
Async XLA Ops:
  0.8 5.2 %collective-permute-start = (bf16[32,1]{1,0:T(8,128)(2,1)S(1)}, bf16[32,1]{1,0:T(8,128)(2,1)S(1)}, u32[]{:S(2)}, u32[]{:S(2)}) collective-permute-start(bf16[32,1]{1,0:T(8,128)(2,1)S(1)} %get-tuple-element.42), channel_id=1, source_target_pairs={{0,16},{16,32},{32,48},{48,64},{64,80},{80,96},{96,112},{112,128},... | collective-permute-start | bytes 200 | tf_op jit(solution)/shard_map/ppermute | solution.py:301
  4.8 4.4 %collective-permute-start.1 = (bf16[32,1]{1,0:T(8,128)(2,1)S(1)}, bf16[32,1]{1,0:T(8,128)(2,1)S(1)}, u32[]{:S(2)}, u32[]{:S(2)}) collective-permute-start(bf16[32,1]{1,0:T(8,128)(2,1)S(1)} %get-tuple-element.41), channel_id=1, source_target_pairs={{16,0},{32,16},{48,32},{64,48},{80,64},{96,80},{112,96},{128,112},... | collective-permute-start | bytes 200 | tf_op jit(solution)/shard_map/ppermute | solution.py:302
  9.2 0.7 copy-start.2
  10.6 0.7 copy-start.4
  32.8 0.9 copy-start
  33.7 0.9 copy-start.1
  35.2 10.3 %copy-start.5 = (s32[384,2]{0,1:T(2,128)S(1)}, s32[384,2]{0,1:T(2,128)}, u32[]{:S(2)}) copy-start(s32[384,2]{0,1:T(2,128)} %param.22) | copy-start | bytes 9220
  35.2 10.3 %copy-start.6 = (f32[384,2]{0,1:T(2,128)S(1)}, f32[384,2]{0,1:T(2,128)}, u32[]{:S(2)}) copy-start(f32[384,2]{0,1:T(2,128)} %param.23) | copy-start | bytes 9220
  35.6 6.6 %collective-permute-start.2 = (bf16[392,128]{1,0:T(8,128)(2,1)S(1)}, bf16[392,128]{1,0:T(8,128)(2,1)S(1)}, u32[]{:S(2)}, u32[]{:S(2)}) collective-permute-start(bf16[392,128]{1,0:T(8,128)(2,1)S(1)} %shard_map.146.aug), channel_id=1, source_target_pairs={{0,2},{2,0},{4,6},{6,4},{8,10},{10,8},{12,14},{14,12},{1,15},{3,5}... | collective-permute-start | bytes 301064 | tf_op jit(solution)/shard_map/ppermute | solution.py:327
  42.2 67.8 %collective-permute-start.5 = (bf16[7680,128]{1,0:T(8,128)(2,1)S(1)}, bf16[7680,128]{1,0:T(8,128)(2,1)S(1)}, u32[]{:S(2)}, u32[]{:S(2)}) collective-permute-start(bf16[7680,128]{1,0:T(8,128)(2,1)S(1)} %get-tuple-element.29), channel_id=1, source_target_pairs={{0,2},{2,0},{4,6},{6,4},{8,10},{10,8},{12,14},{14,12},{1,15},{3,5}... | collective-permute-start | bytes 5898248 | tf_op jit(solution)/shard_map/ppermute | solution.py:329
  79.7 27.4 %collective-permute-start.3 = (bf16[2,488,256]{2,1,0:T(8,128)(2,1)S(1)}, bf16[2,488,256]{2,1,0:T(8,128)(2,1)S(1)}, u32[]{:S(2)}, u32[]{:S(2)}) collective-permute-start(bf16[2,488,256]{2,1,0:T(8,128)(2,1)S(1)} %all_to_all.16.refs_0_), channel_id=1, source_target_pairs={{0,4},{4,8},{8,12},{12,0},{1,5},{5,9},{9,13},{13,1},{2,6},{6,10},{... | collective-permute-start | bytes 1499144 | tf_op jit(solution)/shard_map/ppermute | solution.py:265
  81.7 28.3 %collective-permute-start.4 = (bf16[2,488,256]{2,1,0:T(8,128)(2,1)S(1)}, bf16[2,488,256]{2,1,0:T(8,128)(2,1)S(1)}, u32[]{:S(2)}, u32[]{:S(2)}) collective-permute-start(bf16[2,488,256]{2,1,0:T(8,128)(2,1)S(1)} %all_to_all.16.refs_0_), channel_id=1, source_target_pairs={{4,0},{8,4},{12,8},{0,12},{5,1},{9,5},{13,9},{1,13},{6,2},{10,6},{... | collective-permute-start | bytes 1499144 | tf_op jit(solution)/shard_map/ppermute | solution.py:266
  87.1 32.6 %collective-permute-start.8 = (bf16[7680,128]{1,0:T(8,128)(2,1)S(1)}, bf16[7680,128]{1,0:T(8,128)(2,1)S(1)}, u32[]{:S(2)}, u32[]{:S(2)}) collective-permute-start(bf16[7680,128]{1,0:T(8,128)(2,1)S(1)} %get-tuple-element.32.refs_5_), channel_id=1, source_target_pairs={{0,1},{1,0},{2,3},{3,2},{4,5},{5,4},{6,7},{7,6},{8,9},{9,8},{10,11... | collective-permute-start | bytes 5898248 | tf_op jit(solution)/shard_map/ppermute | solution.py:330
  109.9 17.3 %collective-permute-start.9 = (bf16[7680,128]{1,0:T(8,128)(2,1)S(1)}, bf16[7680,128]{1,0:T(8,128)(2,1)S(1)}, u32[]{:S(2)}, u32[]{:S(2)}) collective-permute-start(bf16[7680,128]{1,0:T(8,128)(2,1)S(1)} %collective-permute-done.5.refs_6_), channel_id=1, source_target_pairs={{0,1},{1,0},{2,3},{3,2},{4,5},{5,4},{6,7},{7,6},{8,9},{9,8},{10,11... | collective-permute-start | bytes 5898248 | tf_op jit(solution)/shard_map/ppermute | solution.py:338
  112.3 11.6 %collective-permute-start.6 = (bf16[1,488,256]{2,1,0:T(8,128)(2,1)S(1)}, bf16[1,488,256]{2,1,0:T(8,128)(2,1)S(1)}, u32[]{:S(2)}, u32[]{:S(2)}) collective-permute-start(bf16[1,488,256]{2,1,0:T(8,128)(2,1)S(1)} %slice.28), channel_id=1, source_target_pairs={{0,4},{4,8},{8,12},{12,0},{1,5},{5,9},{9,13},{13,1},{2,6},{6,10},{... | collective-permute-start | bytes 749576 | tf_op jit(solution)/shard_map/ppermute | solution.py:269
  117.1 10.1 %collective-permute-start.7 = (bf16[1,488,256]{2,1,0:T(8,128)(2,1)S(1)}, bf16[1,488,256]{2,1,0:T(8,128)(2,1)S(1)}, u32[]{:S(2)}, u32[]{:S(2)}) collective-permute-start(bf16[1,488,256]{2,1,0:T(8,128)(2,1)S(1)} %slice.29), channel_id=1, source_target_pairs={{4,0},{8,4},{12,8},{0,12},{5,1},{9,5},{13,9},{1,13},{6,2},{10,6},{... | collective-permute-start | bytes 749576 | tf_op jit(solution)/shard_map/ppermute | solution.py:270
  130.8 14.2 %collective-permute-start.10 = (bf16[2,408,256]{2,1,0:T(8,128)(2,1)S(1)}, bf16[2,408,256]{2,1,0:T(8,128)(2,1)S(1)}, u32[]{:S(2)}, u32[]{:S(2)}) collective-permute-start(bf16[2,408,256]{2,1,0:T(8,128)(2,1)S(1)} %shard_map.150.refs_0_), channel_id=1, source_target_pairs={{0,4},{4,8},{8,12},{12,0},{1,5},{5,9},{9,13},{13,1},{2,6},{6,10},{... | collective-permute-start | bytes 1253384 | tf_op jit(solution)/shard_map/ppermute | solution.py:265
  134.0 13.4 %collective-permute-start.11 = (bf16[2,408,256]{2,1,0:T(8,128)(2,1)S(1)}, bf16[2,408,256]{2,1,0:T(8,128)(2,1)S(1)}, u32[]{:S(2)}, u32[]{:S(2)}) collective-permute-start(bf16[2,408,256]{2,1,0:T(8,128)(2,1)S(1)} %shard_map.150.refs_0_), channel_id=1, source_target_pairs={{4,0},{8,4},{12,8},{0,12},{5,1},{9,5},{13,9},{1,13},{6,2},{10,6},{... | collective-permute-start | bytes 1253384 | tf_op jit(solution)/shard_map/ppermute | solution.py:266
  145.1 9.3 %collective-permute-start.12 = (bf16[1,408,256]{2,1,0:T(8,128)(2,1)S(1)}, bf16[1,408,256]{2,1,0:T(8,128)(2,1)S(1)}, u32[]{:S(2)}, u32[]{:S(2)}) collective-permute-start(bf16[1,408,256]{2,1,0:T(8,128)(2,1)S(1)} %slice.32), channel_id=1, source_target_pairs={{0,4},{4,8},{8,12},{12,0},{1,5},{5,9},{9,13},{13,1},{2,6},{6,10},{... | collective-permute-start | bytes 626696 | tf_op jit(solution)/shard_map/ppermute | solution.py:269
  147.3 11.5 %collective-permute-start.13 = (bf16[1,408,256]{2,1,0:T(8,128)(2,1)S(1)}, bf16[1,408,256]{2,1,0:T(8,128)(2,1)S(1)}, u32[]{:S(2)}, u32[]{:S(2)}) collective-permute-start(bf16[1,408,256]{2,1,0:T(8,128)(2,1)S(1)} %slice.33), channel_id=1, source_target_pairs={{4,0},{8,4},{12,8},{0,12},{5,1},{9,5},{13,9},{1,13},{6,2},{10,6},{... | collective-permute-start | bytes 626696 | tf_op jit(solution)/shard_map/ppermute | solution.py:270
  160.7 6.6 %collective-permute-start.14 = (bf16[384,256]{1,0:T(8,128)(2,1)S(1)}, bf16[384,256]{1,0:T(8,128)(2,1)S(1)}, u32[]{:S(2)}, u32[]{:S(2)}) collective-permute-start(bf16[384,256]{1,0:T(8,128)(2,1)S(1)} %get-tuple-element.35), channel_id=1, source_target_pairs={{0,1},{1,0},{2,3},{3,2},{4,5},{5,4},{6,7},{7,6},{8,9},{9,8},{10,11... | collective-permute-start | bytes 589832 | tf_op jit(solution)/shard_map/ppermute | solution.py:356
  167.9 29.2 %all-to-all-start.2 = ((bf16[32,24,256]{2,1,0:T(8,128)(2,1)}), bf16[32,24,256]{2,1,0:T(8,128)(2,1)S(1)}, u32[]{:S(2)}, u32[]{:S(2)}) async-start(bf16[32,24,256]{2,1,0:T(8,128)(2,1)} %bitcast.8), calls=%async_computation.2 | async-start | bytes 786432 | tf_op jit(solution)/shard_map/all_to_all | solution.py:359
  183.2 3.5 %collective-permute-start.15 = (f32[96,256]{1,0:T(8,128)S(1)}, f32[96,256]{1,0:T(8,128)S(1)}, u32[]{:S(2)}, u32[]{:S(2)}) collective-permute-start(f32[96,256]{1,0:T(8,128)S(1)} %get-tuple-element.38), channel_id=1, source_target_pairs={{0,1},{1,0},{2,3},{3,2},{4,5},{5,4},{6,7},{7,6},{8,9},{9,8},{10,11... | collective-permute-start | bytes 294920 | tf_op jit(solution)/shard_map/ppermute | solution.py:357
  197.7 7.6 %collective-permute-start.16 = (f32[384,128]{1,0:T(8,128)S(1)}, f32[384,128]{1,0:T(8,128)S(1)}, u32[]{:S(2)}, u32[]{:S(2)}) collective-permute-start(f32[384,128]{1,0:T(8,128)S(1)} %get-tuple-element.40), channel_id=1, source_target_pairs={{0,2},{2,0},{4,6},{6,4},{8,10},{10,8},{12,14},{14,12},{1,15},{3,5}... | collective-permute-start | bytes 589832 | tf_op jit(solution)/shard_map/ppermute | solution.py:363
  (3 other events, 2.1 us)

commit v2 on v1

--- a/solution.py
+++ b/solution.py
@@ -18,6 +18,7 @@
 HALF = SP // 2 * CAP
 SHARE = TOK // 4
 GAIN = 8
+MIX = 512
 USED = HALF + SHARE
 BLOCK = USED + GAIN
 HROWS = HALF + SHARE // 4
@@ -39,12 +40,12 @@
     return lax.dot_general(a, b, (((1,), (0,)), ((), ())), preferred_element_type=f32)
 
 
-def call(body, outs, count, scratch=(), limit=8, space=VM):
+def call(body, outs, count, scratch=(), limit=8, space=VM, out_space=None):
     return pl.pallas_call(
         body,
         out_shape=outs,
         in_specs=[space] * count,
-        out_specs=jax.tree.map(lambda _: space, outs),
+        out_specs=jax.tree.map(lambda _: out_space or space, outs),
         scratch_shapes=scratch,
         compiler_params=pltpu.CompilerParams(vmem_limit_bytes=limit * MIB),
     )
@@ -83,8 +84,37 @@
         copy.wait()
 
 
-def mixer_body(outer, inner, conv, taps, before, after, out):
-    product = (inner[...].astype(f32) * conv[...].astype(f32)).astype(bf16).astype(f32)
+def first_body(*refs):
+    outer, inner, conv, weight, residual, gain, taps, routes, scores = refs[:9]
+    last, begin, product, gate, mine, taps_out, routes_out, scores_out = refs[9:17]
+    a, b, g, sem = refs[17:]
+    pairs = (
+        (inner, a),
+        (conv, b),
+        (gain, g),
+        (outer, gate),
+        (weight, mine.at[pl.ds(0, MIX)]),
+        (residual, mine.at[pl.ds(MIX, TOK)]),
+        (taps, taps_out),
+        (routes, routes_out),
+        (scores, scores_out),
+    )
+    copies = [pltpu.make_async_copy(x, y, sem.at[i]) for i, (x, y) in enumerate(pairs)]
+    for copy in copies:
+        copy.start()
+    for copy in copies[:3]:
+        copy.wait()
+    value = (a[...].astype(f32) * b[...].astype(f32)).astype(bf16)
+    last[...] = value[:, TOK - 1 : TOK]
+    begin[...] = value[:, 0:1]
+    product[...] = value
+    mine[MIX + TOK :, :] = jnp.broadcast_to(g[...], (GAIN, 128))
+    for copy in copies[3:]:
+        copy.wait()
+
+
+def mixer_body(gate, value, taps, before, after, out):
+    product = value[...].astype(f32)
     lane = lax.broadcasted_iota(i32, product.shape, 1)
     left = jnp.where(lane == 0, before[...].astype(f32), pltpu.roll(product, 1, 1))
     right = jnp.where(lane == TOK - 1, after[...].astype(f32), pltpu.roll(product, TOK - 1, 1))
@@ -93,15 +123,7 @@
     k = taps[...].astype(f32)
     k = [jnp.sum(jnp.where(i == j, k[n : n + 1, :], 0.0), axis=1, keepdims=True) for n in range(3)]
     filtered = k[0] * left + k[1] * product + k[2] * right
-    out[...] = (outer[...].astype(f32) * filtered).astype(bf16)
-
-
-def stream_body(mixed, weight, residual, gain, out):
-    projected = lax.dot_general(
-        mixed[...], weight[...], (((0,), (0,)), ((), ())), preferred_element_type=f32
-    )
-    out[0:TOK, :] = (residual[...].astype(f32) + projected).astype(bf16)
-    out[TOK : TOK + GAIN, :] = jnp.broadcast_to(gain[...], (GAIN, 128))
+    out[...] = (gate[...].astype(f32) * filtered).astype(bf16)
 
 
 def meta_body(routes, scores, rows_out, cols_out):
@@ -127,18 +149,23 @@
     cols_out[...] = table.T
 
 
-def dispatch_body(aug, near, slots, send, shared):
+def dispatch_body(mixed, mine, near, slots, stream, send, shared, tokens):
     yl = index("yl")
-    tokens = jnp.concatenate([aug[0:TOK, :], near[0:TOK, :]], axis=1)
+    weight = jnp.concatenate([mine[0:MIX, :], near[0:MIX, :]], axis=1)
+    residual = jnp.concatenate([mine[MIX : MIX + TOK, :], near[MIX : MIX + TOK, :]], axis=1)
+    projected = lax.dot_general(
+        mixed[...], weight, (((0,), (0,)), ((), ())), preferred_element_type=f32
+    )
+    tokens[...] = (residual.astype(f32) + projected).astype(bf16)
+    stream[...] = tokens[:, 0:128]
     row = lax.broadcasted_iota(i32, (SP * CAP, TOK), 0).astype(f32)
     pick = (row == slots[0:1, :]) | (row == slots[1:2, :])
-    send[...] = dot(jnp.where(pick, 1.0, 0.0).astype(bf16), tokens).astype(bf16)
+    send[...] = dot(jnp.where(pick, 1.0, 0.0).astype(bf16), tokens[...]).astype(bf16)
     for core in range(2):
         start = pl.multiple_of((yl * 2 + core) * SHARE, SHARE)
-        for h, x in enumerate((aug, near)):
-            lanes = slice(128 * h, 128 * h + 128)
-            shared[core, 0:SHARE, lanes] = x[pl.ds(start, SHARE), :]
-            shared[core, SHARE : SHARE + GAIN, lanes] = x[TOK : TOK + GAIN, :]
+        shared[core, 0:SHARE, :] = tokens[pl.ds(start, SHARE), :]
+        for h, x in enumerate((mine, near)):
+            shared[core, SHARE : SHARE + GAIN, 128 * h : 128 * h + 128] = x[MIX + TOK :, :]
 
 
 def silu(v):
@@ -251,8 +278,8 @@
     give[...] = acc[:, 128:256]
 
 
-def final_body(aug, keep, other, out):
-    out[...] = (aug[0:TOK, :].astype(f32) + keep[...] + other[...]).astype(bf16)
+def final_body(stream, keep, other, out):
+    out[...] = (stream[...].astype(f32) + keep[...] + other[...]).astype(bf16)
 
 
 def sds(shape, dtype=bf16):
@@ -292,18 +319,50 @@
     swap = [(0, 1), (1, 0)]
     tp = ("yh", "yl", "c")
 
-    def edge(i):
-        a = lax.slice_in_dim(inner_gate, i, i + 1, axis=1).astype(f32)
-        b = lax.slice_in_dim(conv_input, i, i + 1, axis=1).astype(f32)
-        return (a * b).astype(bf16)
-
+    column = sds((32, 1))
+    last, begin, product, gate, mine, taps, chosen, scores = call(
+        first_body,
+        (
+            column,
+            column,
+            sds((32, TOK)),
+            sds((32, TOK)),
+            sds((MIX + TOK + GAIN, 128)),
+            sds((3, 32)),
+            sds((2, TOK), i32),
+            sds((2, TOK), f32),
+        ),
+        9,
+        [
+            pltpu.VMEM((32, TOK), bf16),
+            pltpu.VMEM((32, TOK), bf16),
+            pltpu.VMEM((1, 128), bf16),
+            pltpu.SemaphoreType.DMA((9,)),
+        ],
+        space=ANY,
+        out_space=VM,
+    )(
+        *(
+            pltpu.with_memory_space_constraint(w, pltpu.HBM)
+            for w in (
+                outer_gate,
+                inner_gate,
+                conv_input,
+                mix_weight,
+                residual,
+                norm_gain.reshape(1, 128),
+                conv_taps,
+                routes.T,
+                route_scores.T,
+            )
+        )
+    )
     up = [(i, i + 1) for i in range(SP - 1)]
-    before = lax.ppermute(edge(TOK - 1), "sp", up)
-    after = lax.ppermute(edge(0), "sp", [(j, i) for i, j in up])
-
-    slots, cols = call(meta_body, (sds((8, TOK), f32), sds((TOK, 128), f32)), 2)(
-        routes.T, route_scores.T
-    )
+    before = lax.ppermute(last, "sp", up)
+    after = lax.ppermute(begin, "sp", [(j, i) for i, j in up])
+    near = lax.ppermute(mine, tp, NEAR)
+
+    slots, cols = call(meta_body, (sds((8, TOK), f32), sds((TOK, 128), f32)), 2)(chosen, scores)
     w_own, w_other = call(
         pick_body,
         (sds((WROWS, 128)), sds((WROWS, 128))),
@@ -317,20 +376,20 @@
         )
     )
 
-    mixed = call(mixer_body, sds((32, TOK)), 6)(
-        outer_gate, inner_gate, conv_input, conv_taps, before, after
-    )
-    mixed = lax.all_gather(mixed, ("yh", "yl", "c"), axis=0, tiled=True)
-    aug = call(stream_body, sds((TOK + GAIN, 128)), 4)(
-        mixed, mix_weight, residual, norm_gain.reshape(1, 128)
-    )
-    near = lax.ppermute(aug, tp, NEAR)
-    near, w_other, w_own = lax.optimization_barrier((near, w_other, w_own))
+    mixed = call(mixer_body, sds((32, TOK)), 5)(
+        gate, product, taps, before, after
+    )
+    mixed, near, w_other, w_own = lax.optimization_barrier((mixed, near, w_other, w_own))
+    mixed = lax.all_gather(mixed, tp, axis=0, tiled=True)
+    mixed, w_other, w_own = lax.optimization_barrier((mixed, w_other, w_own))
     w_got = lax.ppermute(w_other, tp, NEAR)
     w_own_c = lax.ppermute(w_own, "c", swap)
-    send, shared = call(
-        dispatch_body, (sds((SP * CAP, 256)), sds((2, SHARE + GAIN, 256))), 3
-    )(aug, near, slots)
+    stream, send, shared = call(
+        dispatch_body,
+        (sds((TOK, 128)), sds((SP * CAP, 256)), sds((2, SHARE + GAIN, 256))),
+        4,
+        [pltpu.VMEM((TOK, 256), bf16)],
+    )(mixed, mine, near, slots)
     arrived = lax.all_to_all(send.reshape(SP, CAP, 256), "sp", 0, 0, tiled=True)
     block = jnp.concatenate([arrived.reshape(2, HALF, 256), shared], axis=1)
     block = lax.all_to_all(block, "c", 0, 0, tiled=True)
@@ -357,11 +416,11 @@
     sgot = lax.ppermute(sgive, "c", swap)
     back = lax.dynamic_update_index_in_dim(back, got, 1 - c, 0)
     back = lax.all_to_all(back.reshape(SP, CAP, 256), "sp", 0, 0, tiled=True)
-    mine, other = call(
+    keep, other = call(
         combine_body, (sds((TOK, 128), f32), sds((TOK, 128), f32)), 4, [pltpu.VMEM((TOK, 256), f32)]
     )(back.reshape(SP * CAP, 256), cols, skeep, sgot)
     other = lax.ppermute(other, tp, NEAR)
-    return call(final_body, sds((TOK, 128)), 3)(aug, mine, other)
+    return call(final_body, sds((TOK, 128)), 3)(stream, keep, other)
 
 
 def solution(mesh):

time: 209 us -> 201 us (0.962)
  local copies, waits for them, and re-layouts: 6.1 us -> 0.76 us
  starting transfers between devices: 74.8 us -> 71 us
  waiting for transfers between devices: 59.6 us -> 62.6 us
    unnamed x18 -> x0, local copies, waits for them, and re-layouts: 5.35 us -> none
    ppermute x2, waiting for transfers between devices: 24 us -> 28.5 us  [ring(): u = lax.ppermute(block, 'yh', up)]
    ppermute x2, waiting for transfers between devices: 5.99 us -> 9.84 us  [ring(): u2 = lax.ppermute(u[:1], 'yh', up)]
    ppermute x2, waiting for transfers between devices: 7.71 us -> 4.08 us  [ring(): d2 = lax.ppermute(d[1:], 'yh', down)]
    ppermute x3, waiting for transfers between devices: 3.73 us -> 0.87 us  [the longest x1 0.86 us: layer(): after = lax.ppermute(begin, 'sp', [(j, i) for i, j in up])]
    ppermute x1, starting transfers between devices: 5.52 us -> 2.9 us  [layer(): got = lax.ppermute(give, 'c', swap)]
  transfers between devices with their start and end apart: 18 -> 18, of which waited for: 13 -> 12; matrix products, arithmetic and copies ran while one was open for 0% -> 0% of each run, Pallas kernels for 2% -> 2%
where the time goes in v2:
time: 201 us; the launch traced here: 200 us
  starting transfers between devices  71 us (35%)
  waiting for transfers between devices  62.6 us (31%)
  blocking collectives  53.2 us (26%)
  Pallas kernels  11.8 us (6%)
    all_to_all x1, blocking collectives, layer(): arrived = lax.all_to_all(send.reshape(SP, CAP, 256), 'sp', 0, 0, tiled=True)  28.6 us
    ppermute x2, waiting for transfers between devices, ring(): u = lax.ppermute(block, 'yh', up)  28.5 us
    all_gather x1, blocking collectives, layer(): mixed = lax.all_gather(mixed, tp, axis=0, tiled=True)  18.9 us
    all_to_all x1, starting transfers between devices, layer(): back = lax.all_to_all(back.reshape(SP, CAP, 256), 'sp', 0, 0, tiled=True)  14.4 us
    all_to_all x1, waiting for transfers between devices, layer(): back = lax.all_to_all(back.reshape(SP, CAP, 256), 'sp', 0, 0, tiled=True)  10.4 us
    ppermute x2, waiting for transfers between devices, ring(): u2 = lax.ppermute(u[:1], 'yh', up)  9.84 us
    ppermute x2, starting transfers between devices, ring(): d = lax.ppermute(block, 'yh', down)  8.09 us
    ppermute x2, starting transfers between devices, ring(): u2 = lax.ppermute(u[:1], 'yh', up)  7.52 us
  transfers between devices with their start and end apart: 18, of which 12 were waited for; matrix products, arithmetic and copies ran while one was open for 0% of the time, Pallas kernels for 2%

profile of v2, /device:TPU:1, one launch (start us, length us, event | category | flops | bytes accessed | tf_op | source)
XLA Modules:
  0.0 199.6 jit_solution(309779972145856423)
XLA Ops:
  1.1 5.9 %collective-permute-start.2 = (bf16[904,128]{1,0:T(8,128)(2,1)S(1)}, bf16[904,128]{1,0:T(8,128)(2,1)S(1)}, u32[]{:S(2)}, u32[]{:S(2)}) collective-permute-start(bf16[904,128]{1,0:T(8,128)(2,1)S(1)} %get-tuple-element.41.mine), channel_id=1, source_target_pairs={{0,2},{2,0},{4,6},{6,4},{8,10},{10,8},{12,14},{14,12},{1,15},{3,5}... | collective-permute-start | bytes 694280 | tf_op jit(solution)/shard_map/ppermute | solution.py:363
  7.0 3.1 %collective-permute-start = (bf16[32,1]{1,0:T(8,128)(2,1)S(1)}, bf16[32,1]{1,0:T(8,128)(2,1)S(1)}, u32[]{:S(2)}, u32[]{:S(2)}) collective-permute-start(bf16[32,1]{1,0:T(8,128)(2,1)S(1)} %get-tuple-element.39), channel_id=1, source_target_pairs={{0,16},{16,32},{32,48},{48,64},{64,80},{80,96},{96,112},{112,128},... | collective-permute-start | bytes 200 | tf_op jit(solution)/shard_map/ppermute | solution.py:361
  15.0 18.9 %all_gather.3.mixed = bf16[512,384]{1,0:T(8,128)(2,1)S(1)} all-gather(bf16[32,384]{1,0:T(8,128)(2,1)S(1)} %shard_map.146), channel_id=1, replica_groups=mesh['sp'=32,'yh'=4,'yl'=2,'c'=2] {'yh','yl','c'}, dimensions={0}, use_global_device_ids=true | all-gather | bytes 417792 | tf_op jit(solution)/shard_map/all_gather | solution.py:383
  37.1 28.6 %all_to_all.15 = bf16[32,24,256]{2,1,0:T(8,128)(2,1)S(1)} all-to-all(bf16[32,24,256]{2,1,0:T(8,128)(2,1)S(1)} %bitcast.12), channel_id=1, replica_groups=mesh['sp'=32,'yh'=4,'yl'=2,'c'=2] {'sp'}, dimensions={0} | all-to-all | bytes 786432 | tf_op jit(solution)/shard_map/all_to_all | solution.py:393
  65.7 5.7 %all_to_all.16.refs_0_ = bf16[2,488,256]{2,1,0:T(8,128)(2,1)S(1)} all-to-all(bf16[2,488,256]{2,1,0:T(8,128)(2,1)S(1)} %pad_maximum_fusion), channel_id=1, replica_groups=mesh['sp'=32,'yh'=4,'yl'=2,'c'=2] {'c'}, dimensions={0} | all-to-all | bytes 999424 | tf_op jit(solution)/shard_map/all_to_all | solution.py:395
  73.7 5.1 %collective-permute-start.4 = (bf16[2,488,256]{2,1,0:T(8,128)(2,1)S(1)}, bf16[2,488,256]{2,1,0:T(8,128)(2,1)S(1)}, u32[]{:S(2)}, u32[]{:S(2)}) collective-permute-start(bf16[2,488,256]{2,1,0:T(8,128)(2,1)S(1)} %all_to_all.16.refs_0_), channel_id=1, source_target_pairs={{4,0},{8,4},{12,8},{0,12},{5,1},{9,5},{13,9},{1,13},{6,2},{10,6},{... | collective-permute-start | bytes 1499144 | tf_op jit(solution)/shard_map/ppermute | solution.py:293
  78.8 2.8 %collective-permute-start.8 = (bf16[7680,128]{1,0:T(8,128)(2,1)S(1)}, bf16[7680,128]{1,0:T(8,128)(2,1)S(1)}, u32[]{:S(2)}, u32[]{:S(2)}) collective-permute-start(bf16[7680,128]{1,0:T(8,128)(2,1)S(1)} %get-tuple-element.58.refs_5_), channel_id=1, source_target_pairs={{0,1},{1,0},{2,3},{3,2},{4,5},{5,4},{6,7},{7,6},{8,9},{9,8},{10,11... | collective-permute-start | bytes 5898248 | tf_op jit(solution)/shard_map/ppermute | solution.py:386
  81.7 16.3 %collective-permute-done.3.refs_1_ = bf16[2,488,256]{2,1,0:T(8,128)(2,1)S(1)} collective-permute-done((bf16[2,488,256]{2,1,0:T(8,128)(2,1)S(1)}, bf16[2,488,256]{2,1,0:T(8,128)(2,1)S(1)}, u32[]{:S(2)}, u32[]{:S(2)}) %collective-permute-start.3) | collective-permute-done | bytes 499744 | tf_op jit(solution)/shard_map/ppermute | solution.py:292
  97.9 2.6 %collective-permute-done.4.refs_2_ = bf16[2,488,256]{2,1,0:T(8,128)(2,1)S(1)} collective-permute-done((bf16[2,488,256]{2,1,0:T(8,128)(2,1)S(1)}, bf16[2,488,256]{2,1,0:T(8,128)(2,1)S(1)}, u32[]{:S(2)}, u32[]{:S(2)}) %collective-permute-start.4) | collective-permute-done | bytes 499744 | tf_op jit(solution)/shard_map/ppermute | solution.py:293
  100.5 3.0 %collective-permute-start.9 = (bf16[7680,128]{1,0:T(8,128)(2,1)S(1)}, bf16[7680,128]{1,0:T(8,128)(2,1)S(1)}, u32[]{:S(2)}, u32[]{:S(2)}) collective-permute-start(bf16[7680,128]{1,0:T(8,128)(2,1)S(1)} %collective-permute-done.5.refs_6_), channel_id=1, source_target_pairs={{0,1},{1,0},{2,3},{3,2},{4,5},{5,4},{6,7},{7,6},{8,9},{9,8},{10,11... | collective-permute-start | bytes 5898248 | tf_op jit(solution)/shard_map/ppermute | solution.py:397
  103.6 5.4 %collective-permute-start.6 = (bf16[1,488,256]{2,1,0:T(8,128)(2,1)S(1)}, bf16[1,488,256]{2,1,0:T(8,128)(2,1)S(1)}, u32[]{:S(2)}, u32[]{:S(2)}) collective-permute-start(bf16[1,488,256]{2,1,0:T(8,128)(2,1)S(1)} %slice.12), channel_id=1, source_target_pairs={{0,4},{4,8},{8,12},{12,0},{1,5},{5,9},{9,13},{13,1},{2,6},{6,10},{... | collective-permute-start | bytes 749576 | tf_op jit(solution)/shard_map/ppermute | solution.py:296
  111.2 7.1 %collective-permute-done.6.refs_3_ = bf16[1,488,256]{2,1,0:T(8,128)(2,1)S(1)} collective-permute-done((bf16[1,488,256]{2,1,0:T(8,128)(2,1)S(1)}, bf16[1,488,256]{2,1,0:T(8,128)(2,1)S(1)}, u32[]{:S(2)}, u32[]{:S(2)}) %collective-permute-start.6) | collective-permute-done | bytes 249888 | tf_op jit(solution)/shard_map/ppermute | solution.py:296
  120.4 3.6 %shard_map.150.refs_0_ = bf16[2,408,256]{2,1,0:T(8,128)(2,1)S(1)} custom-call(bf16[2,488,256]{2,1,0:T(8,128)(2,1)S(1)} %all_to_all.16.refs_0_, bf16[2,488,256]{2,1,0:T(8,128)(2,1)S(1)} %collective-permute-done.3.refs_1_, bf16[2,488,256]{2,1,0:T(8,128)(2,1)S(1)} %collective-permute-done.4.refs_2_, bf16[1,488,256]{2,1,0:T(8,128)(2,1)S(1)} %collective-permute-done.6.refs_3_, ...), custom_call_target="tpu_custom_call" | custom-call | tf_op jit(solution)/shard_map/pallas_call | solution.py:400
  124.1 4.4 %collective-permute-start.10 = (bf16[2,408,256]{2,1,0:T(8,128)(2,1)S(1)}, bf16[2,408,256]{2,1,0:T(8,128)(2,1)S(1)}, u32[]{:S(2)}, u32[]{:S(2)}) collective-permute-start(bf16[2,408,256]{2,1,0:T(8,128)(2,1)S(1)} %shard_map.150.refs_0_), channel_id=1, source_target_pairs={{0,4},{4,8},{8,12},{12,0},{1,5},{5,9},{9,13},{13,1},{2,6},{6,10},{... | collective-permute-start | bytes 1253384 | tf_op jit(solution)/shard_map/ppermute | solution.py:292
  128.5 3.0 %collective-permute-start.11 = (bf16[2,408,256]{2,1,0:T(8,128)(2,1)S(1)}, bf16[2,408,256]{2,1,0:T(8,128)(2,1)S(1)}, u32[]{:S(2)}, u32[]{:S(2)}) collective-permute-start(bf16[2,408,256]{2,1,0:T(8,128)(2,1)S(1)} %shard_map.150.refs_0_), channel_id=1, source_target_pairs={{4,0},{8,4},{12,8},{0,12},{5,1},{9,5},{13,9},{1,13},{6,2},{10,6},{... | collective-permute-start | bytes 1253384 | tf_op jit(solution)/shard_map/ppermute | solution.py:293
  131.5 12.2 %collective-permute-done.10.refs_1_ = bf16[2,408,256]{2,1,0:T(8,128)(2,1)S(1)} collective-permute-done((bf16[2,408,256]{2,1,0:T(8,128)(2,1)S(1)}, bf16[2,408,256]{2,1,0:T(8,128)(2,1)S(1)}, u32[]{:S(2)}, u32[]{:S(2)}) %collective-permute-start.10) | collective-permute-done | bytes 417824 | tf_op jit(solution)/shard_map/ppermute | solution.py:292
  145.9 5.2 %collective-permute-start.13 = (bf16[1,408,256]{2,1,0:T(8,128)(2,1)S(1)}, bf16[1,408,256]{2,1,0:T(8,128)(2,1)S(1)}, u32[]{:S(2)}, u32[]{:S(2)}) collective-permute-start(bf16[1,408,256]{2,1,0:T(8,128)(2,1)S(1)} %slice.17), channel_id=1, source_target_pairs={{4,0},{8,4},{12,8},{0,12},{5,1},{9,5},{13,9},{1,13},{6,2},{10,6},{... | collective-permute-start | bytes 626696 | tf_op jit(solution)/shard_map/ppermute | solution.py:297
  151.2 2.8 %collective-permute-done.12.refs_3_ = bf16[1,408,256]{2,1,0:T(8,128)(2,1)S(1)} collective-permute-done((bf16[1,408,256]{2,1,0:T(8,128)(2,1)S(1)}, bf16[1,408,256]{2,1,0:T(8,128)(2,1)S(1)}, u32[]{:S(2)}, u32[]{:S(2)}) %collective-permute-start.12) | collective-permute-done | bytes 208928 | tf_op jit(solution)/shard_map/ppermute | solution.py:296
  157.8 2.9 %collective-permute-start.14 = (bf16[384,256]{1,0:T(8,128)(2,1)S(1)}, bf16[384,256]{1,0:T(8,128)(2,1)S(1)}, u32[]{:S(2)}, u32[]{:S(2)}) collective-permute-start(bf16[384,256]{1,0:T(8,128)(2,1)S(1)} %get-tuple-element.61), channel_id=1, source_target_pairs={{0,1},{1,0},{2,3},{3,2},{4,5},{5,4},{6,7},{7,6},{8,9},{9,8},{10,11... | collective-permute-start | bytes 589832 | tf_op jit(solution)/shard_map/ppermute | solution.py:415
  162.4 14.4 %all-to-all-start.2 = ((bf16[32,24,256]{2,1,0:T(8,128)(2,1)}), bf16[32,24,256]{2,1,0:T(8,128)(2,1)S(1)}, u32[]{:S(2)}, u32[]{:S(2)}) async-start(bf16[32,24,256]{2,1,0:T(8,128)(2,1)} %bitcast.8), calls=%async_computation.2 | async-start | bytes 786432 | tf_op jit(solution)/shard_map/all_to_all | solution.py:418
  176.8 2.6 %collective-permute-start.15 = (f32[96,256]{1,0:T(8,128)S(1)}, f32[96,256]{1,0:T(8,128)S(1)}, u32[]{:S(2)}, u32[]{:S(2)}) collective-permute-start(f32[96,256]{1,0:T(8,128)S(1)} %get-tuple-element.64), channel_id=1, source_target_pairs={{0,1},{1,0},{2,3},{3,2},{4,5},{5,4},{6,7},{7,6},{8,9},{9,8},{10,11... | collective-permute-start | bytes 294920 | tf_op jit(solution)/shard_map/ppermute | solution.py:416
  180.3 10.4 %all-to-all-done.2 = bf16[32,24,256]{2,1,0:T(8,128)(2,1)S(1)} async-done(((bf16[32,24,256]{2,1,0:T(8,128)(2,1)}), bf16[32,24,256]{2,1,0:T(8,128)(2,1)S(1)}, u32[]{:S(2)}, u32[]{:S(2)}) %all-to-all-start.2) | async-done | bytes 393248 | tf_op jit(solution)/shard_map/all_to_all | solution.py:418
  191.3 3.3 %collective-permute-start.16 = (f32[384,128]{1,0:T(8,128)S(1)}, f32[384,128]{1,0:T(8,128)S(1)}, u32[]{:S(2)}, u32[]{:S(2)}) collective-permute-start(f32[384,128]{1,0:T(8,128)S(1)} %get-tuple-element.66), channel_id=1, source_target_pairs={{0,2},{2,0},{4,6},{6,4},{8,10},{10,8},{12,14},{14,12},{1,15},{3,5}... | collective-permute-start | bytes 589832 | tf_op jit(solution)/shard_map/ppermute | solution.py:422
  194.6 4.3 %collective-permute-done.16.other = f32[384,128]{1,0:T(8,128)S(1)} collective-permute-done((f32[384,128]{1,0:T(8,128)S(1)}, f32[384,128]{1,0:T(8,128)S(1)}, u32[]{:S(2)}, u32[]{:S(2)}) %collective-permute-start.16) | collective-permute-done | bytes 196640 | tf_op jit(solution)/shard_map/ppermute | solution.py:422
  (30 shorter events, 25.7 us)
Async XLA Ops:
  1.1 13.9 %collective-permute-start.2 = (bf16[904,128]{1,0:T(8,128)(2,1)S(1)}, bf16[904,128]{1,0:T(8,128)(2,1)S(1)}, u32[]{:S(2)}, u32[]{:S(2)}) collective-permute-start(bf16[904,128]{1,0:T(8,128)(2,1)S(1)} %get-tuple-element.41.mine), channel_id=1, source_target_pairs={{0,2},{2,0},{4,6},{6,4},{8,10},{10,8},{12,14},{14,12},{1,15},{3,5}... | collective-permute-start | bytes 694280 | tf_op jit(solution)/shard_map/ppermute | solution.py:363
  7.0 6.9 %collective-permute-start = (bf16[32,1]{1,0:T(8,128)(2,1)S(1)}, bf16[32,1]{1,0:T(8,128)(2,1)S(1)}, u32[]{:S(2)}, u32[]{:S(2)}) collective-permute-start(bf16[32,1]{1,0:T(8,128)(2,1)S(1)} %get-tuple-element.39), channel_id=1, source_target_pairs={{0,16},{16,32},{32,48},{48,64},{64,80},{80,96},{96,112},{112,128},... | collective-permute-start | bytes 200 | tf_op jit(solution)/shard_map/ppermute | solution.py:361
  10.2 4.7 %collective-permute-start.1 = (bf16[32,1]{1,0:T(8,128)(2,1)S(1)}, bf16[32,1]{1,0:T(8,128)(2,1)S(1)}, u32[]{:S(2)}, u32[]{:S(2)}) collective-permute-start(bf16[32,1]{1,0:T(8,128)(2,1)S(1)} %get-tuple-element.40), channel_id=1, source_target_pairs={{16,0},{32,16},{48,32},{64,48},{80,64},{96,80},{112,96},{128,112},... | collective-permute-start | bytes 200 | tf_op jit(solution)/shard_map/ppermute | solution.py:362
  33.9 66.6 %collective-permute-start.5 = (bf16[7680,128]{1,0:T(8,128)(2,1)S(1)}, bf16[7680,128]{1,0:T(8,128)(2,1)S(1)}, u32[]{:S(2)}, u32[]{:S(2)}) collective-permute-start(bf16[7680,128]{1,0:T(8,128)(2,1)S(1)} %get-tuple-element.55), channel_id=1, source_target_pairs={{0,2},{2,0},{4,6},{6,4},{8,10},{10,8},{12,14},{14,12},{1,15},{3,5}... | collective-permute-start | bytes 5898248 | tf_op jit(solution)/shard_map/ppermute | solution.py:385
  71.4 26.5 %collective-permute-start.3 = (bf16[2,488,256]{2,1,0:T(8,128)(2,1)S(1)}, bf16[2,488,256]{2,1,0:T(8,128)(2,1)S(1)}, u32[]{:S(2)}, u32[]{:S(2)}) collective-permute-start(bf16[2,488,256]{2,1,0:T(8,128)(2,1)S(1)} %all_to_all.16.refs_0_), channel_id=1, source_target_pairs={{0,4},{4,8},{8,12},{12,0},{1,5},{5,9},{9,13},{13,1},{2,6},{6,10},{... | collective-permute-start | bytes 1499144 | tf_op jit(solution)/shard_map/ppermute | solution.py:292
  73.7 26.8 %collective-permute-start.4 = (bf16[2,488,256]{2,1,0:T(8,128)(2,1)S(1)}, bf16[2,488,256]{2,1,0:T(8,128)(2,1)S(1)}, u32[]{:S(2)}, u32[]{:S(2)}) collective-permute-start(bf16[2,488,256]{2,1,0:T(8,128)(2,1)S(1)} %all_to_all.16.refs_0_), channel_id=1, source_target_pairs={{4,0},{8,4},{12,8},{0,12},{5,1},{9,5},{13,9},{1,13},{6,2},{10,6},{... | collective-permute-start | bytes 1499144 | tf_op jit(solution)/shard_map/ppermute | solution.py:293
  78.8 32.4 %collective-permute-start.8 = (bf16[7680,128]{1,0:T(8,128)(2,1)S(1)}, bf16[7680,128]{1,0:T(8,128)(2,1)S(1)}, u32[]{:S(2)}, u32[]{:S(2)}) collective-permute-start(bf16[7680,128]{1,0:T(8,128)(2,1)S(1)} %get-tuple-element.58.refs_5_), channel_id=1, source_target_pairs={{0,1},{1,0},{2,3},{3,2},{4,5},{5,4},{6,7},{7,6},{8,9},{9,8},{10,11... | collective-permute-start | bytes 5898248 | tf_op jit(solution)/shard_map/ppermute | solution.py:386
  100.5 19.9 %collective-permute-start.9 = (bf16[7680,128]{1,0:T(8,128)(2,1)S(1)}, bf16[7680,128]{1,0:T(8,128)(2,1)S(1)}, u32[]{:S(2)}, u32[]{:S(2)}) collective-permute-start(bf16[7680,128]{1,0:T(8,128)(2,1)S(1)} %collective-permute-done.5.refs_6_), channel_id=1, source_target_pairs={{0,1},{1,0},{2,3},{3,2},{4,5},{5,4},{6,7},{7,6},{8,9},{9,8},{10,11... | collective-permute-start | bytes 5898248 | tf_op jit(solution)/shard_map/ppermute | solution.py:397
  103.6 14.7 %collective-permute-start.6 = (bf16[1,488,256]{2,1,0:T(8,128)(2,1)S(1)}, bf16[1,488,256]{2,1,0:T(8,128)(2,1)S(1)}, u32[]{:S(2)}, u32[]{:S(2)}) collective-permute-start(bf16[1,488,256]{2,1,0:T(8,128)(2,1)S(1)} %slice.12), channel_id=1, source_target_pairs={{0,4},{4,8},{8,12},{12,0},{1,5},{5,9},{9,13},{13,1},{2,6},{6,10},{... | collective-permute-start | bytes 749576 | tf_op jit(solution)/shard_map/ppermute | solution.py:296
  109.0 11.4 %collective-permute-start.7 = (bf16[1,488,256]{2,1,0:T(8,128)(2,1)S(1)}, bf16[1,488,256]{2,1,0:T(8,128)(2,1)S(1)}, u32[]{:S(2)}, u32[]{:S(2)}) collective-permute-start(bf16[1,488,256]{2,1,0:T(8,128)(2,1)S(1)} %slice.13), channel_id=1, source_target_pairs={{4,0},{8,4},{12,8},{0,12},{5,1},{9,5},{13,9},{1,13},{6,2},{10,6},{... | collective-permute-start | bytes 749576 | tf_op jit(solution)/shard_map/ppermute | solution.py:297
  124.1 19.6 %collective-permute-start.10 = (bf16[2,408,256]{2,1,0:T(8,128)(2,1)S(1)}, bf16[2,408,256]{2,1,0:T(8,128)(2,1)S(1)}, u32[]{:S(2)}, u32[]{:S(2)}) collective-permute-start(bf16[2,408,256]{2,1,0:T(8,128)(2,1)S(1)} %shard_map.150.refs_0_), channel_id=1, source_target_pairs={{0,4},{4,8},{8,12},{12,0},{1,5},{5,9},{9,13},{13,1},{2,6},{6,10},{... | collective-permute-start | bytes 1253384 | tf_op jit(solution)/shard_map/ppermute | solution.py:292
  128.5 17.4 %collective-permute-start.11 = (bf16[2,408,256]{2,1,0:T(8,128)(2,1)S(1)}, bf16[2,408,256]{2,1,0:T(8,128)(2,1)S(1)}, u32[]{:S(2)}, u32[]{:S(2)}) collective-permute-start(bf16[2,408,256]{2,1,0:T(8,128)(2,1)S(1)} %shard_map.150.refs_0_), channel_id=1, source_target_pairs={{4,0},{8,4},{12,8},{0,12},{5,1},{9,5},{13,9},{1,13},{6,2},{10,6},{... | collective-permute-start | bytes 1253384 | tf_op jit(solution)/shard_map/ppermute | solution.py:293
  143.7 10.2 %collective-permute-start.12 = (bf16[1,408,256]{2,1,0:T(8,128)(2,1)S(1)}, bf16[1,408,256]{2,1,0:T(8,128)(2,1)S(1)}, u32[]{:S(2)}, u32[]{:S(2)}) collective-permute-start(bf16[1,408,256]{2,1,0:T(8,128)(2,1)S(1)} %slice.16), channel_id=1, source_target_pairs={{0,4},{4,8},{8,12},{12,0},{1,5},{5,9},{9,13},{13,1},{2,6},{6,10},{... | collective-permute-start | bytes 626696 | tf_op jit(solution)/shard_map/ppermute | solution.py:296
  145.9 10.0 %collective-permute-start.13 = (bf16[1,408,256]{2,1,0:T(8,128)(2,1)S(1)}, bf16[1,408,256]{2,1,0:T(8,128)(2,1)S(1)}, u32[]{:S(2)}, u32[]{:S(2)}) collective-permute-start(bf16[1,408,256]{2,1,0:T(8,128)(2,1)S(1)} %slice.17), channel_id=1, source_target_pairs={{4,0},{8,4},{12,8},{0,12},{5,1},{9,5},{13,9},{1,13},{6,2},{10,6},{... | collective-permute-start | bytes 626696 | tf_op jit(solution)/shard_map/ppermute | solution.py:297
  157.8 4.0 %collective-permute-start.14 = (bf16[384,256]{1,0:T(8,128)(2,1)S(1)}, bf16[384,256]{1,0:T(8,128)(2,1)S(1)}, u32[]{:S(2)}, u32[]{:S(2)}) collective-permute-start(bf16[384,256]{1,0:T(8,128)(2,1)S(1)} %get-tuple-element.61), channel_id=1, source_target_pairs={{0,1},{1,0},{2,3},{3,2},{4,5},{5,4},{6,7},{7,6},{8,9},{9,8},{10,11... | collective-permute-start | bytes 589832 | tf_op jit(solution)/shard_map/ppermute | solution.py:415
  162.4 28.3 %all-to-all-start.2 = ((bf16[32,24,256]{2,1,0:T(8,128)(2,1)}), bf16[32,24,256]{2,1,0:T(8,128)(2,1)S(1)}, u32[]{:S(2)}, u32[]{:S(2)}) async-start(bf16[32,24,256]{2,1,0:T(8,128)(2,1)} %bitcast.8), calls=%async_computation.2 | async-start | bytes 786432 | tf_op jit(solution)/shard_map/all_to_all | solution.py:418
  176.8 3.5 %collective-permute-start.15 = (f32[96,256]{1,0:T(8,128)S(1)}, f32[96,256]{1,0:T(8,128)S(1)}, u32[]{:S(2)}, u32[]{:S(2)}) collective-permute-start(f32[96,256]{1,0:T(8,128)S(1)} %get-tuple-element.64), channel_id=1, source_target_pairs={{0,1},{1,0},{2,3},{3,2},{4,5},{5,4},{6,7},{7,6},{8,9},{9,8},{10,11... | collective-permute-start | bytes 294920 | tf_op jit(solution)/shard_map/ppermute | solution.py:416
  191.3 7.6 %collective-permute-start.16 = (f32[384,128]{1,0:T(8,128)S(1)}, f32[384,128]{1,0:T(8,128)S(1)}, u32[]{:S(2)}, u32[]{:S(2)}) collective-permute-start(f32[384,128]{1,0:T(8,128)S(1)} %get-tuple-element.66), channel_id=1, source_target_pairs={{0,2},{2,0},{4,6},{6,4},{8,10},{10,8},{12,14},{14,12},{1,15},{3,5}... | collective-permute-start | bytes 589832 | tf_op jit(solution)/shard_map/ppermute | solution.py:422

commit v3 on v2

--- a/solution.py
+++ b/solution.py
@@ -1,3 +1,5 @@
+import functools
+
 import jax
 import jax.numpy as jnp
 from jax import lax
@@ -55,17 +57,14 @@
     return lax.axis_index(axis)
 
 
-def pick_body(gate, up, down, sg, su, sd, own, other, pack, sem):
-    yl = index("yl")
-    copies = [
-        (w.at[which], out.at[pl.ds(i * D, D)])
-        for out, which in ((other, 1 - yl), (own, yl))
-        for i, w in enumerate((gate, up, down))
-    ] + [(sd, out.at[pl.ds(SDOWN, 512)]) for out in (other, own)]
+def pick_body(mine, gate, up, down, sg, su, sd, out, pack, sem):
+    which = index("yl") if mine else 1 - index("yl")
+    copies = [(w.at[which], out.at[pl.ds(i * D, D)]) for i, w in enumerate((gate, up, down))]
+    copies.append((sd, out.at[pl.ds(SDOWN, 512)]))
     copies = [pltpu.make_async_copy(a, b, sem.at[i]) for i, (a, b) in enumerate(copies)]
     loads = [
         pltpu.make_async_copy(
-            w.at[:, pl.ds(128 * b, 128)], pack.at[pl.ds(64 * b + 32 * i, 32)], sem.at[8 + 16 * i + b]
+            w.at[:, pl.ds(128 * b, 128)], pack.at[pl.ds(64 * b + 32 * i, 32)], sem.at[4 + 16 * i + b]
         )
         for i, w in enumerate((sg, su))
         for b in range(16)
@@ -74,13 +73,9 @@
         copy.start()
     for copy in loads:
         copy.wait()
-    stores = [
-        pltpu.make_async_copy(pack, out.at[pl.ds(PACK, D // 2)], sem.at[40 + i])
-        for i, out in enumerate((own, other))
-    ]
-    for copy in stores:
-        copy.start()
-    for copy in copies + stores:
+    store = pltpu.make_async_copy(pack, out.at[pl.ds(PACK, D // 2)], sem.at[36])
+    store.start()
+    for copy in copies + [store]:
         copy.wait()
 
 
@@ -172,13 +167,13 @@
     return v * (1.0 / (1.0 + jnp.exp(-v)))
 
 
-def placed(own, up, down, up2, down2):
+def placed(own, up_low, up_high, down_low, down_high, far_low, far_high):
     yh, yl = index("yh"), index("yl")
     return (
         (2 * yh + yl, own.at[0], own.at[1]),
-        (2 * ((yh + 3) % 4) + yl, up.at[0], up.at[1]),
-        (2 * ((yh + 1) % 4) + yl, down.at[0], down.at[1]),
-        (2 * ((yh + 2) % 4) + yl, up2.at[0], down2.at[0]),
+        (2 * ((yh + 3) % 4) + yl, up_low, up_high),
+        (2 * ((yh + 1) % 4) + yl, down_low, down_high),
+        (2 * ((yh + 2) % 4) + yl, far_low, far_high),
     )
 
 
@@ -190,7 +185,7 @@
 
 
 def up_body(*refs):
-    ring, (wa, wb, wc, wd), (out, normed, hidden) = refs[0:5], refs[5:9], refs[9:]
+    ring, (wa, wb, wc, wd), (out, normed, hidden) = refs[0:7], refs[7:11], refs[11:]
     c = index("c")
     blocks = placed(*ring)
     total = jnp.zeros((USED, 128), f32)
@@ -236,7 +231,7 @@
 
 
 def down_body(*refs):
-    ring, (wa, wb, wc, wd), (back, give, skeep, sgive, hidden) = refs[0:5], refs[5:9], refs[9:]
+    ring, (wa, wb, wc, wd), (back, give, skeep, sgive, hidden) = refs[0:7], refs[7:11], refs[11:]
     blocks = placed(*ring)
 
     def rows_of(pair, first, count):
@@ -286,16 +281,17 @@
     return jax.ShapeDtypeStruct(shape, dtype)
 
 
-def ring(block, after=None):
+def ring(block):
     up = [(i, (i + 1) % 4) for i in range(4)]
     down = [(j, i) for i, j in up]
-    u = lax.ppermute(block, "yh", up)
-    d = lax.ppermute(block, "yh", down)
-    if after is not None:
-        u, d, after = lax.optimization_barrier((u, d, after))
-    u2 = lax.ppermute(u[:1], "yh", up)
-    d2 = lax.ppermute(d[1:], "yh", down)
-    return (block, u, d, u2, d2), after
+    low, high = block[0], block[1]
+    up_low = lax.ppermute(low, "yh", up)
+    down_high = lax.ppermute(high, "yh", down)
+    up_high = lax.ppermute(high, "yh", up)
+    down_low = lax.ppermute(low, "yh", down)
+    far_low = lax.ppermute(up_low, "yh", up)
+    far_high = lax.ppermute(down_high, "yh", down)
+    return (block, up_low, up_high, down_low, down_high, far_low, far_high)
 
 
 def layer(
@@ -363,25 +359,30 @@
     near = lax.ppermute(mine, tp, NEAR)
 
     slots, cols = call(meta_body, (sds((8, TOK), f32), sds((TOK, 128), f32)), 2)(chosen, scores)
-    w_own, w_other = call(
-        pick_body,
-        (sds((WROWS, 128)), sds((WROWS, 128))),
-        6,
-        [pltpu.VMEM((D // 2, 128), bf16), pltpu.SemaphoreType.DMA((42,))],
-        space=ANY,
-    )(
-        *(
-            pltpu.with_memory_space_constraint(w, pltpu.HBM)
-            for w in (expert_gate, expert_up, expert_down, shared_gate.T, shared_up.T, shared_down)
+
+    def picked(mine):
+        return call(
+            functools.partial(pick_body, mine),
+            sds((WROWS, 128)),
+            6,
+            [pltpu.VMEM((D // 2, 128), bf16), pltpu.SemaphoreType.DMA((37,))],
+            space=ANY,
+        )(
+            *(
+                pltpu.with_memory_space_constraint(w, pltpu.HBM)
+                for w in (expert_gate, expert_up, expert_down, shared_gate.T, shared_up.T, shared_down)
+            )
         )
-    )
+
+    w_other = picked(False)
+    w_own = picked(True)
 
     mixed = call(mixer_body, sds((32, TOK)), 5)(
         gate, product, taps, before, after
     )
-    mixed, near, w_other, w_own = lax.optimization_barrier((mixed, near, w_other, w_own))
+    mixed, near, w_other = lax.optimization_barrier((mixed, near, w_other))
     mixed = lax.all_gather(mixed, tp, axis=0, tiled=True)
-    mixed, w_other, w_own = lax.optimization_barrier((mixed, w_other, w_own))
+    mixed, w_other = lax.optimization_barrier((mixed, w_other))
     w_got = lax.ppermute(w_other, tp, NEAR)
     w_own_c = lax.ppermute(w_own, "c", swap)
     stream, send, shared = call(
@@ -393,22 +394,22 @@
     arrived = lax.all_to_all(send.reshape(SP, CAP, 256), "sp", 0, 0, tiled=True)
     block = jnp.concatenate([arrived.reshape(2, HALF, 256), shared], axis=1)
     block = lax.all_to_all(block, "c", 0, 0, tiled=True)
-    x_ring, w_got = ring(block, w_got)
+    x_ring = ring(block)
     w_got_c = lax.ppermute(w_got, "c", swap)
     weights = (w_own, w_got, w_own_c, w_got_c)
 
     hidden = call(
         up_body,
         sds((2, HROWS, 256)),
-        9,
+        11,
         [pltpu.VMEM((USED, D), bf16), pltpu.VMEM((SHARE, 128), f32)],
         limit=16,
     )(*x_ring, *weights)
-    h_ring, _ = ring(hidden)
+    h_ring = ring(hidden)
     back, give, skeep, sgive = call(
         down_body,
         (sds((2, HALF, 256)), sds((HALF, 256)), sds((SHARE, 256), f32), sds((SHARE, 256), f32)),
-        9,
+        11,
         [pltpu.VMEM((SHARE, 128), f32)],
         limit=12,
     )(*h_ring, *weights)

time: 201 us -> 219 us (1.090)
  waiting for transfers between devices: 62.6 us -> 81.8 us
  starting transfers between devices: 71 us -> 67.7 us
    ppermute x1, waiting for transfers between devices: 0.01 us -> 20.6 us  [layer(): w_got = lax.ppermute(w_other, tp, NEAR)]
    ppermute x8 -> x12, starting transfers between devices: 29.7 us -> 40.8 us  [the longest x2 10.9 us: ring(): far_high = lax.ppermute(down_high, 'yh', down)]
    all_to_all x1, starting transfers between devices: 14.4 us -> 3.88 us  [layer(): back = lax.all_to_all(back.reshape(SP, CAP, 256), 'sp', 0, 0, tiled=True)]
    ppermute x8 -> x12, waiting for transfers between devices: 45 us -> 40.9 us  [the longest x2 17.3 us: ring(): far_high = lax.ppermute(down_high, 'yh', down)]
    pallas_call x2 -> x3, Pallas kernels: 6.16 us -> 7.55 us  [the longest x2 3.9 us: picked(): call(functools.partial(pick_body, mine), sds((WROWS, 128)), 6, [pltpu.VME...]
  transfers between devices with their start and end apart: 18 -> 22, of which waited for: 12 -> 14; matrix products, arithmetic and copies ran while one was open for 0% -> 0% of each run, Pallas kernels for 2% -> 2%
where the time goes in v3:
time: 219 us; the launch traced here: 217 us
  waiting for transfers between devices  81.8 us (37%)
  starting transfers between devices  67.7 us (31%)
  blocking collectives  53.1 us (24%)
  Pallas kernels  13.1 us (6%)
    all_to_all x1, blocking collectives, layer(): arrived = lax.all_to_all(send.reshape(SP, CAP, 256), 'sp', 0, 0, tiled=True)  28.1 us
    ppermute x1, waiting for transfers between devices, layer(): w_got = lax.ppermute(w_other, tp, NEAR)  20.6 us
    all_gather x1, blocking collectives, layer(): mixed = lax.all_gather(mixed, tp, axis=0, tiled=True)  18.9 us
    ppermute x2, waiting for transfers between devices, ring(): far_high = lax.ppermute(down_high, 'yh', down)  17.3 us
    all_to_all x1, waiting for transfers between devices, layer(): back = lax.all_to_all(back.reshape(SP, CAP, 256), 'sp', 0, 0, tiled=True)  11.2 us
    ppermute x2, starting transfers between devices, ring(): far_high = lax.ppermute(down_high, 'yh', down)  10.9 us
    ppermute x2, waiting for transfers between devices, ring(): up_high = lax.ppermute(high, 'yh', up)  10.7 us
    ppermute x2, starting transfers between devices, ring(): down_high = lax.ppermute(high, 'yh', down)  7.97 us
  transfers between devices with their start and end apart: 22, of which 14 were waited for; matrix products, arithmetic and copies ran while one was open for 0% of the time, Pallas kernels for 2%

profile of v3, /device:TPU:1, one launch (start us, length us, event | category | flops | bytes accessed | tf_op | source)
XLA Modules:
  0.0 216.9 jit_solution(12918338364575887888)
XLA Ops:
  1.1 5.9 %collective-permute-start.2 = (bf16[904,128]{1,0:T(8,128)(2,1)S(1)}, bf16[904,128]{1,0:T(8,128)(2,1)S(1)}, u32[]{:S(2)}, u32[]{:S(2)}) collective-permute-start(bf16[904,128]{1,0:T(8,128)(2,1)S(1)} %get-tuple-element.34.mine), channel_id=1, source_target_pairs={{0,2},{2,0},{4,6},{6,4},{8,10},{10,8},{12,14},{14,12},{1,15},{3,5}... | collective-permute-start | bytes 694280 | tf_op jit(solution)/shard_map/ppermute | solution.py:359
  7.0 3.1 %collective-permute-start = (bf16[32,1]{1,0:T(8,128)(2,1)S(1)}, bf16[32,1]{1,0:T(8,128)(2,1)S(1)}, u32[]{:S(2)}, u32[]{:S(2)}) collective-permute-start(bf16[32,1]{1,0:T(8,128)(2,1)S(1)} %get-tuple-element.32), channel_id=1, source_target_pairs={{0,16},{16,32},{32,48},{48,64},{64,80},{80,96},{96,112},{112,128},... | collective-permute-start | bytes 200 | tf_op jit(solution)/shard_map/ppermute | solution.py:357
  15.0 18.9 %all_gather.3.mixed = bf16[512,384]{1,0:T(8,128)(2,1)S(1)} all-gather(bf16[32,384]{1,0:T(8,128)(2,1)S(1)} %shard_map.146), channel_id=1, replica_groups=mesh['sp'=32,'yh'=4,'yl'=2,'c'=2] {'yh','yl','c'}, dimensions={0}, use_global_device_ids=true | all-gather | bytes 417792 | tf_op jit(solution)/shard_map/all_gather | solution.py:384
  39.9 20.6 %collective-permute-done.9.refs_8_ = bf16[7680,128]{1,0:T(8,128)(2,1)S(1)} collective-permute-done((bf16[7680,128]{1,0:T(8,128)(2,1)S(1)}, bf16[7680,128]{1,0:T(8,128)(2,1)S(1)}, u32[]{:S(2)}, u32[]{:S(2)}) %collective-permute-start.9) | collective-permute-done | bytes 1966112 | tf_op jit(solution)/shard_map/ppermute | solution.py:386
  63.7 28.1 %all_to_all.15 = bf16[32,24,256]{2,1,0:T(8,128)(2,1)S(1)} all-to-all(bf16[32,24,256]{2,1,0:T(8,128)(2,1)S(1)} %bitcast.20), channel_id=1, replica_groups=mesh['sp'=32,'yh'=4,'yl'=2,'c'=2] {'sp'}, dimensions={0} | all-to-all | bytes 786432 | tf_op jit(solution)/shard_map/all_to_all | solution.py:394
  91.9 6.1 %all_to_all.16.refs_0_ = bf16[2,488,256]{2,1,0:T(8,128)(2,1)S(1)} all-to-all(bf16[2,488,256]{2,1,0:T(8,128)(2,1)S(1)} %pad_maximum_fusion), channel_id=1, replica_groups=mesh['sp'=32,'yh'=4,'yl'=2,'c'=2] {'c'}, dimensions={0} | all-to-all | bytes 999424 | tf_op jit(solution)/shard_map/all_to_all | solution.py:396
  100.0 4.9 %collective-permute-start.4 = (bf16[488,256]{1,0:T(8,128)(2,1)S(1)}, bf16[488,256]{1,0:T(8,128)(2,1)S(1)}, u32[]{:S(2)}, u32[]{:S(2)}) collective-permute-start(bf16[488,256]{1,0:T(8,128)(2,1)S(1)} %get-tuple-element.53), channel_id=1, source_target_pairs={{0,4},{4,8},{8,12},{12,0},{1,5},{5,9},{9,13},{13,1},{2,6},{6,10},{... | collective-permute-start | bytes 749576 | tf_op jit(solution)/shard_map/ppermute | solution.py:290
  104.9 2.5 %collective-permute-start.6 = (bf16[488,256]{1,0:T(8,128)(2,1)S(1)}, bf16[488,256]{1,0:T(8,128)(2,1)S(1)}, u32[]{:S(2)}, u32[]{:S(2)}) collective-permute-start(bf16[488,256]{1,0:T(8,128)(2,1)S(1)} %get-tuple-element.53), channel_id=1, source_target_pairs={{4,0},{8,4},{12,8},{0,12},{5,1},{9,5},{13,9},{1,13},{6,2},{10,6},{... | collective-permute-start | bytes 749576 | tf_op jit(solution)/shard_map/ppermute | solution.py:289
  107.4 4.3 %collective-permute-done.3.refs_1_ = bf16[488,256]{1,0:T(8,128)(2,1)S(1)} collective-permute-done((bf16[488,256]{1,0:T(8,128)(2,1)S(1)}, bf16[488,256]{1,0:T(8,128)(2,1)S(1)}, u32[]{:S(2)}, u32[]{:S(2)}) %collective-permute-start.3) | collective-permute-done | bytes 249888 | tf_op jit(solution)/shard_map/ppermute | solution.py:288
  113.6 8.2 %collective-permute-done.4.refs_2_ = bf16[488,256]{1,0:T(8,128)(2,1)S(1)} collective-permute-done((bf16[488,256]{1,0:T(8,128)(2,1)S(1)}, bf16[488,256]{1,0:T(8,128)(2,1)S(1)}, u32[]{:S(2)}, u32[]{:S(2)}) %collective-permute-start.4) | collective-permute-done | bytes 249888 | tf_op jit(solution)/shard_map/ppermute | solution.py:290
  123.8 5.5 %collective-permute-start.8 = (bf16[488,256]{1,0:T(8,128)(2,1)S(1)}, bf16[488,256]{1,0:T(8,128)(2,1)S(1)}, u32[]{:S(2)}, u32[]{:S(2)}) collective-permute-start(bf16[488,256]{1,0:T(8,128)(2,1)S(1)} %collective-permute-done.6.refs_4_), channel_id=1, source_target_pairs={{4,0},{8,4},{12,8},{0,12},{5,1},{9,5},{13,9},{1,13},{6,2},{10,6},{... | collective-permute-start | bytes 749576 | tf_op jit(solution)/shard_map/ppermute | solution.py:293
  131.0 11.8 %collective-permute-done.8.refs_6_ = bf16[488,256]{1,0:T(8,128)(2,1)S(1)} collective-permute-done((bf16[488,256]{1,0:T(8,128)(2,1)S(1)}, bf16[488,256]{1,0:T(8,128)(2,1)S(1)}, u32[]{:S(2)}, u32[]{:S(2)}) %collective-permute-start.8) | collective-permute-done | bytes 249888 | tf_op jit(solution)/shard_map/ppermute | solution.py:293
  142.9 3.6 %shard_map.151.refs_0_ = bf16[2,408,256]{2,1,0:T(8,128)(2,1)S(1)} custom-call(bf16[2,488,256]{2,1,0:T(8,128)(2,1)S(1)} %all_to_all.16.refs_0_, bf16[488,256]{1,0:T(8,128)(2,1)S(1)} %collective-permute-done.3.refs_1_, bf16[488,256]{1,0:T(8,128)(2,1)S(1)} %collective-permute-done.4.refs_2_, bf16[488,256]{1,0:T(8,128)(2,1)S(1)} %collective-permute-done.5.refs_3_, ...), custom_call_target="tpu_custom_call" | custom-call | tf_op jit(solution)/shard_map/pallas_call | solution.py:401
  148.5 5.5 %collective-permute-start.15 = (bf16[408,256]{1,0:T(8,128)(2,1)S(1)}, bf16[408,256]{1,0:T(8,128)(2,1)S(1)}, u32[]{:S(2)}, u32[]{:S(2)}) collective-permute-start(bf16[408,256]{1,0:T(8,128)(2,1)S(1)} %get-tuple-element.55), channel_id=1, source_target_pairs={{4,0},{8,4},{12,8},{0,12},{5,1},{9,5},{13,9},{1,13},{6,2},{10,6},{... | collective-permute-start | bytes 626696 | tf_op jit(solution)/shard_map/ppermute | solution.py:289
  155.9 5.5 %collective-permute-start.14 = (bf16[408,256]{1,0:T(8,128)(2,1)S(1)}, bf16[408,256]{1,0:T(8,128)(2,1)S(1)}, u32[]{:S(2)}, u32[]{:S(2)}) collective-permute-start(bf16[408,256]{1,0:T(8,128)(2,1)S(1)} %get-tuple-element.56), channel_id=1, source_target_pairs={{4,0},{8,4},{12,8},{0,12},{5,1},{9,5},{13,9},{1,13},{6,2},{10,6},{... | collective-permute-start | bytes 626696 | tf_op jit(solution)/shard_map/ppermute | solution.py:291
  163.3 5.5 %collective-permute-start.17 = (bf16[408,256]{1,0:T(8,128)(2,1)S(1)}, bf16[408,256]{1,0:T(8,128)(2,1)S(1)}, u32[]{:S(2)}, u32[]{:S(2)}) collective-permute-start(bf16[408,256]{1,0:T(8,128)(2,1)S(1)} %collective-permute-done.15.refs_4_), channel_id=1, source_target_pairs={{4,0},{8,4},{12,8},{0,12},{5,1},{9,5},{13,9},{1,13},{6,2},{10,6},{... | collective-permute-start | bytes 626696 | tf_op jit(solution)/shard_map/ppermute | solution.py:293
  168.8 2.5 %collective-permute-done.13.refs_2_ = bf16[408,256]{1,0:T(8,128)(2,1)S(1)} collective-permute-done((bf16[408,256]{1,0:T(8,128)(2,1)S(1)}, bf16[408,256]{1,0:T(8,128)(2,1)S(1)}, u32[]{:S(2)}, u32[]{:S(2)}) %collective-permute-start.13) | collective-permute-done | bytes 208928 | tf_op jit(solution)/shard_map/ppermute | solution.py:290
  171.3 5.6 %collective-permute-done.14.refs_3_ = bf16[408,256]{1,0:T(8,128)(2,1)S(1)} collective-permute-done((bf16[408,256]{1,0:T(8,128)(2,1)S(1)}, bf16[408,256]{1,0:T(8,128)(2,1)S(1)}, u32[]{:S(2)}, u32[]{:S(2)}) %collective-permute-start.14) | collective-permute-done | bytes 208928 | tf_op jit(solution)/shard_map/ppermute | solution.py:291
  178.1 5.5 %collective-permute-done.17.refs_6_ = bf16[408,256]{1,0:T(8,128)(2,1)S(1)} collective-permute-done((bf16[408,256]{1,0:T(8,128)(2,1)S(1)}, bf16[408,256]{1,0:T(8,128)(2,1)S(1)}, u32[]{:S(2)}, u32[]{:S(2)}) %collective-permute-start.17) | collective-permute-done | bytes 208928 | tf_op jit(solution)/shard_map/ppermute | solution.py:293
  185.4 2.5 %collective-permute-start.18 = (bf16[384,256]{1,0:T(8,128)(2,1)S(1)}, bf16[384,256]{1,0:T(8,128)(2,1)S(1)}, u32[]{:S(2)}, u32[]{:S(2)}) collective-permute-start(bf16[384,256]{1,0:T(8,128)(2,1)S(1)} %get-tuple-element.47), channel_id=1, source_target_pairs={{0,1},{1,0},{2,3},{3,2},{4,5},{5,4},{6,7},{7,6},{8,9},{9,8},{10,11... | collective-permute-start | bytes 589832 | tf_op jit(solution)/shard_map/ppermute | solution.py:416
  189.7 3.9 %all-to-all-start.2 = ((bf16[32,24,256]{2,1,0:T(8,128)(2,1)}), bf16[32,24,256]{2,1,0:T(8,128)(2,1)S(1)}, u32[]{:S(2)}, u32[]{:S(2)}) async-start(bf16[32,24,256]{2,1,0:T(8,128)(2,1)} %bitcast.12), calls=%async_computation.2 | async-start | bytes 786432 | tf_op jit(solution)/shard_map/all_to_all | solution.py:419
  193.6 2.3 %collective-permute-start.19 = (f32[96,256]{1,0:T(8,128)S(1)}, f32[96,256]{1,0:T(8,128)S(1)}, u32[]{:S(2)}, u32[]{:S(2)}) collective-permute-start(f32[96,256]{1,0:T(8,128)S(1)} %get-tuple-element.50), channel_id=1, source_target_pairs={{0,1},{1,0},{2,3},{3,2},{4,5},{5,4},{6,7},{7,6},{8,9},{9,8},{10,11... | collective-permute-start | bytes 294920 | tf_op jit(solution)/shard_map/ppermute | solution.py:417
  196.8 11.2 %all-to-all-done.2 = bf16[32,24,256]{2,1,0:T(8,128)(2,1)S(1)} async-done(((bf16[32,24,256]{2,1,0:T(8,128)(2,1)}), bf16[32,24,256]{2,1,0:T(8,128)(2,1)S(1)}, u32[]{:S(2)}, u32[]{:S(2)}) %all-to-all-start.2) | async-done | bytes 393248 | tf_op jit(solution)/shard_map/all_to_all | solution.py:419
  210.6 5.7 %collective-permute-done.20.other = f32[384,128]{1,0:T(8,128)S(1)} collective-permute-done((f32[384,128]{1,0:T(8,128)S(1)}, f32[384,128]{1,0:T(8,128)S(1)}, u32[]{:S(2)}, u32[]{:S(2)}) %collective-permute-start.20) | collective-permute-done | bytes 196640 | tf_op jit(solution)/shard_map/ppermute | solution.py:423
  (37 shorter events, 37.4 us)
Async XLA Ops:
  1.1 13.9 %collective-permute-start.2 = (bf16[904,128]{1,0:T(8,128)(2,1)S(1)}, bf16[904,128]{1,0:T(8,128)(2,1)S(1)}, u32[]{:S(2)}, u32[]{:S(2)}) collective-permute-start(bf16[904,128]{1,0:T(8,128)(2,1)S(1)} %get-tuple-element.34.mine), channel_id=1, source_target_pairs={{0,2},{2,0},{4,6},{6,4},{8,10},{10,8},{12,14},{14,12},{1,15},{3,5}... | collective-permute-start | bytes 694280 | tf_op jit(solution)/shard_map/ppermute | solution.py:359
  7.0 6.4 %collective-permute-start = (bf16[32,1]{1,0:T(8,128)(2,1)S(1)}, bf16[32,1]{1,0:T(8,128)(2,1)S(1)}, u32[]{:S(2)}, u32[]{:S(2)}) collective-permute-start(bf16[32,1]{1,0:T(8,128)(2,1)S(1)} %get-tuple-element.32), channel_id=1, source_target_pairs={{0,16},{16,32},{32,48},{48,64},{64,80},{80,96},{96,112},{112,128},... | collective-permute-start | bytes 200 | tf_op jit(solution)/shard_map/ppermute | solution.py:357
  10.2 4.7 %collective-permute-start.1 = (bf16[32,1]{1,0:T(8,128)(2,1)S(1)}, bf16[32,1]{1,0:T(8,128)(2,1)S(1)}, u32[]{:S(2)}, u32[]{:S(2)}) collective-permute-start(bf16[32,1]{1,0:T(8,128)(2,1)S(1)} %get-tuple-element.33), channel_id=1, source_target_pairs={{16,0},{32,16},{48,32},{64,48},{80,64},{96,80},{112,96},{128,112},... | collective-permute-start | bytes 200 | tf_op jit(solution)/shard_map/ppermute | solution.py:358
  33.9 26.6 %collective-permute-start.9 = (bf16[7680,128]{1,0:T(8,128)(2,1)S(1)}, bf16[7680,128]{1,0:T(8,128)(2,1)S(1)}, u32[]{:S(2)}, u32[]{:S(2)}) collective-permute-start(bf16[7680,128]{1,0:T(8,128)(2,1)S(1)} %shard_map.147), channel_id=1, source_target_pairs={{0,2},{2,0},{4,6},{6,4},{8,10},{10,8},{12,14},{14,12},{1,15},{3,5}... | collective-permute-start | bytes 5898248 | tf_op jit(solution)/shard_map/ppermute | solution.py:386
  37.8 105.1 %collective-permute-start.10 = (bf16[7680,128]{1,0:T(8,128)(2,1)S(1)}, bf16[7680,128]{1,0:T(8,128)(2,1)S(1)}, u32[]{:S(2)}, u32[]{:S(2)}) collective-permute-start(bf16[7680,128]{1,0:T(8,128)(2,1)S(1)} %shard_map.150.refs_7_), channel_id=1, source_target_pairs={{0,1},{1,0},{2,3},{3,2},{4,5},{5,4},{6,7},{7,6},{8,9},{9,8},{10,11... | collective-permute-start | bytes 5898248 | tf_op jit(solution)/shard_map/ppermute | solution.py:387
  60.5 82.4 %collective-permute-start.11 = (bf16[7680,128]{1,0:T(8,128)(2,1)S(1)}, bf16[7680,128]{1,0:T(8,128)(2,1)S(1)}, u32[]{:S(2)}, u32[]{:S(2)}) collective-permute-start(bf16[7680,128]{1,0:T(8,128)(2,1)S(1)} %collective-permute-done.9.refs_8_), channel_id=1, source_target_pairs={{0,1},{1,0},{2,3},{3,2},{4,5},{5,4},{6,7},{7,6},{8,9},{9,8},{10,11... | collective-permute-start | bytes 5898248 | tf_op jit(solution)/shard_map/ppermute | solution.py:398
  98.0 13.7 %collective-permute-start.3 = (bf16[488,256]{1,0:T(8,128)(2,1)S(1)}, bf16[488,256]{1,0:T(8,128)(2,1)S(1)}, u32[]{:S(2)}, u32[]{:S(2)}) collective-permute-start(bf16[488,256]{1,0:T(8,128)(2,1)S(1)} %get-tuple-element.54), channel_id=1, source_target_pairs={{0,4},{4,8},{8,12},{12,0},{1,5},{5,9},{9,13},{13,1},{2,6},{6,10},{... | collective-permute-start | bytes 749576 | tf_op jit(solution)/shard_map/ppermute | solution.py:288
  100.0 21.8 %collective-permute-start.4 = (bf16[488,256]{1,0:T(8,128)(2,1)S(1)}, bf16[488,256]{1,0:T(8,128)(2,1)S(1)}, u32[]{:S(2)}, u32[]{:S(2)}) collective-permute-start(bf16[488,256]{1,0:T(8,128)(2,1)S(1)} %get-tuple-element.53), channel_id=1, source_target_pairs={{0,4},{4,8},{8,12},{12,0},{1,5},{5,9},{9,13},{13,1},{2,6},{6,10},{... | collective-permute-start | bytes 749576 | tf_op jit(solution)/shard_map/ppermute | solution.py:290
  104.9 18.9 %collective-permute-start.6 = (bf16[488,256]{1,0:T(8,128)(2,1)S(1)}, bf16[488,256]{1,0:T(8,128)(2,1)S(1)}, u32[]{:S(2)}, u32[]{:S(2)}) collective-permute-start(bf16[488,256]{1,0:T(8,128)(2,1)S(1)} %get-tuple-element.53), channel_id=1, source_target_pairs={{4,0},{8,4},{12,8},{0,12},{5,1},{9,5},{13,9},{1,13},{6,2},{10,6},{... | collective-permute-start | bytes 749576 | tf_op jit(solution)/shard_map/ppermute | solution.py:289
  111.7 17.5 %collective-permute-start.5 = (bf16[488,256]{1,0:T(8,128)(2,1)S(1)}, bf16[488,256]{1,0:T(8,128)(2,1)S(1)}, u32[]{:S(2)}, u32[]{:S(2)}) collective-permute-start(bf16[488,256]{1,0:T(8,128)(2,1)S(1)} %get-tuple-element.54), channel_id=1, source_target_pairs={{4,0},{8,4},{12,8},{0,12},{5,1},{9,5},{13,9},{1,13},{6,2},{10,6},{... | collective-permute-start | bytes 749576 | tf_op jit(solution)/shard_map/ppermute | solution.py:291
  121.8 9.2 %collective-permute-start.7 = (bf16[488,256]{1,0:T(8,128)(2,1)S(1)}, bf16[488,256]{1,0:T(8,128)(2,1)S(1)}, u32[]{:S(2)}, u32[]{:S(2)}) collective-permute-start(bf16[488,256]{1,0:T(8,128)(2,1)S(1)} %collective-permute-done.3.refs_1_), channel_id=1, source_target_pairs={{0,4},{4,8},{8,12},{12,0},{1,5},{5,9},{9,13},{13,1},{2,6},{6,10},{... | collective-permute-start | bytes 749576 | tf_op jit(solution)/shard_map/ppermute | solution.py:292
  123.8 19.1 %collective-permute-start.8 = (bf16[488,256]{1,0:T(8,128)(2,1)S(1)}, bf16[488,256]{1,0:T(8,128)(2,1)S(1)}, u32[]{:S(2)}, u32[]{:S(2)}) collective-permute-start(bf16[488,256]{1,0:T(8,128)(2,1)S(1)} %collective-permute-done.6.refs_4_), channel_id=1, source_target_pairs={{4,0},{8,4},{12,8},{0,12},{5,1},{9,5},{13,9},{1,13},{6,2},{10,6},{... | collective-permute-start | bytes 749576 | tf_op jit(solution)/shard_map/ppermute | solution.py:293
  146.6 14.8 %collective-permute-start.12 = (bf16[408,256]{1,0:T(8,128)(2,1)S(1)}, bf16[408,256]{1,0:T(8,128)(2,1)S(1)}, u32[]{:S(2)}, u32[]{:S(2)}) collective-permute-start(bf16[408,256]{1,0:T(8,128)(2,1)S(1)} %get-tuple-element.56), channel_id=1, source_target_pairs={{0,4},{4,8},{8,12},{12,0},{1,5},{5,9},{9,13},{13,1},{2,6},{6,10},{... | collective-permute-start | bytes 626696 | tf_op jit(solution)/shard_map/ppermute | solution.py:288
  148.5 14.8 %collective-permute-start.15 = (bf16[408,256]{1,0:T(8,128)(2,1)S(1)}, bf16[408,256]{1,0:T(8,128)(2,1)S(1)}, u32[]{:S(2)}, u32[]{:S(2)}) collective-permute-start(bf16[408,256]{1,0:T(8,128)(2,1)S(1)} %get-tuple-element.55), channel_id=1, source_target_pairs={{4,0},{8,4},{12,8},{0,12},{5,1},{9,5},{13,9},{1,13},{6,2},{10,6},{... | collective-permute-start | bytes 626696 | tf_op jit(solution)/shard_map/ppermute | solution.py:289
  154.0 17.3 %collective-permute-start.13 = (bf16[408,256]{1,0:T(8,128)(2,1)S(1)}, bf16[408,256]{1,0:T(8,128)(2,1)S(1)}, u32[]{:S(2)}, u32[]{:S(2)}) collective-permute-start(bf16[408,256]{1,0:T(8,128)(2,1)S(1)} %get-tuple-element.55), channel_id=1, source_target_pairs={{0,4},{4,8},{8,12},{12,0},{1,5},{5,9},{9,13},{13,1},{2,6},{6,10},{... | collective-permute-start | bytes 626696 | tf_op jit(solution)/shard_map/ppermute | solution.py:290
  155.9 21.0 %collective-permute-start.14 = (bf16[408,256]{1,0:T(8,128)(2,1)S(1)}, bf16[408,256]{1,0:T(8,128)(2,1)S(1)}, u32[]{:S(2)}, u32[]{:S(2)}) collective-permute-start(bf16[408,256]{1,0:T(8,128)(2,1)S(1)} %get-tuple-element.56), channel_id=1, source_target_pairs={{4,0},{8,4},{12,8},{0,12},{5,1},{9,5},{13,9},{1,13},{6,2},{10,6},{... | collective-permute-start | bytes 626696 | tf_op jit(solution)/shard_map/ppermute | solution.py:291
  161.4 16.7 %collective-permute-start.16 = (bf16[408,256]{1,0:T(8,128)(2,1)S(1)}, bf16[408,256]{1,0:T(8,128)(2,1)S(1)}, u32[]{:S(2)}, u32[]{:S(2)}) collective-permute-start(bf16[408,256]{1,0:T(8,128)(2,1)S(1)} %collective-permute-done.12.refs_1_), channel_id=1, source_target_pairs={{0,4},{4,8},{8,12},{12,0},{1,5},{5,9},{9,13},{13,1},{2,6},{6,10},{... | collective-permute-start | bytes 626696 | tf_op jit(solution)/shard_map/ppermute | solution.py:292
  163.3 20.3 %collective-permute-start.17 = (bf16[408,256]{1,0:T(8,128)(2,1)S(1)}, bf16[408,256]{1,0:T(8,128)(2,1)S(1)}, u32[]{:S(2)}, u32[]{:S(2)}) collective-permute-start(bf16[408,256]{1,0:T(8,128)(2,1)S(1)} %collective-permute-done.15.refs_4_), channel_id=1, source_target_pairs={{4,0},{8,4},{12,8},{0,12},{5,1},{9,5},{13,9},{1,13},{6,2},{10,6},{... | collective-permute-start | bytes 626696 | tf_op jit(solution)/shard_map/ppermute | solution.py:293
  185.4 3.6 %collective-permute-start.18 = (bf16[384,256]{1,0:T(8,128)(2,1)S(1)}, bf16[384,256]{1,0:T(8,128)(2,1)S(1)}, u32[]{:S(2)}, u32[]{:S(2)}) collective-permute-start(bf16[384,256]{1,0:T(8,128)(2,1)S(1)} %get-tuple-element.47), channel_id=1, source_target_pairs={{0,1},{1,0},{2,3},{3,2},{4,5},{5,4},{6,7},{7,6},{8,9},{9,8},{10,11... | collective-permute-start | bytes 589832 | tf_op jit(solution)/shard_map/ppermute | solution.py:416
  189.7 18.3 %all-to-all-start.2 = ((bf16[32,24,256]{2,1,0:T(8,128)(2,1)}), bf16[32,24,256]{2,1,0:T(8,128)(2,1)S(1)}, u32[]{:S(2)}, u32[]{:S(2)}) async-start(bf16[32,24,256]{2,1,0:T(8,128)(2,1)} %bitcast.12), calls=%async_computation.2 | async-start | bytes 786432 | tf_op jit(solution)/shard_map/all_to_all | solution.py:419
  193.6 3.2 %collective-permute-start.19 = (f32[96,256]{1,0:T(8,128)S(1)}, f32[96,256]{1,0:T(8,128)S(1)}, u32[]{:S(2)}, u32[]{:S(2)}) collective-permute-start(f32[96,256]{1,0:T(8,128)S(1)} %get-tuple-element.50), channel_id=1, source_target_pairs={{0,1},{1,0},{2,3},{3,2},{4,5},{5,4},{6,7},{7,6},{8,9},{9,8},{10,11... | collective-permute-start | bytes 294920 | tf_op jit(solution)/shard_map/ppermute | solution.py:417
  208.6 7.6 %collective-permute-start.20 = (f32[384,128]{1,0:T(8,128)S(1)}, f32[384,128]{1,0:T(8,128)S(1)}, u32[]{:S(2)}, u32[]{:S(2)}) collective-permute-start(f32[384,128]{1,0:T(8,128)S(1)} %get-tuple-element.52), channel_id=1, source_target_pairs={{0,2},{2,0},{4,6},{6,4},{8,10},{10,8},{12,14},{14,12},{1,15},{3,5}... | collective-permute-start | bytes 589832 | tf_op jit(solution)/shard_map/ppermute | solution.py:423

commit v4 on v3

--- a/solution.py
+++ b/solution.py
@@ -167,95 +167,159 @@
     return v * (1.0 / (1.0 + jnp.exp(-v)))
 
 
-def placed(own, up_low, up_high, down_low, down_high, far_low, far_high):
+def split_body(arrived, shared, mine, give):
+    c = index("c")
+    for out, core in ((mine, c), (give, 1 - c)):
+        out[0:HALF, :] = arrived[pl.ds(pl.multiple_of(core * HALF, HALF), HALF), :]
+        out[HALF:, :] = shared[core]
+
+
+def placed(mine, other, up_mine, up_other, down_mine, down_other, far_mine, far_other):
     yh, yl = index("yh"), index("yl")
     return (
-        (2 * yh + yl, own.at[0], own.at[1]),
-        (2 * ((yh + 3) % 4) + yl, up_low, up_high),
-        (2 * ((yh + 1) % 4) + yl, down_low, down_high),
-        (2 * ((yh + 2) % 4) + yl, far_low, far_high),
+        (2 * yh + yl, mine, other),
+        (2 * ((yh + 3) % 4) + yl, up_mine, up_other),
+        (2 * ((yh + 1) % 4) + yl, down_mine, down_other),
+        (2 * ((yh + 2) % 4) + yl, far_mine, far_other),
     )
 
 
 def slice_of(y, core, near):
     if near:
         yl = index("yl")
-        y = (y + 2 * yl + 7) % 8 if core else y + 1 - 2 * yl
+        y = jnp.where(core == 1, (y + 2 * yl + 7) % 8, y + 1 - 2 * yl)
     return 2 * y + core
 
 
-def up_body(*refs):
-    ring, (wa, wb, wc, wd), (out, normed, hidden) = refs[0:7], refs[7:11], refs[11:]
+def rows_of(weights, first, count):
+    n = pl.multiple_of(first, 32)
+    return jnp.concatenate([w[pl.ds(n, count), :] for w in weights], axis=1)
+
+
+def pieces(y, c):
+    return [slice_of(y, core, h) for core in (c, 1 - c) for h in range(2)]
+
+
+def up_part(blocks, weights, scaled, squares):
+    wa, wb, wc, wd = weights
     c = index("c")
-    blocks = placed(*ring)
-    total = jnp.zeros((USED, 128), f32)
-    for _, *halves in blocks:
-        for x in halves:
-            for h in range(2):
-                v = x[0:USED, 128 * h : 128 * h + 128].astype(f32)
-                total = total + v * v
-    inverse = lax.rsqrt(jnp.sum(total, axis=1, keepdims=True) / D + epsilon)
-    for y, *halves in blocks:
-        for core, x in enumerate(halves):
+    for n, (y, *halves) in enumerate(blocks):
+        for i, x in enumerate(halves):
             for h in range(2):
                 lanes = slice(128 * h, 128 * h + 128)
+                v = x[0:USED, lanes].astype(f32)
+                squares = squares + v * v
                 gain = x[USED:BLOCK, lanes].astype(f32)[0:1, :]
-                column = pl.ds(pl.multiple_of(128 * slice_of(y, core, h), 128), 128)
-                normed[:, column] = (x[0:USED, lanes].astype(f32) * inverse * gain).astype(bf16)
-    x = normed[0:HALF, :]
-    for pair, core in (((wa, wb), c), ((wc, wd), 1 - c)):
-        g = dot(x, jnp.concatenate([w[0:D, :] for w in pair], axis=1))
-        u = dot(x, jnp.concatenate([w[D : 2 * D, :] for w in pair], axis=1))
-        out[core, 0:HALF, :] = (silu(g) * u).astype(bf16)
-    packed = jnp.concatenate(
-        [
-            jnp.concatenate([w[PACK + 64 * b : PACK + 64 * b + 64, :] for b in range(16)], axis=1)
-            for w in (wa, wc, wb, wd)
-        ],
-        axis=0,
-    )
-    s = lax.dot_general(
-        normed[HALF:, :], packed, (((1,), (1,)), ((), ())), preferred_element_type=f32
-    )
+                at = 512 * n + 256 * i + 128 * h
+                scaled[:, at : at + 128] = (v * gain).astype(bf16)
+    results = []
+    for pair in ((wa, wb), (wc, wd)):
+        for base in (0, D):
+            total = jnp.zeros((HALF, 256), f32)
+            for n, (y, *_) in enumerate(blocks):
+                w = [rows_of(pair, base + 128 * p, 128) for p in pieces(y, c)]
+                x = scaled[0:HALF, 512 * n : 512 * n + 512]
+                total = total + dot(x, jnp.concatenate(w, axis=0))
+            results.append(total)
+    shared = jnp.zeros((SHARE, 256), f32)
+    for n, (y, *_) in enumerate(blocks):
+        packed = jnp.concatenate(
+            [
+                jnp.concatenate([rows_of([w], PACK + 64 * p, 64) for p in pieces(y, c)], axis=1)
+                for w in (wa, wc, wb, wd)
+            ],
+            axis=0,
+        )
+        x = scaled[HALF:USED, 512 * n : 512 * n + 512]
+        shared = shared + lax.dot_general(
+            x, packed, (((1,), (1,)), ((), ())), preferred_element_type=f32
+        )
+    return squares, results, shared
+
+
+def up_near_body(*refs):
+    halves, weights, (squares, products, shared, scaled) = refs[0:6], refs[6:10], refs[10:]
+    blocks = placed(*halves, None, None)[:3]
+    total, results, part = up_part(blocks, weights, scaled, jnp.zeros((USED, 128), f32))
+    squares[...] = total
+    for i, value in enumerate(results):
+        products[i] = value
+    shared[...] = part
+
+
+def up_far_body(*refs):
+    far, weights, (squares, products, shared), (mine, other, scaled, hidden) = (
+        refs[0:2],
+        refs[2:6],
+        refs[6:9],
+        refs[9:],
+    )
+    c = index("c")
+    blocks = placed(*[None] * 6, *far)[3:]
+    total, results, part = up_part(blocks, weights, scaled, squares[...])
+    inverse = lax.rsqrt(jnp.sum(total, axis=1, keepdims=True) / D + epsilon)
+    rows = inverse[0:HALF]
+    for i, out in enumerate((mine, other)):
+        g = (products[2 * i] + results[2 * i]) * rows
+        u = (products[2 * i + 1] + results[2 * i + 1]) * rows
+        out[0:HALF, :] = (silu(g) * u).astype(bf16)
+    s = (shared[...] + part) * inverse[HALF:]
     h = (silu(s) * pltpu.roll(s, 256 - 32, 1)).astype(bf16)
     i = lax.broadcasted_iota(i32, (256, 128), 0)
     j = lax.broadcasted_iota(i32, (256, 128), 1)
     goes = (lax.shift_right_logical(i, 6) * 32 + (i & 31)) ^ (c * 32)
     perm = jnp.where(((i & 32) == 0) & (goes == j), 1.0, 0.0).astype(bf16)
     hidden[...] = dot(h, perm)
-    for half in range(2):
+    for half, out in enumerate((mine, other)):
         n = 48 * half
-        out[half, HALF:HROWS, :] = jnp.concatenate(
+        out[HALF:HROWS, :] = jnp.concatenate(
             [hidden[n : n + 24, :], hidden[n + 24 : n + 48, :]], axis=1
         ).astype(bf16)
 
 
-def down_body(*refs):
-    ring, (wa, wb, wc, wd), (back, give, skeep, sgive, hidden) = refs[0:7], refs[7:11], refs[11:]
-    blocks = placed(*ring)
-
-    def rows_of(pair, first, count):
-        n = pl.multiple_of(first, 32)
-        return jnp.concatenate([w[pl.ds(n, count), :] for w in pair], axis=1)
-
-    for pair, out, sout in (((wc, wd), give, sgive), ((wa, wb), back.at[index("c")], skeep)):
+def down_part(blocks, weights, hidden):
+    wa, wb, wc, wd = weights
+    c = index("c")
+    results = []
+    for pair in ((wa, wb), (wc, wd)):
         total = jnp.zeros((HALF, 256), f32)
         shared = jnp.zeros((SHARE, 256), f32)
         for y, *halves in blocks:
-            for core, x in enumerate(halves):
-                w = [rows_of(pair, DOWN + 128 * slice_of(y, core, h), 128) for h in range(2)]
+            order = pieces(y, c)
+            for i, x in enumerate(halves):
+                w = [rows_of(pair, DOWN + 128 * p, 128) for p in order[2 * i : 2 * i + 2]]
                 total = total + dot(x[0:HALF, :], jnp.concatenate(w, axis=0))
                 tail = x[HALF:HROWS, :].astype(f32)
-                hidden[48 * core : 48 * core + 24, :] = tail[:, 0:128]
-                hidden[48 * core + 24 : 48 * core + 48, :] = tail[:, 128:256]
+                hidden[48 * i : 48 * i + 24, :] = tail[:, 0:128]
+                hidden[48 * i + 24 : 48 * i + 48, :] = tail[:, 128:256]
             w = [
                 rows_of(pair, SDOWN + 32 * slice_of(y, core, h), 32)
                 for h in range(2)
                 for core in range(2)
             ]
             shared = shared + dot(hidden[...].astype(bf16), jnp.concatenate(w, axis=0))
-        out[...] = total.astype(bf16)
-        sout[...] = shared
+        results.append((total, shared))
+    return results
+
+
+def down_near_body(*refs):
+    halves, weights, (products, shared, hidden) = refs[0:6], refs[6:10], refs[10:]
+    for i, (a, b) in enumerate(down_part(placed(*halves, None, None)[:3], weights, hidden)):
+        products[i] = a
+        shared[i] = b
+
+
+def down_far_body(*refs):
+    far, weights, (products, shared), (back, give, skeep, sgive, hidden) = (
+        refs[0:2],
+        refs[2:6],
+        refs[6:8],
+        refs[8:],
+    )
+    parts = down_part(placed(*[None] * 6, *far)[3:], weights, hidden)
+    for i, (out, sout) in enumerate(((back.at[index("c")], skeep), (give, sgive))):
+        out[...] = (products[i] + parts[i][0]).astype(bf16)
+        sout[...] = shared[i] + parts[i][1]
 
 
 def combine_body(rows, cols, skeep, sother, keep, give, acc):
@@ -281,17 +345,16 @@
     return jax.ShapeDtypeStruct(shape, dtype)
 
 
-def ring(block):
+def ring(mine, other):
     up = [(i, (i + 1) % 4) for i in range(4)]
     down = [(j, i) for i, j in up]
-    low, high = block[0], block[1]
-    up_low = lax.ppermute(low, "yh", up)
-    down_high = lax.ppermute(high, "yh", down)
-    up_high = lax.ppermute(high, "yh", up)
-    down_low = lax.ppermute(low, "yh", down)
-    far_low = lax.ppermute(up_low, "yh", up)
-    far_high = lax.ppermute(down_high, "yh", down)
-    return (block, up_low, up_high, down_low, down_high, far_low, far_high)
+    up_mine = lax.ppermute(mine, "yh", up)
+    down_other = lax.ppermute(other, "yh", down)
+    up_other = lax.ppermute(other, "yh", up)
+    down_mine = lax.ppermute(mine, "yh", down)
+    far_mine = lax.ppermute(up_mine, "yh", up)
+    far_other = lax.ppermute(down_other, "yh", down)
+    return (mine, other, up_mine, up_other, down_mine, down_other, far_mine, far_other)
 
 
 def layer(
@@ -359,7 +422,6 @@
     near = lax.ppermute(mine, tp, NEAR)
 
     slots, cols = call(meta_body, (sds((8, TOK), f32), sds((TOK, 128), f32)), 2)(chosen, scores)
-
     def picked(mine):
         return call(
             functools.partial(pick_body, mine),
@@ -392,27 +454,43 @@
         [pltpu.VMEM((TOK, 256), bf16)],
     )(mixed, mine, near, slots)
     arrived = lax.all_to_all(send.reshape(SP, CAP, 256), "sp", 0, 0, tiled=True)
-    block = jnp.concatenate([arrived.reshape(2, HALF, 256), shared], axis=1)
-    block = lax.all_to_all(block, "c", 0, 0, tiled=True)
-    x_ring = ring(block)
+    rows, give = call(split_body, (sds((BLOCK, 256)), sds((BLOCK, 256))), 2)(
+        arrived.reshape(SP * CAP, 256), shared
+    )
+    got = lax.ppermute(give, "c", swap)
+    x_ring = ring(rows, got)
     w_got_c = lax.ppermute(w_got, "c", swap)
     weights = (w_own, w_got, w_own_c, w_got_c)
 
+    near_parts = call(
+        up_near_body,
+        (sds((USED, 128), f32), sds((4, HALF, 256), f32), sds((SHARE, 256), f32)),
+        10,
+        [pltpu.VMEM((USED, 3 * 512), bf16)],
+        limit=16,
+    )(*x_ring[:6], *weights)
     hidden = call(
-        up_body,
-        sds((2, HROWS, 256)),
-        11,
-        [pltpu.VMEM((USED, D), bf16), pltpu.VMEM((SHARE, 128), f32)],
-        limit=16,
-    )(*x_ring, *weights)
-    h_ring = ring(hidden)
-    back, give, skeep, sgive = call(
-        down_body,
-        (sds((2, HALF, 256)), sds((HALF, 256)), sds((SHARE, 256), f32), sds((SHARE, 256), f32)),
-        11,
+        up_far_body,
+        (sds((HROWS, 256)), sds((HROWS, 256))),
+        9,
+        [pltpu.VMEM((USED, 512), bf16), pltpu.VMEM((SHARE, 128), f32)],
+        limit=12,
+    )(*x_ring[6:], *weights, *near_parts)
+    h_ring = ring(*hidden)
+    near_parts = call(
+        down_near_body,
+        (sds((2, HALF, 256), f32), sds((2, SHARE, 256), f32)),
+        10,
         [pltpu.VMEM((SHARE, 128), f32)],
         limit=12,
-    )(*h_ring, *weights)
+    )(*h_ring[:6], *weights)
+    back, give, skeep, sgive = call(
+        down_far_body,
+        (sds((2, HALF, 256)), sds((HALF, 256)), sds((SHARE, 256), f32), sds((SHARE, 256), f32)),
+        8,
+        [pltpu.VMEM((SHARE, 128), f32)],
+        limit=12,
+    )(*h_ring[6:], *weights, *near_parts)
     got = lax.ppermute(give, "c", swap)
     sgot = lax.ppermute(sgive, "c", swap)
     back = lax.dynamic_update_index_in_dim(back, got, 1 - c, 0)

time: 219 us -> 206 us (0.941)
  waiting for transfers between devices: 81.8 us -> 64 us
  starting transfers between devices: 67.7 us -> 79.6 us
  blocking collectives: 53.1 us -> 47.1 us
    ppermute x12, waiting for transfers between devices: 40.9 us -> 26.6 us  [the longest x2 10.8 us: ring(): down_mine = lax.ppermute(mine, 'yh', down)]
    all_to_all x1 -> x0, blocking collectives: 6.08 us -> none  [layer(): block = lax.all_to_all(block, 'c', 0, 0, tiled=True)]
    ppermute x1 -> x2, starting transfers between devices: 2.54 us -> 7.03 us  [layer(): got = lax.ppermute(give, 'c', swap)]
    ppermute x1, starting transfers between devices: 1.92 us -> 4.96 us  [layer(): other = lax.ppermute(other, tp, NEAR)]
    ppermute x1, waiting for transfers between devices: 5.7 us -> 3.04 us  [layer(): other = lax.ppermute(other, tp, NEAR)]
    all_to_all x1, starting transfers between devices: 3.88 us -> 6.09 us  [layer(): back = lax.all_to_all(back.reshape(SP, CAP, 256), 'sp', 0, 0, tiled=True)]
    pallas_call x2 -> x5, Pallas kernels: 5.5 us -> 4.83 us  [the longest x1 1.73 us: layer(): call(up_near_body, (sds((USED, 128), f32), sds((4, HALF, 256), f32), sds(...]
  transfers between devices with their start and end apart: 22 -> 23, of which waited for: 14 -> 13; matrix products, arithmetic and copies ran while one was open for 0% -> 0% of each run, Pallas kernels for 2% -> 4%
where the time goes in v4:
time: 206 us; the launch traced here: 204 us
  starting transfers between devices  79.6 us (39%)
  waiting for transfers between devices  64 us (31%)
  blocking collectives  47.1 us (23%)
  Pallas kernels  12.5 us (6%)
    all_to_all x1, blocking collectives, layer(): arrived = lax.all_to_all(send.reshape(SP, CAP, 256), 'sp', 0, 0, tiled=True)  28.1 us
    ppermute x1, waiting for transfers between devices, layer(): w_got = lax.ppermute(w_other, tp, NEAR)  20.6 us
    all_gather x1, blocking collectives, layer(): mixed = lax.all_gather(mixed, tp, axis=0, tiled=True)  18.9 us
    ppermute x2, waiting for transfers between devices, ring(): down_mine = lax.ppermute(mine, 'yh', down)  10.8 us
    all_to_all x1, waiting for transfers between devices, layer(): back = lax.all_to_all(back.reshape(SP, CAP, 256), 'sp', 0, 0, tiled=True)  10.4 us
    ppermute x2, starting transfers between devices, ring(): far_other = lax.ppermute(down_other, 'yh', down)  9.51 us
    ppermute x2, starting transfers between devices, ring(): down_other = lax.ppermute(other, 'yh', down)  8.36 us
    ppermute x2, starting transfers between devices, ring(): down_mine = lax.ppermute(mine, 'yh', down)  8.11 us
  transfers between devices with their start and end apart: 23, of which 13 were waited for; matrix products, arithmetic and copies ran while one was open for 0% of the time, Pallas kernels for 4%

profile of v4, /device:TPU:1, one launch (start us, length us, event | category | flops | bytes accessed | tf_op | source)
XLA Modules:
  0.0 204.1 jit_solution(8660301699934667848)
XLA Ops:
  1.1 5.9 %collective-permute-start.2 = (bf16[904,128]{1,0:T(8,128)(2,1)S(1)}, bf16[904,128]{1,0:T(8,128)(2,1)S(1)}, u32[]{:S(2)}, u32[]{:S(2)}) collective-permute-start(bf16[904,128]{1,0:T(8,128)(2,1)S(1)} %get-tuple-element.43.mine), channel_id=1, source_target_pairs={{0,2},{2,0},{4,6},{6,4},{8,10},{10,8},{12,14},{14,12},{1,15},{3,5}... | collective-permute-start | bytes 694280 | tf_op jit(solution)/shard_map/ppermute | solution.py:422
  7.0 3.1 %collective-permute-start = (bf16[32,1]{1,0:T(8,128)(2,1)S(1)}, bf16[32,1]{1,0:T(8,128)(2,1)S(1)}, u32[]{:S(2)}, u32[]{:S(2)}) collective-permute-start(bf16[32,1]{1,0:T(8,128)(2,1)S(1)} %get-tuple-element.41), channel_id=1, source_target_pairs={{0,16},{16,32},{32,48},{48,64},{64,80},{80,96},{96,112},{112,128},... | collective-permute-start | bytes 200 | tf_op jit(solution)/shard_map/ppermute | solution.py:420
  15.0 18.9 %all_gather.3.mixed = bf16[512,384]{1,0:T(8,128)(2,1)S(1)} all-gather(bf16[32,384]{1,0:T(8,128)(2,1)S(1)} %shard_map.146), channel_id=1, replica_groups=mesh['sp'=32,'yh'=4,'yl'=2,'c'=2] {'yh','yl','c'}, dimensions={0}, use_global_device_ids=true | all-gather | bytes 417792 | tf_op jit(solution)/shard_map/all_gather | solution.py:446
  39.9 20.6 %collective-permute-done.8.refs_7_.refs_3_ = bf16[7680,128]{1,0:T(8,128)(2,1)S(1)} collective-permute-done((bf16[7680,128]{1,0:T(8,128)(2,1)S(1)}, bf16[7680,128]{1,0:T(8,128)(2,1)S(1)}, u32[]{:S(2)}, u32[]{:S(2)}) %collective-permute-start.8) | collective-permute-done | bytes 1966112 | tf_op jit(solution)/shard_map/ppermute | solution.py:448
  63.7 28.1 %all_to_all.10 = bf16[32,24,256]{2,1,0:T(8,128)(2,1)S(1)} all-to-all(bf16[32,24,256]{2,1,0:T(8,128)(2,1)S(1)} %bitcast.13), channel_id=1, replica_groups=mesh['sp'=32,'yh'=4,'yl'=2,'c'=2] {'sp'}, dimensions={0} | all-to-all | bytes 786432 | tf_op jit(solution)/shard_map/all_to_all | solution.py:456
  91.9 4.2 %collective-permute-start.5 = (bf16[488,256]{1,0:T(8,128)(2,1)S(1)}, bf16[488,256]{1,0:T(8,128)(2,1)S(1)}, u32[]{:S(2)}, u32[]{:S(2)}) collective-permute-start(bf16[488,256]{1,0:T(8,128)(2,1)S(1)} %get-tuple-element.55), channel_id=1, source_target_pairs={{0,1},{1,0},{2,3},{3,2},{4,5},{5,4},{6,7},{7,6},{8,9},{9,8},{10,11... | collective-permute-start | bytes 749576 | tf_op jit(solution)/shard_map/ppermute | solution.py:460
  96.2 2.6 %collective-permute-start.12 = (bf16[488,256]{1,0:T(8,128)(2,1)S(1)}, bf16[488,256]{1,0:T(8,128)(2,1)S(1)}, u32[]{:S(2)}, u32[]{:S(2)}) collective-permute-start(bf16[488,256]{1,0:T(8,128)(2,1)S(1)} %get-tuple-element.54.refs_0_), channel_id=1, source_target_pairs={{4,0},{8,4},{12,8},{0,12},{5,1},{9,5},{13,9},{1,13},{6,2},{10,6},{... | collective-permute-start | bytes 749576 | tf_op jit(solution)/shard_map/ppermute | solution.py:354
  98.8 3.5 %collective-permute-start.3 = (bf16[488,256]{1,0:T(8,128)(2,1)S(1)}, bf16[488,256]{1,0:T(8,128)(2,1)S(1)}, u32[]{:S(2)}, u32[]{:S(2)}) collective-permute-start(bf16[488,256]{1,0:T(8,128)(2,1)S(1)} %get-tuple-element.54.refs_0_), channel_id=1, source_target_pairs={{0,4},{4,8},{8,12},{12,0},{1,5},{5,9},{9,13},{13,1},{2,6},{6,10},{... | collective-permute-start | bytes 749576 | tf_op jit(solution)/shard_map/ppermute | solution.py:351
  102.4 3.8 %collective-permute-start.6 = (bf16[488,256]{1,0:T(8,128)(2,1)S(1)}, bf16[488,256]{1,0:T(8,128)(2,1)S(1)}, u32[]{:S(2)}, u32[]{:S(2)}) collective-permute-start(bf16[488,256]{1,0:T(8,128)(2,1)S(1)} %collective-permute-done.5.refs_1_), channel_id=1, source_target_pairs={{4,0},{8,4},{12,8},{0,12},{5,1},{9,5},{13,9},{1,13},{6,2},{10,6},{... | collective-permute-start | bytes 749576 | tf_op jit(solution)/shard_map/ppermute | solution.py:352
  106.2 9.6 %collective-permute-done.12.refs_4_ = bf16[488,256]{1,0:T(8,128)(2,1)S(1)} collective-permute-done((bf16[488,256]{1,0:T(8,128)(2,1)S(1)}, bf16[488,256]{1,0:T(8,128)(2,1)S(1)}, u32[]{:S(2)}, u32[]{:S(2)}) %collective-permute-start.12) | collective-permute-done | bytes 249888 | tf_op jit(solution)/shard_map/ppermute | solution.py:354
  117.7 4.5 %collective-permute-start.4 = (bf16[488,256]{1,0:T(8,128)(2,1)S(1)}, bf16[488,256]{1,0:T(8,128)(2,1)S(1)}, u32[]{:S(2)}, u32[]{:S(2)}) collective-permute-start(bf16[488,256]{1,0:T(8,128)(2,1)S(1)} %collective-permute-done.3.refs_2_), channel_id=1, source_target_pairs={{0,4},{4,8},{8,12},{12,0},{1,5},{5,9},{9,13},{13,1},{2,6},{6,10},{... | collective-permute-start | bytes 749576 | tf_op jit(solution)/shard_map/ppermute | solution.py:355
  122.6 4.0 %collective-permute-start.7 = (bf16[488,256]{1,0:T(8,128)(2,1)S(1)}, bf16[488,256]{1,0:T(8,128)(2,1)S(1)}, u32[]{:S(2)}, u32[]{:S(2)}) collective-permute-start(bf16[488,256]{1,0:T(8,128)(2,1)S(1)} %collective-permute-done.6.refs_5_), channel_id=1, source_target_pairs={{4,0},{8,4},{12,8},{0,12},{5,1},{9,5},{13,9},{1,13},{6,2},{10,6},{... | collective-permute-start | bytes 749576 | tf_op jit(solution)/shard_map/ppermute | solution.py:356
  126.7 5.8 %collective-permute-done.11.refs_3_ = bf16[488,256]{1,0:T(8,128)(2,1)S(1)} collective-permute-done((bf16[488,256]{1,0:T(8,128)(2,1)S(1)}, bf16[488,256]{1,0:T(8,128)(2,1)S(1)}, u32[]{:S(2)}, u32[]{:S(2)}) %collective-permute-start.11) | collective-permute-done | bytes 249888 | tf_op jit(solution)/shard_map/ppermute | solution.py:353
  134.3 3.7 %collective-permute-done.4.refs_0_ = bf16[488,256]{1,0:T(8,128)(2,1)S(1)} collective-permute-done((bf16[488,256]{1,0:T(8,128)(2,1)S(1)}, bf16[488,256]{1,0:T(8,128)(2,1)S(1)}, u32[]{:S(2)}, u32[]{:S(2)}) %collective-permute-start.4) | collective-permute-done | bytes 249888 | tf_op jit(solution)/shard_map/ppermute | solution.py:355
  139.1 2.9 %collective-permute-start.13 = (bf16[408,256]{1,0:T(8,128)(2,1)S(1)}, bf16[408,256]{1,0:T(8,128)(2,1)S(1)}, u32[]{:S(2)}, u32[]{:S(2)}) collective-permute-start(bf16[408,256]{1,0:T(8,128)(2,1)S(1)} %get-tuple-element.60.refs_0_), channel_id=1, source_target_pairs={{0,4},{4,8},{8,12},{12,0},{1,5},{5,9},{9,13},{13,1},{2,6},{6,10},{... | collective-permute-start | bytes 626696 | tf_op jit(solution)/shard_map/ppermute | solution.py:351
  142.0 4.5 %collective-permute-start.15 = (bf16[408,256]{1,0:T(8,128)(2,1)S(1)}, bf16[408,256]{1,0:T(8,128)(2,1)S(1)}, u32[]{:S(2)}, u32[]{:S(2)}) collective-permute-start(bf16[408,256]{1,0:T(8,128)(2,1)S(1)} %get-tuple-element.61.refs_1_), channel_id=1, source_target_pairs={{4,0},{8,4},{12,8},{0,12},{5,1},{9,5},{13,9},{1,13},{6,2},{10,6},{... | collective-permute-start | bytes 626696 | tf_op jit(solution)/shard_map/ppermute | solution.py:352
  148.4 5.5 %collective-permute-start.18 = (bf16[408,256]{1,0:T(8,128)(2,1)S(1)}, bf16[408,256]{1,0:T(8,128)(2,1)S(1)}, u32[]{:S(2)}, u32[]{:S(2)}) collective-permute-start(bf16[408,256]{1,0:T(8,128)(2,1)S(1)} %get-tuple-element.60.refs_0_), channel_id=1, source_target_pairs={{4,0},{8,4},{12,8},{0,12},{5,1},{9,5},{13,9},{1,13},{6,2},{10,6},{... | collective-permute-start | bytes 626696 | tf_op jit(solution)/shard_map/ppermute | solution.py:354
  155.8 5.5 %collective-permute-start.16 = (bf16[408,256]{1,0:T(8,128)(2,1)S(1)}, bf16[408,256]{1,0:T(8,128)(2,1)S(1)}, u32[]{:S(2)}, u32[]{:S(2)}) collective-permute-start(bf16[408,256]{1,0:T(8,128)(2,1)S(1)} %collective-permute-done.15.refs_5_), channel_id=1, source_target_pairs={{4,0},{8,4},{12,8},{0,12},{5,1},{9,5},{13,9},{1,13},{6,2},{10,6},{... | collective-permute-start | bytes 626696 | tf_op jit(solution)/shard_map/ppermute | solution.py:356
  163.4 3.3 %collective-permute-done.14.refs_0_ = bf16[408,256]{1,0:T(8,128)(2,1)S(1)} collective-permute-done((bf16[408,256]{1,0:T(8,128)(2,1)S(1)}, bf16[408,256]{1,0:T(8,128)(2,1)S(1)}, u32[]{:S(2)}, u32[]{:S(2)}) %collective-permute-start.14) | collective-permute-done | bytes 208928 | tf_op jit(solution)/shard_map/ppermute | solution.py:355
  170.3 2.8 %collective-permute-start.19 = (bf16[384,256]{1,0:T(8,128)(2,1)S(1)}, bf16[384,256]{1,0:T(8,128)(2,1)S(1)}, u32[]{:S(2)}, u32[]{:S(2)}) collective-permute-start(bf16[384,256]{1,0:T(8,128)(2,1)S(1)} %get-tuple-element.65), channel_id=1, source_target_pairs={{0,1},{1,0},{2,3},{3,2},{4,5},{5,4},{6,7},{7,6},{8,9},{9,8},{10,11... | collective-permute-start | bytes 589832 | tf_op jit(solution)/shard_map/ppermute | solution.py:494
  174.9 6.1 %all-to-all-start.1 = ((bf16[32,24,256]{2,1,0:T(8,128)(2,1)}), bf16[32,24,256]{2,1,0:T(8,128)(2,1)S(1)}, u32[]{:S(2)}, u32[]{:S(2)}) async-start(bf16[32,24,256]{2,1,0:T(8,128)(2,1)} %bitcast.8), calls=%async_computation.1 | async-start | bytes 786432 | tf_op jit(solution)/shard_map/all_to_all | solution.py:497
  184.4 10.4 %all-to-all-done.1 = bf16[32,24,256]{2,1,0:T(8,128)(2,1)S(1)} async-done(((bf16[32,24,256]{2,1,0:T(8,128)(2,1)}), bf16[32,24,256]{2,1,0:T(8,128)(2,1)S(1)}, u32[]{:S(2)}, u32[]{:S(2)}) %all-to-all-start.1) | async-done | bytes 393248 | tf_op jit(solution)/shard_map/all_to_all | solution.py:497
  195.4 5.0 %collective-permute-start.21 = (f32[384,128]{1,0:T(8,128)S(1)}, f32[384,128]{1,0:T(8,128)S(1)}, u32[]{:S(2)}, u32[]{:S(2)}) collective-permute-start(f32[384,128]{1,0:T(8,128)S(1)} %get-tuple-element.70), channel_id=1, source_target_pairs={{0,2},{2,0},{4,6},{6,4},{8,10},{10,8},{12,14},{14,12},{1,15},{3,5}... | collective-permute-start | bytes 589832 | tf_op jit(solution)/shard_map/ppermute | solution.py:501
  200.4 3.0 %collective-permute-done.21.other = f32[384,128]{1,0:T(8,128)S(1)} collective-permute-done((f32[384,128]{1,0:T(8,128)S(1)}, f32[384,128]{1,0:T(8,128)S(1)}, u32[]{:S(2)}, u32[]{:S(2)}) %collective-permute-start.21) | collective-permute-done | bytes 196640 | tf_op jit(solution)/shard_map/ppermute | solution.py:501
  (38 shorter events, 36.3 us)
Async XLA Ops:
  1.1 13.9 %collective-permute-start.2 = (bf16[904,128]{1,0:T(8,128)(2,1)S(1)}, bf16[904,128]{1,0:T(8,128)(2,1)S(1)}, u32[]{:S(2)}, u32[]{:S(2)}) collective-permute-start(bf16[904,128]{1,0:T(8,128)(2,1)S(1)} %get-tuple-element.43.mine), channel_id=1, source_target_pairs={{0,2},{2,0},{4,6},{6,4},{8,10},{10,8},{12,14},{14,12},{1,15},{3,5}... | collective-permute-start | bytes 694280 | tf_op jit(solution)/shard_map/ppermute | solution.py:422
  7.0 6.4 %collective-permute-start = (bf16[32,1]{1,0:T(8,128)(2,1)S(1)}, bf16[32,1]{1,0:T(8,128)(2,1)S(1)}, u32[]{:S(2)}, u32[]{:S(2)}) collective-permute-start(bf16[32,1]{1,0:T(8,128)(2,1)S(1)} %get-tuple-element.41), channel_id=1, source_target_pairs={{0,16},{16,32},{32,48},{48,64},{64,80},{80,96},{96,112},{112,128},... | collective-permute-start | bytes 200 | tf_op jit(solution)/shard_map/ppermute | solution.py:420
  10.2 4.7 %collective-permute-start.1 = (bf16[32,1]{1,0:T(8,128)(2,1)S(1)}, bf16[32,1]{1,0:T(8,128)(2,1)S(1)}, u32[]{:S(2)}, u32[]{:S(2)}) collective-permute-start(bf16[32,1]{1,0:T(8,128)(2,1)S(1)} %get-tuple-element.42), channel_id=1, source_target_pairs={{16,0},{32,16},{48,32},{64,48},{80,64},{96,80},{112,96},{128,112},... | collective-permute-start | bytes 200 | tf_op jit(solution)/shard_map/ppermute | solution.py:421
  33.9 26.6 %collective-permute-start.8 = (bf16[7680,128]{1,0:T(8,128)(2,1)S(1)}, bf16[7680,128]{1,0:T(8,128)(2,1)S(1)}, u32[]{:S(2)}, u32[]{:S(2)}) collective-permute-start(bf16[7680,128]{1,0:T(8,128)(2,1)S(1)} %shard_map.147), channel_id=1, source_target_pairs={{0,2},{2,0},{4,6},{6,4},{8,10},{10,8},{12,14},{14,12},{1,15},{3,5}... | collective-permute-start | bytes 5898248 | tf_op jit(solution)/shard_map/ppermute | solution.py:448
  37.8 94.7 %collective-permute-start.9 = (bf16[7680,128]{1,0:T(8,128)(2,1)S(1)}, bf16[7680,128]{1,0:T(8,128)(2,1)S(1)}, u32[]{:S(2)}, u32[]{:S(2)}) collective-permute-start(bf16[7680,128]{1,0:T(8,128)(2,1)S(1)} %shard_map.151.refs_6_.refs_2_), channel_id=1, source_target_pairs={{0,1},{1,0},{2,3},{3,2},{4,5},{5,4},{6,7},{7,6},{8,9},{9,8},{10,11... | collective-permute-start | bytes 5898248 | tf_op jit(solution)/shard_map/ppermute | solution.py:449
  60.5 72.0 %collective-permute-start.10 = (bf16[7680,128]{1,0:T(8,128)(2,1)S(1)}, bf16[7680,128]{1,0:T(8,128)(2,1)S(1)}, u32[]{:S(2)}, u32[]{:S(2)}) collective-permute-start(bf16[7680,128]{1,0:T(8,128)(2,1)S(1)} %collective-permute-done.8.refs_7_.refs_3_), channel_id=1, source_target_pairs={{0,1},{1,0},{2,3},{3,2},{4,5},{5,4},{6,7},{7,6},{8,9},{9,8},{10,11... | collective-permute-start | bytes 5898248 | tf_op jit(solution)/shard_map/ppermute | solution.py:462
  91.9 10.4 %collective-permute-start.5 = (bf16[488,256]{1,0:T(8,128)(2,1)S(1)}, bf16[488,256]{1,0:T(8,128)(2,1)S(1)}, u32[]{:S(2)}, u32[]{:S(2)}) collective-permute-start(bf16[488,256]{1,0:T(8,128)(2,1)S(1)} %get-tuple-element.55), channel_id=1, source_target_pairs={{0,1},{1,0},{2,3},{3,2},{4,5},{5,4},{6,7},{7,6},{8,9},{9,8},{10,11... | collective-permute-start | bytes 749576 | tf_op jit(solution)/shard_map/ppermute | solution.py:460
  96.2 19.7 %collective-permute-start.12 = (bf16[488,256]{1,0:T(8,128)(2,1)S(1)}, bf16[488,256]{1,0:T(8,128)(2,1)S(1)}, u32[]{:S(2)}, u32[]{:S(2)}) collective-permute-start(bf16[488,256]{1,0:T(8,128)(2,1)S(1)} %get-tuple-element.54.refs_0_), channel_id=1, source_target_pairs={{4,0},{8,4},{12,8},{0,12},{5,1},{9,5},{13,9},{1,13},{6,2},{10,6},{... | collective-permute-start | bytes 749576 | tf_op jit(solution)/shard_map/ppermute | solution.py:354
  98.8 18.9 %collective-permute-start.3 = (bf16[488,256]{1,0:T(8,128)(2,1)S(1)}, bf16[488,256]{1,0:T(8,128)(2,1)S(1)}, u32[]{:S(2)}, u32[]{:S(2)}) collective-permute-start(bf16[488,256]{1,0:T(8,128)(2,1)S(1)} %get-tuple-element.54.refs_0_), channel_id=1, source_target_pairs={{0,4},{4,8},{8,12},{12,0},{1,5},{5,9},{9,13},{13,1},{2,6},{6,10},{... | collective-permute-start | bytes 749576 | tf_op jit(solution)/shard_map/ppermute | solution.py:351
  102.4 20.3 %collective-permute-start.6 = (bf16[488,256]{1,0:T(8,128)(2,1)S(1)}, bf16[488,256]{1,0:T(8,128)(2,1)S(1)}, u32[]{:S(2)}, u32[]{:S(2)}) collective-permute-start(bf16[488,256]{1,0:T(8,128)(2,1)S(1)} %collective-permute-done.5.refs_1_), channel_id=1, source_target_pairs={{4,0},{8,4},{12,8},{0,12},{5,1},{9,5},{13,9},{1,13},{6,2},{10,6},{... | collective-permute-start | bytes 749576 | tf_op jit(solution)/shard_map/ppermute | solution.py:352
  115.8 16.7 %collective-permute-start.11 = (bf16[488,256]{1,0:T(8,128)(2,1)S(1)}, bf16[488,256]{1,0:T(8,128)(2,1)S(1)}, u32[]{:S(2)}, u32[]{:S(2)}) collective-permute-start(bf16[488,256]{1,0:T(8,128)(2,1)S(1)} %collective-permute-done.5.refs_1_), channel_id=1, source_target_pairs={{0,4},{4,8},{8,12},{12,0},{1,5},{5,9},{9,13},{13,1},{2,6},{6,10},{... | collective-permute-start | bytes 749576 | tf_op jit(solution)/shard_map/ppermute | solution.py:353
  117.7 20.3 %collective-permute-start.4 = (bf16[488,256]{1,0:T(8,128)(2,1)S(1)}, bf16[488,256]{1,0:T(8,128)(2,1)S(1)}, u32[]{:S(2)}, u32[]{:S(2)}) collective-permute-start(bf16[488,256]{1,0:T(8,128)(2,1)S(1)} %collective-permute-done.3.refs_2_), channel_id=1, source_target_pairs={{0,4},{4,8},{8,12},{12,0},{1,5},{5,9},{9,13},{13,1},{2,6},{6,10},{... | collective-permute-start | bytes 749576 | tf_op jit(solution)/shard_map/ppermute | solution.py:355
  122.6 15.3 %collective-permute-start.7 = (bf16[488,256]{1,0:T(8,128)(2,1)S(1)}, bf16[488,256]{1,0:T(8,128)(2,1)S(1)}, u32[]{:S(2)}, u32[]{:S(2)}) collective-permute-start(bf16[488,256]{1,0:T(8,128)(2,1)S(1)} %collective-permute-done.6.refs_5_), channel_id=1, source_target_pairs={{4,0},{8,4},{12,8},{0,12},{5,1},{9,5},{13,9},{1,13},{6,2},{10,6},{... | collective-permute-start | bytes 749576 | tf_op jit(solution)/shard_map/ppermute | solution.py:356
  139.1 14.8 %collective-permute-start.13 = (bf16[408,256]{1,0:T(8,128)(2,1)S(1)}, bf16[408,256]{1,0:T(8,128)(2,1)S(1)}, u32[]{:S(2)}, u32[]{:S(2)}) collective-permute-start(bf16[408,256]{1,0:T(8,128)(2,1)S(1)} %get-tuple-element.60.refs_0_), channel_id=1, source_target_pairs={{0,4},{4,8},{8,12},{12,0},{1,5},{5,9},{9,13},{13,1},{2,6},{6,10},{... | collective-permute-start | bytes 626696 | tf_op jit(solution)/shard_map/ppermute | solution.py:351
  142.0 13.9 %collective-permute-start.15 = (bf16[408,256]{1,0:T(8,128)(2,1)S(1)}, bf16[408,256]{1,0:T(8,128)(2,1)S(1)}, u32[]{:S(2)}, u32[]{:S(2)}) collective-permute-start(bf16[408,256]{1,0:T(8,128)(2,1)S(1)} %get-tuple-element.61.refs_1_), channel_id=1, source_target_pairs={{4,0},{8,4},{12,8},{0,12},{5,1},{9,5},{13,9},{1,13},{6,2},{10,6},{... | collective-permute-start | bytes 626696 | tf_op jit(solution)/shard_map/ppermute | solution.py:352
  146.5 14.8 %collective-permute-start.17 = (bf16[408,256]{1,0:T(8,128)(2,1)S(1)}, bf16[408,256]{1,0:T(8,128)(2,1)S(1)}, u32[]{:S(2)}, u32[]{:S(2)}) collective-permute-start(bf16[408,256]{1,0:T(8,128)(2,1)S(1)} %get-tuple-element.61.refs_1_), channel_id=1, source_target_pairs={{0,4},{4,8},{8,12},{12,0},{1,5},{5,9},{9,13},{13,1},{2,6},{6,10},{... | collective-permute-start | bytes 626696 | tf_op jit(solution)/shard_map/ppermute | solution.py:353
  148.4 14.1 %collective-permute-start.18 = (bf16[408,256]{1,0:T(8,128)(2,1)S(1)}, bf16[408,256]{1,0:T(8,128)(2,1)S(1)}, u32[]{:S(2)}, u32[]{:S(2)}) collective-permute-start(bf16[408,256]{1,0:T(8,128)(2,1)S(1)} %get-tuple-element.60.refs_0_), channel_id=1, source_target_pairs={{4,0},{8,4},{12,8},{0,12},{5,1},{9,5},{13,9},{1,13},{6,2},{10,6},{... | collective-permute-start | bytes 626696 | tf_op jit(solution)/shard_map/ppermute | solution.py:354
  153.9 12.8 %collective-permute-start.14 = (bf16[408,256]{1,0:T(8,128)(2,1)S(1)}, bf16[408,256]{1,0:T(8,128)(2,1)S(1)}, u32[]{:S(2)}, u32[]{:S(2)}) collective-permute-start(bf16[408,256]{1,0:T(8,128)(2,1)S(1)} %collective-permute-done.13.refs_2_), channel_id=1, source_target_pairs={{0,4},{4,8},{8,12},{12,0},{1,5},{5,9},{9,13},{13,1},{2,6},{6,10},{... | collective-permute-start | bytes 626696 | tf_op jit(solution)/shard_map/ppermute | solution.py:355
  155.8 13.4 %collective-permute-start.16 = (bf16[408,256]{1,0:T(8,128)(2,1)S(1)}, bf16[408,256]{1,0:T(8,128)(2,1)S(1)}, u32[]{:S(2)}, u32[]{:S(2)}) collective-permute-start(bf16[408,256]{1,0:T(8,128)(2,1)S(1)} %collective-permute-done.15.refs_5_), channel_id=1, source_target_pairs={{4,0},{8,4},{12,8},{0,12},{5,1},{9,5},{13,9},{1,13},{6,2},{10,6},{... | collective-permute-start | bytes 626696 | tf_op jit(solution)/shard_map/ppermute | solution.py:356
  170.3 3.8 %collective-permute-start.19 = (bf16[384,256]{1,0:T(8,128)(2,1)S(1)}, bf16[384,256]{1,0:T(8,128)(2,1)S(1)}, u32[]{:S(2)}, u32[]{:S(2)}) collective-permute-start(bf16[384,256]{1,0:T(8,128)(2,1)S(1)} %get-tuple-element.65), channel_id=1, source_target_pairs={{0,1},{1,0},{2,3},{3,2},{4,5},{5,4},{6,7},{7,6},{8,9},{9,8},{10,11... | collective-permute-start | bytes 589832 | tf_op jit(solution)/shard_map/ppermute | solution.py:494
  174.9 20.0 %all-to-all-start.1 = ((bf16[32,24,256]{2,1,0:T(8,128)(2,1)}), bf16[32,24,256]{2,1,0:T(8,128)(2,1)S(1)}, u32[]{:S(2)}, u32[]{:S(2)}) async-start(bf16[32,24,256]{2,1,0:T(8,128)(2,1)} %bitcast.8), calls=%async_computation.1 | async-start | bytes 786432 | tf_op jit(solution)/shard_map/all_to_all | solution.py:497
  180.9 3.5 %collective-permute-start.20 = (f32[96,256]{1,0:T(8,128)S(1)}, f32[96,256]{1,0:T(8,128)S(1)}, u32[]{:S(2)}, u32[]{:S(2)}) collective-permute-start(f32[96,256]{1,0:T(8,128)S(1)} %get-tuple-element.68), channel_id=1, source_target_pairs={{0,1},{1,0},{2,3},{3,2},{4,5},{5,4},{6,7},{7,6},{8,9},{9,8},{10,11... | collective-permute-start | bytes 294920 | tf_op jit(solution)/shard_map/ppermute | solution.py:495
  195.4 8.0 %collective-permute-start.21 = (f32[384,128]{1,0:T(8,128)S(1)}, f32[384,128]{1,0:T(8,128)S(1)}, u32[]{:S(2)}, u32[]{:S(2)}) collective-permute-start(f32[384,128]{1,0:T(8,128)S(1)} %get-tuple-element.70), channel_id=1, source_target_pairs={{0,2},{2,0},{4,6},{6,4},{8,10},{10,8},{12,14},{14,12},{1,15},{3,5}... | collective-permute-start | bytes 589832 | tf_op jit(solution)/shard_map/ppermute | solution.py:501

commit v5 on v4

--- a/solution.py
+++ b/solution.py
@@ -334,11 +334,11 @@
         start = pl.multiple_of((yl * 2 + core) * SHARE, SHARE)
         acc[pl.ds(start, SHARE), :] += part[...]
     keep[...] = acc[:, 0:128]
-    give[...] = acc[:, 128:256]
+    give[...] = acc[:, 128:256].astype(bf16)
 
 
 def final_body(stream, keep, other, out):
-    out[...] = (stream[...].astype(f32) + keep[...] + other[...]).astype(bf16)
+    out[...] = (stream[...].astype(f32) + keep[...] + other[...].astype(f32)).astype(bf16)
 
 
 def sds(shape, dtype=bf16):
@@ -442,7 +442,9 @@
     mixed = call(mixer_body, sds((32, TOK)), 5)(
         gate, product, taps, before, after
     )
-    mixed, near, w_other = lax.optimization_barrier((mixed, near, w_other))
+    mixed, near, w_other, slots, cols = lax.optimization_barrier(
+        (mixed, near, w_other, slots, cols)
+    )
     mixed = lax.all_gather(mixed, tp, axis=0, tiled=True)
     mixed, w_other = lax.optimization_barrier((mixed, w_other))
     w_got = lax.ppermute(w_other, tp, NEAR)
@@ -496,7 +498,7 @@
     back = lax.dynamic_update_index_in_dim(back, got, 1 - c, 0)
     back = lax.all_to_all(back.reshape(SP, CAP, 256), "sp", 0, 0, tiled=True)
     keep, other = call(
-        combine_body, (sds((TOK, 128), f32), sds((TOK, 128), f32)), 4, [pltpu.VMEM((TOK, 256), f32)]
+        combine_body, (sds((TOK, 128), f32), sds((TOK, 128))), 4, [pltpu.VMEM((TOK, 256), f32)]
     )(back.reshape(SP * CAP, 256), cols, skeep, sgot)
     other = lax.ppermute(other, tp, NEAR)
     return call(final_body, sds((TOK, 128)), 3)(stream, keep, other)

time: 206 us -> 205 us (level)
  transfers between devices with their start and end apart: 23 -> 23, of which waited for: 13 -> 14; matrix products, arithmetic and copies ran while one was open for 0% -> 0% of each run, Pallas kernels for 4% -> 4%
where the time goes in v5:
time: 205 us; the launch traced here: 203 us
  starting transfers between devices  79.5 us (39%)
  waiting for transfers between devices  62.8 us (31%)
  blocking collectives  47.1 us (23%)
  Pallas kernels  12.5 us (6%)
    all_to_all x1, blocking collectives, layer(): arrived = lax.all_to_all(send.reshape(SP, CAP, 256), 'sp', 0, 0, tiled=True)  28.1 us
    ppermute x1, waiting for transfers between devices, layer(): w_got = lax.ppermute(w_other, tp, NEAR)  20.6 us
    all_gather x1, blocking collectives, layer(): mixed = lax.all_gather(mixed, tp, axis=0, tiled=True)  18.9 us
    ppermute x2, waiting for transfers between devices, ring(): down_mine = lax.ppermute(mine, 'yh', down)  10.4 us
    all_to_all x1, waiting for transfers between devices, layer(): back = lax.all_to_all(back.reshape(SP, CAP, 256), 'sp', 0, 0, tiled=True)  10.4 us
    ppermute x2, starting transfers between devices, ring(): far_other = lax.ppermute(down_other, 'yh', down)  9.5 us
    ppermute x2, starting transfers between devices, ring(): down_other = lax.ppermute(other, 'yh', down)  8.38 us
    ppermute x2, starting transfers between devices, ring(): down_mine = lax.ppermute(mine, 'yh', down)  8.11 us
  transfers between devices with their start and end apart: 23, of which 14 were waited for; matrix products, arithmetic and copies ran while one was open for 0% of the time, Pallas kernels for 4%

profile of v5, /device:TPU:1, one launch (start us, length us, event | category | flops | bytes accessed | tf_op | source)
XLA Modules:
  0.0 202.8 jit_solution(1509444272117309098)
XLA Ops:
  1.1 5.9 %collective-permute-start.2 = (bf16[904,128]{1,0:T(8,128)(2,1)S(1)}, bf16[904,128]{1,0:T(8,128)(2,1)S(1)}, u32[]{:S(2)}, u32[]{:S(2)}) collective-permute-start(bf16[904,128]{1,0:T(8,128)(2,1)S(1)} %get-tuple-element.45.mine), channel_id=1, source_target_pairs={{0,2},{2,0},{4,6},{6,4},{8,10},{10,8},{12,14},{14,12},{1,15},{3,5}... | collective-permute-start | bytes 694280 | tf_op jit(solution)/shard_map/ppermute | solution.py:422
  7.0 3.1 %collective-permute-start = (bf16[32,1]{1,0:T(8,128)(2,1)S(1)}, bf16[32,1]{1,0:T(8,128)(2,1)S(1)}, u32[]{:S(2)}, u32[]{:S(2)}) collective-permute-start(bf16[32,1]{1,0:T(8,128)(2,1)S(1)} %get-tuple-element.43), channel_id=1, source_target_pairs={{0,16},{16,32},{32,48},{48,64},{64,80},{80,96},{96,112},{112,128},... | collective-permute-start | bytes 200 | tf_op jit(solution)/shard_map/ppermute | solution.py:420
  15.0 18.9 %all_gather.3.mixed = bf16[512,384]{1,0:T(8,128)(2,1)S(1)} all-gather(bf16[32,384]{1,0:T(8,128)(2,1)S(1)} %shard_map.146), channel_id=1, replica_groups=mesh['sp'=32,'yh'=4,'yl'=2,'c'=2] {'yh','yl','c'}, dimensions={0}, use_global_device_ids=true | all-gather | bytes 417792 | tf_op jit(solution)/shard_map/all_gather | solution.py:448
  39.9 20.6 %collective-permute-done.8.refs_7_.refs_3_ = bf16[7680,128]{1,0:T(8,128)(2,1)S(1)} collective-permute-done((bf16[7680,128]{1,0:T(8,128)(2,1)S(1)}, bf16[7680,128]{1,0:T(8,128)(2,1)S(1)}, u32[]{:S(2)}, u32[]{:S(2)}) %collective-permute-start.8) | collective-permute-done | bytes 1966112 | tf_op jit(solution)/shard_map/ppermute | solution.py:450
  63.4 28.1 %all_to_all.10 = bf16[32,24,256]{2,1,0:T(8,128)(2,1)S(1)} all-to-all(bf16[32,24,256]{2,1,0:T(8,128)(2,1)S(1)} %bitcast.13), channel_id=1, replica_groups=mesh['sp'=32,'yh'=4,'yl'=2,'c'=2] {'sp'}, dimensions={0} | all-to-all | bytes 786432 | tf_op jit(solution)/shard_map/all_to_all | solution.py:458
  91.6 4.2 %collective-permute-start.5 = (bf16[488,256]{1,0:T(8,128)(2,1)S(1)}, bf16[488,256]{1,0:T(8,128)(2,1)S(1)}, u32[]{:S(2)}, u32[]{:S(2)}) collective-permute-start(bf16[488,256]{1,0:T(8,128)(2,1)S(1)} %get-tuple-element.59), channel_id=1, source_target_pairs={{0,1},{1,0},{2,3},{3,2},{4,5},{5,4},{6,7},{7,6},{8,9},{9,8},{10,11... | collective-permute-start | bytes 749576 | tf_op jit(solution)/shard_map/ppermute | solution.py:462
  95.8 2.6 %collective-permute-start.12 = (bf16[488,256]{1,0:T(8,128)(2,1)S(1)}, bf16[488,256]{1,0:T(8,128)(2,1)S(1)}, u32[]{:S(2)}, u32[]{:S(2)}) collective-permute-start(bf16[488,256]{1,0:T(8,128)(2,1)S(1)} %get-tuple-element.58.refs_0_), channel_id=1, source_target_pairs={{4,0},{8,4},{12,8},{0,12},{5,1},{9,5},{13,9},{1,13},{6,2},{10,6},{... | collective-permute-start | bytes 749576 | tf_op jit(solution)/shard_map/ppermute | solution.py:354
  98.5 3.5 %collective-permute-start.3 = (bf16[488,256]{1,0:T(8,128)(2,1)S(1)}, bf16[488,256]{1,0:T(8,128)(2,1)S(1)}, u32[]{:S(2)}, u32[]{:S(2)}) collective-permute-start(bf16[488,256]{1,0:T(8,128)(2,1)S(1)} %get-tuple-element.58.refs_0_), channel_id=1, source_target_pairs={{0,4},{4,8},{8,12},{12,0},{1,5},{5,9},{9,13},{13,1},{2,6},{6,10},{... | collective-permute-start | bytes 749576 | tf_op jit(solution)/shard_map/ppermute | solution.py:351
  102.0 3.8 %collective-permute-start.6 = (bf16[488,256]{1,0:T(8,128)(2,1)S(1)}, bf16[488,256]{1,0:T(8,128)(2,1)S(1)}, u32[]{:S(2)}, u32[]{:S(2)}) collective-permute-start(bf16[488,256]{1,0:T(8,128)(2,1)S(1)} %collective-permute-done.5.refs_1_), channel_id=1, source_target_pairs={{4,0},{8,4},{12,8},{0,12},{5,1},{9,5},{13,9},{1,13},{6,2},{10,6},{... | collective-permute-start | bytes 749576 | tf_op jit(solution)/shard_map/ppermute | solution.py:352
  105.9 9.6 %collective-permute-done.12.refs_4_ = bf16[488,256]{1,0:T(8,128)(2,1)S(1)} collective-permute-done((bf16[488,256]{1,0:T(8,128)(2,1)S(1)}, bf16[488,256]{1,0:T(8,128)(2,1)S(1)}, u32[]{:S(2)}, u32[]{:S(2)}) %collective-permute-start.12) | collective-permute-done | bytes 249888 | tf_op jit(solution)/shard_map/ppermute | solution.py:354
  117.5 4.4 %collective-permute-start.4 = (bf16[488,256]{1,0:T(8,128)(2,1)S(1)}, bf16[488,256]{1,0:T(8,128)(2,1)S(1)}, u32[]{:S(2)}, u32[]{:S(2)}) collective-permute-start(bf16[488,256]{1,0:T(8,128)(2,1)S(1)} %collective-permute-done.3.refs_2_), channel_id=1, source_target_pairs={{0,4},{4,8},{8,12},{12,0},{1,5},{5,9},{9,13},{13,1},{2,6},{6,10},{... | collective-permute-start | bytes 749576 | tf_op jit(solution)/shard_map/ppermute | solution.py:355
  122.3 4.0 %collective-permute-start.7 = (bf16[488,256]{1,0:T(8,128)(2,1)S(1)}, bf16[488,256]{1,0:T(8,128)(2,1)S(1)}, u32[]{:S(2)}, u32[]{:S(2)}) collective-permute-start(bf16[488,256]{1,0:T(8,128)(2,1)S(1)} %collective-permute-done.6.refs_5_), channel_id=1, source_target_pairs={{4,0},{8,4},{12,8},{0,12},{5,1},{9,5},{13,9},{1,13},{6,2},{10,6},{... | collective-permute-start | bytes 749576 | tf_op jit(solution)/shard_map/ppermute | solution.py:356
  126.4 5.8 %collective-permute-done.11.refs_3_ = bf16[488,256]{1,0:T(8,128)(2,1)S(1)} collective-permute-done((bf16[488,256]{1,0:T(8,128)(2,1)S(1)}, bf16[488,256]{1,0:T(8,128)(2,1)S(1)}, u32[]{:S(2)}, u32[]{:S(2)}) %collective-permute-start.11) | collective-permute-done | bytes 249888 | tf_op jit(solution)/shard_map/ppermute | solution.py:353
  133.9 3.7 %collective-permute-done.4.refs_0_ = bf16[488,256]{1,0:T(8,128)(2,1)S(1)} collective-permute-done((bf16[488,256]{1,0:T(8,128)(2,1)S(1)}, bf16[488,256]{1,0:T(8,128)(2,1)S(1)}, u32[]{:S(2)}, u32[]{:S(2)}) %collective-permute-start.4) | collective-permute-done | bytes 249888 | tf_op jit(solution)/shard_map/ppermute | solution.py:355
  138.8 2.9 %collective-permute-start.13 = (bf16[408,256]{1,0:T(8,128)(2,1)S(1)}, bf16[408,256]{1,0:T(8,128)(2,1)S(1)}, u32[]{:S(2)}, u32[]{:S(2)}) collective-permute-start(bf16[408,256]{1,0:T(8,128)(2,1)S(1)} %get-tuple-element.64.refs_0_), channel_id=1, source_target_pairs={{0,4},{4,8},{8,12},{12,0},{1,5},{5,9},{9,13},{13,1},{2,6},{6,10},{... | collective-permute-start | bytes 626696 | tf_op jit(solution)/shard_map/ppermute | solution.py:351
  141.6 4.5 %collective-permute-start.15 = (bf16[408,256]{1,0:T(8,128)(2,1)S(1)}, bf16[408,256]{1,0:T(8,128)(2,1)S(1)}, u32[]{:S(2)}, u32[]{:S(2)}) collective-permute-start(bf16[408,256]{1,0:T(8,128)(2,1)S(1)} %get-tuple-element.65.refs_1_), channel_id=1, source_target_pairs={{4,0},{8,4},{12,8},{0,12},{5,1},{9,5},{13,9},{1,13},{6,2},{10,6},{... | collective-permute-start | bytes 626696 | tf_op jit(solution)/shard_map/ppermute | solution.py:352
  148.1 5.5 %collective-permute-start.18 = (bf16[408,256]{1,0:T(8,128)(2,1)S(1)}, bf16[408,256]{1,0:T(8,128)(2,1)S(1)}, u32[]{:S(2)}, u32[]{:S(2)}) collective-permute-start(bf16[408,256]{1,0:T(8,128)(2,1)S(1)} %get-tuple-element.64.refs_0_), channel_id=1, source_target_pairs={{4,0},{8,4},{12,8},{0,12},{5,1},{9,5},{13,9},{1,13},{6,2},{10,6},{... | collective-permute-start | bytes 626696 | tf_op jit(solution)/shard_map/ppermute | solution.py:354
  155.5 5.5 %collective-permute-start.16 = (bf16[408,256]{1,0:T(8,128)(2,1)S(1)}, bf16[408,256]{1,0:T(8,128)(2,1)S(1)}, u32[]{:S(2)}, u32[]{:S(2)}) collective-permute-start(bf16[408,256]{1,0:T(8,128)(2,1)S(1)} %collective-permute-done.15.refs_5_), channel_id=1, source_target_pairs={{4,0},{8,4},{12,8},{0,12},{5,1},{9,5},{13,9},{1,13},{6,2},{10,6},{... | collective-permute-start | bytes 626696 | tf_op jit(solution)/shard_map/ppermute | solution.py:356
  163.3 2.9 %collective-permute-done.14.refs_0_ = bf16[408,256]{1,0:T(8,128)(2,1)S(1)} collective-permute-done((bf16[408,256]{1,0:T(8,128)(2,1)S(1)}, bf16[408,256]{1,0:T(8,128)(2,1)S(1)}, u32[]{:S(2)}, u32[]{:S(2)}) %collective-permute-start.14) | collective-permute-done | bytes 208928 | tf_op jit(solution)/shard_map/ppermute | solution.py:355
  166.2 2.8 %collective-permute-done.16.refs_1_ = bf16[408,256]{1,0:T(8,128)(2,1)S(1)} collective-permute-done((bf16[408,256]{1,0:T(8,128)(2,1)S(1)}, bf16[408,256]{1,0:T(8,128)(2,1)S(1)}, u32[]{:S(2)}, u32[]{:S(2)}) %collective-permute-start.16) | collective-permute-done | bytes 208928 | tf_op jit(solution)/shard_map/ppermute | solution.py:356
  170.1 2.7 %collective-permute-start.19 = (bf16[384,256]{1,0:T(8,128)(2,1)S(1)}, bf16[384,256]{1,0:T(8,128)(2,1)S(1)}, u32[]{:S(2)}, u32[]{:S(2)}) collective-permute-start(bf16[384,256]{1,0:T(8,128)(2,1)S(1)} %get-tuple-element.69), channel_id=1, source_target_pairs={{0,1},{1,0},{2,3},{3,2},{4,5},{5,4},{6,7},{7,6},{8,9},{9,8},{10,11... | collective-permute-start | bytes 589832 | tf_op jit(solution)/shard_map/ppermute | solution.py:496
  174.6 6.0 %all-to-all-start.1 = ((bf16[32,24,256]{2,1,0:T(8,128)(2,1)}), bf16[32,24,256]{2,1,0:T(8,128)(2,1)S(1)}, u32[]{:S(2)}, u32[]{:S(2)}) async-start(bf16[32,24,256]{2,1,0:T(8,128)(2,1)} %bitcast.8), calls=%async_computation.1 | async-start | bytes 786432 | tf_op jit(solution)/shard_map/all_to_all | solution.py:499
  184.1 10.4 %all-to-all-done.1 = bf16[32,24,256]{2,1,0:T(8,128)(2,1)S(1)} async-done(((bf16[32,24,256]{2,1,0:T(8,128)(2,1)}), bf16[32,24,256]{2,1,0:T(8,128)(2,1)S(1)}, u32[]{:S(2)}, u32[]{:S(2)}) %all-to-all-start.1) | async-done | bytes 393248 | tf_op jit(solution)/shard_map/all_to_all | solution.py:499
  195.1 5.0 %collective-permute-start.21 = (bf16[384,128]{1,0:T(8,128)(2,1)S(1)}, bf16[384,128]{1,0:T(8,128)(2,1)S(1)}, u32[]{:S(2)}, u32[]{:S(2)}) collective-permute-start(bf16[384,128]{1,0:T(8,128)(2,1)S(1)} %get-tuple-element.74), channel_id=1, source_target_pairs={{0,2},{2,0},{4,6},{6,4},{8,10},{10,8},{12,14},{14,12},{1,15},{3,5}... | collective-permute-start | bytes 294920 | tf_op jit(solution)/shard_map/ppermute | solution.py:503
  (38 shorter events, 35.7 us)
Async XLA Ops:
  1.1 13.9 %collective-permute-start.2 = (bf16[904,128]{1,0:T(8,128)(2,1)S(1)}, bf16[904,128]{1,0:T(8,128)(2,1)S(1)}, u32[]{:S(2)}, u32[]{:S(2)}) collective-permute-start(bf16[904,128]{1,0:T(8,128)(2,1)S(1)} %get-tuple-element.45.mine), channel_id=1, source_target_pairs={{0,2},{2,0},{4,6},{6,4},{8,10},{10,8},{12,14},{14,12},{1,15},{3,5}... | collective-permute-start | bytes 694280 | tf_op jit(solution)/shard_map/ppermute | solution.py:422
  7.0 6.7 %collective-permute-start = (bf16[32,1]{1,0:T(8,128)(2,1)S(1)}, bf16[32,1]{1,0:T(8,128)(2,1)S(1)}, u32[]{:S(2)}, u32[]{:S(2)}) collective-permute-start(bf16[32,1]{1,0:T(8,128)(2,1)S(1)} %get-tuple-element.43), channel_id=1, source_target_pairs={{0,16},{16,32},{32,48},{48,64},{64,80},{80,96},{96,112},{112,128},... | collective-permute-start | bytes 200 | tf_op jit(solution)/shard_map/ppermute | solution.py:420
  10.2 4.7 %collective-permute-start.1 = (bf16[32,1]{1,0:T(8,128)(2,1)S(1)}, bf16[32,1]{1,0:T(8,128)(2,1)S(1)}, u32[]{:S(2)}, u32[]{:S(2)}) collective-permute-start(bf16[32,1]{1,0:T(8,128)(2,1)S(1)} %get-tuple-element.44), channel_id=1, source_target_pairs={{16,0},{32,16},{48,32},{64,48},{80,64},{96,80},{112,96},{128,112},... | collective-permute-start | bytes 200 | tf_op jit(solution)/shard_map/ppermute | solution.py:421
  33.9 26.6 %collective-permute-start.8 = (bf16[7680,128]{1,0:T(8,128)(2,1)S(1)}, bf16[7680,128]{1,0:T(8,128)(2,1)S(1)}, u32[]{:S(2)}, u32[]{:S(2)}) collective-permute-start(bf16[7680,128]{1,0:T(8,128)(2,1)S(1)} %shard_map.147), channel_id=1, source_target_pairs={{0,2},{2,0},{4,6},{6,4},{8,10},{10,8},{12,14},{14,12},{1,15},{3,5}... | collective-permute-start | bytes 5898248 | tf_op jit(solution)/shard_map/ppermute | solution.py:450
  37.8 94.4 %collective-permute-start.9 = (bf16[7680,128]{1,0:T(8,128)(2,1)S(1)}, bf16[7680,128]{1,0:T(8,128)(2,1)S(1)}, u32[]{:S(2)}, u32[]{:S(2)}) collective-permute-start(bf16[7680,128]{1,0:T(8,128)(2,1)S(1)} %shard_map.151.refs_6_.refs_2_), channel_id=1, source_target_pairs={{0,1},{1,0},{2,3},{3,2},{4,5},{5,4},{6,7},{7,6},{8,9},{9,8},{10,11... | collective-permute-start | bytes 5898248 | tf_op jit(solution)/shard_map/ppermute | solution.py:451
  60.5 71.7 %collective-permute-start.10 = (bf16[7680,128]{1,0:T(8,128)(2,1)S(1)}, bf16[7680,128]{1,0:T(8,128)(2,1)S(1)}, u32[]{:S(2)}, u32[]{:S(2)}) collective-permute-start(bf16[7680,128]{1,0:T(8,128)(2,1)S(1)} %collective-permute-done.8.refs_7_.refs_3_), channel_id=1, source_target_pairs={{0,1},{1,0},{2,3},{3,2},{4,5},{5,4},{6,7},{7,6},{8,9},{9,8},{10,11... | collective-permute-start | bytes 5898248 | tf_op jit(solution)/shard_map/ppermute | solution.py:464
  91.6 10.4 %collective-permute-start.5 = (bf16[488,256]{1,0:T(8,128)(2,1)S(1)}, bf16[488,256]{1,0:T(8,128)(2,1)S(1)}, u32[]{:S(2)}, u32[]{:S(2)}) collective-permute-start(bf16[488,256]{1,0:T(8,128)(2,1)S(1)} %get-tuple-element.59), channel_id=1, source_target_pairs={{0,1},{1,0},{2,3},{3,2},{4,5},{5,4},{6,7},{7,6},{8,9},{9,8},{10,11... | collective-permute-start | bytes 749576 | tf_op jit(solution)/shard_map/ppermute | solution.py:462
  95.8 19.7 %collective-permute-start.12 = (bf16[488,256]{1,0:T(8,128)(2,1)S(1)}, bf16[488,256]{1,0:T(8,128)(2,1)S(1)}, u32[]{:S(2)}, u32[]{:S(2)}) collective-permute-start(bf16[488,256]{1,0:T(8,128)(2,1)S(1)} %get-tuple-element.58.refs_0_), channel_id=1, source_target_pairs={{4,0},{8,4},{12,8},{0,12},{5,1},{9,5},{13,9},{1,13},{6,2},{10,6},{... | collective-permute-start | bytes 749576 | tf_op jit(solution)/shard_map/ppermute | solution.py:354
  98.5 19.0 %collective-permute-start.3 = (bf16[488,256]{1,0:T(8,128)(2,1)S(1)}, bf16[488,256]{1,0:T(8,128)(2,1)S(1)}, u32[]{:S(2)}, u32[]{:S(2)}) collective-permute-start(bf16[488,256]{1,0:T(8,128)(2,1)S(1)} %get-tuple-element.58.refs_0_), channel_id=1, source_target_pairs={{0,4},{4,8},{8,12},{12,0},{1,5},{5,9},{9,13},{13,1},{2,6},{6,10},{... | collective-permute-start | bytes 749576 | tf_op jit(solution)/shard_map/ppermute | solution.py:351
  102.0 20.3 %collective-permute-start.6 = (bf16[488,256]{1,0:T(8,128)(2,1)S(1)}, bf16[488,256]{1,0:T(8,128)(2,1)S(1)}, u32[]{:S(2)}, u32[]{:S(2)}) collective-permute-start(bf16[488,256]{1,0:T(8,128)(2,1)S(1)} %collective-permute-done.5.refs_1_), channel_id=1, source_target_pairs={{4,0},{8,4},{12,8},{0,12},{5,1},{9,5},{13,9},{1,13},{6,2},{10,6},{... | collective-permute-start | bytes 749576 | tf_op jit(solution)/shard_map/ppermute | solution.py:352
  115.5 16.7 %collective-permute-start.11 = (bf16[488,256]{1,0:T(8,128)(2,1)S(1)}, bf16[488,256]{1,0:T(8,128)(2,1)S(1)}, u32[]{:S(2)}, u32[]{:S(2)}) collective-permute-start(bf16[488,256]{1,0:T(8,128)(2,1)S(1)} %collective-permute-done.5.refs_1_), channel_id=1, source_target_pairs={{0,4},{4,8},{8,12},{12,0},{1,5},{5,9},{9,13},{13,1},{2,6},{6,10},{... | collective-permute-start | bytes 749576 | tf_op jit(solution)/shard_map/ppermute | solution.py:353
  117.5 20.2 %collective-permute-start.4 = (bf16[488,256]{1,0:T(8,128)(2,1)S(1)}, bf16[488,256]{1,0:T(8,128)(2,1)S(1)}, u32[]{:S(2)}, u32[]{:S(2)}) collective-permute-start(bf16[488,256]{1,0:T(8,128)(2,1)S(1)} %collective-permute-done.3.refs_2_), channel_id=1, source_target_pairs={{0,4},{4,8},{8,12},{12,0},{1,5},{5,9},{9,13},{13,1},{2,6},{6,10},{... | collective-permute-start | bytes 749576 | tf_op jit(solution)/shard_map/ppermute | solution.py:355
  122.3 15.4 %collective-permute-start.7 = (bf16[488,256]{1,0:T(8,128)(2,1)S(1)}, bf16[488,256]{1,0:T(8,128)(2,1)S(1)}, u32[]{:S(2)}, u32[]{:S(2)}) collective-permute-start(bf16[488,256]{1,0:T(8,128)(2,1)S(1)} %collective-permute-done.6.refs_5_), channel_id=1, source_target_pairs={{4,0},{8,4},{12,8},{0,12},{5,1},{9,5},{13,9},{1,13},{6,2},{10,6},{... | collective-permute-start | bytes 749576 | tf_op jit(solution)/shard_map/ppermute | solution.py:356
  138.8 14.8 %collective-permute-start.13 = (bf16[408,256]{1,0:T(8,128)(2,1)S(1)}, bf16[408,256]{1,0:T(8,128)(2,1)S(1)}, u32[]{:S(2)}, u32[]{:S(2)}) collective-permute-start(bf16[408,256]{1,0:T(8,128)(2,1)S(1)} %get-tuple-element.64.refs_0_), channel_id=1, source_target_pairs={{0,4},{4,8},{8,12},{12,0},{1,5},{5,9},{9,13},{13,1},{2,6},{6,10},{... | collective-permute-start | bytes 626696 | tf_op jit(solution)/shard_map/ppermute | solution.py:351
  141.6 13.9 %collective-permute-start.15 = (bf16[408,256]{1,0:T(8,128)(2,1)S(1)}, bf16[408,256]{1,0:T(8,128)(2,1)S(1)}, u32[]{:S(2)}, u32[]{:S(2)}) collective-permute-start(bf16[408,256]{1,0:T(8,128)(2,1)S(1)} %get-tuple-element.65.refs_1_), channel_id=1, source_target_pairs={{4,0},{8,4},{12,8},{0,12},{5,1},{9,5},{13,9},{1,13},{6,2},{10,6},{... | collective-permute-start | bytes 626696 | tf_op jit(solution)/shard_map/ppermute | solution.py:352
  146.2 15.5 %collective-permute-start.17 = (bf16[408,256]{1,0:T(8,128)(2,1)S(1)}, bf16[408,256]{1,0:T(8,128)(2,1)S(1)}, u32[]{:S(2)}, u32[]{:S(2)}) collective-permute-start(bf16[408,256]{1,0:T(8,128)(2,1)S(1)} %get-tuple-element.65.refs_1_), channel_id=1, source_target_pairs={{0,4},{4,8},{8,12},{12,0},{1,5},{5,9},{9,13},{13,1},{2,6},{6,10},{... | collective-permute-start | bytes 626696 | tf_op jit(solution)/shard_map/ppermute | solution.py:353
  148.1 14.4 %collective-permute-start.18 = (bf16[408,256]{1,0:T(8,128)(2,1)S(1)}, bf16[408,256]{1,0:T(8,128)(2,1)S(1)}, u32[]{:S(2)}, u32[]{:S(2)}) collective-permute-start(bf16[408,256]{1,0:T(8,128)(2,1)S(1)} %get-tuple-element.64.refs_0_), channel_id=1, source_target_pairs={{4,0},{8,4},{12,8},{0,12},{5,1},{9,5},{13,9},{1,13},{6,2},{10,6},{... | collective-permute-start | bytes 626696 | tf_op jit(solution)/shard_map/ppermute | solution.py:354
  153.6 12.6 %collective-permute-start.14 = (bf16[408,256]{1,0:T(8,128)(2,1)S(1)}, bf16[408,256]{1,0:T(8,128)(2,1)S(1)}, u32[]{:S(2)}, u32[]{:S(2)}) collective-permute-start(bf16[408,256]{1,0:T(8,128)(2,1)S(1)} %collective-permute-done.13.refs_2_), channel_id=1, source_target_pairs={{0,4},{4,8},{8,12},{12,0},{1,5},{5,9},{9,13},{13,1},{2,6},{6,10},{... | collective-permute-start | bytes 626696 | tf_op jit(solution)/shard_map/ppermute | solution.py:355
  155.5 13.4 %collective-permute-start.16 = (bf16[408,256]{1,0:T(8,128)(2,1)S(1)}, bf16[408,256]{1,0:T(8,128)(2,1)S(1)}, u32[]{:S(2)}, u32[]{:S(2)}) collective-permute-start(bf16[408,256]{1,0:T(8,128)(2,1)S(1)} %collective-permute-done.15.refs_5_), channel_id=1, source_target_pairs={{4,0},{8,4},{12,8},{0,12},{5,1},{9,5},{13,9},{1,13},{6,2},{10,6},{... | collective-permute-start | bytes 626696 | tf_op jit(solution)/shard_map/ppermute | solution.py:356
  170.1 3.8 %collective-permute-start.19 = (bf16[384,256]{1,0:T(8,128)(2,1)S(1)}, bf16[384,256]{1,0:T(8,128)(2,1)S(1)}, u32[]{:S(2)}, u32[]{:S(2)}) collective-permute-start(bf16[384,256]{1,0:T(8,128)(2,1)S(1)} %get-tuple-element.69), channel_id=1, source_target_pairs={{0,1},{1,0},{2,3},{3,2},{4,5},{5,4},{6,7},{7,6},{8,9},{9,8},{10,11... | collective-permute-start | bytes 589832 | tf_op jit(solution)/shard_map/ppermute | solution.py:496
  174.6 19.9 %all-to-all-start.1 = ((bf16[32,24,256]{2,1,0:T(8,128)(2,1)}), bf16[32,24,256]{2,1,0:T(8,128)(2,1)S(1)}, u32[]{:S(2)}, u32[]{:S(2)}) async-start(bf16[32,24,256]{2,1,0:T(8,128)(2,1)} %bitcast.8), calls=%async_computation.1 | async-start | bytes 786432 | tf_op jit(solution)/shard_map/all_to_all | solution.py:499
  180.6 3.5 %collective-permute-start.20 = (f32[96,256]{1,0:T(8,128)S(1)}, f32[96,256]{1,0:T(8,128)S(1)}, u32[]{:S(2)}, u32[]{:S(2)}) collective-permute-start(f32[96,256]{1,0:T(8,128)S(1)} %get-tuple-element.72), channel_id=1, source_target_pairs={{0,1},{1,0},{2,3},{3,2},{4,5},{5,4},{6,7},{7,6},{8,9},{9,8},{10,11... | collective-permute-start | bytes 294920 | tf_op jit(solution)/shard_map/ppermute | solution.py:497
  195.1 7.0 %collective-permute-start.21 = (bf16[384,128]{1,0:T(8,128)(2,1)S(1)}, bf16[384,128]{1,0:T(8,128)(2,1)S(1)}, u32[]{:S(2)}, u32[]{:S(2)}) collective-permute-start(bf16[384,128]{1,0:T(8,128)(2,1)S(1)} %get-tuple-element.74), channel_id=1, source_target_pairs={{0,2},{2,0},{4,6},{6,4},{8,10},{10,8},{12,14},{14,12},{1,15},{3,5}... | collective-permute-start | bytes 294920 | tf_op jit(solution)/shard_map/ppermute | solution.py:503
